TPU v7x, 512 devices: a whole 4x4x16 slice. The times are simulated.
512 devices in a mesh: sp: 64 (over z, y), tp: 8 (over x, core).
Axes of the slice: x: 4, y: 4, z: 16, core: 2. Of those that a mesh axis runs over, the one named last changes fastest.
Arguments:
- latent: bfloat16 [16384, 2048], P(('sp', 'tp')), may hold values from -3 to 3
- context: bfloat16 [1024, 2048], P('sp'), may hold values from -6 to 6
- condition: float32 [2048], replicated, may hold values from -6 to 6
- ctx_cond: float32 [2048], replicated, may hold values from -6 to 6
- norm_gain: float32 [2048], replicated, may hold values from 0.1 to 1.9
- w_shift: bfloat16 [2048, 2048], P('sp', 'tp'), may hold values from -0.25 to 0.25
- w_scale: bfloat16 [2048, 2048], P('sp', 'tp'), may hold values from -0.25 to 0.25
- w_gate: bfloat16 [2048, 2048], P('sp', 'tp'), may hold values from -0.25 to 0.25
- w_query: bfloat16 [2048, 2048], P(None, 'tp'), may hold values from -0.125 to 0.125
- w_key: bfloat16 [2048, 2048], P(None, 'tp'), may hold values from -0.125 to 0.125
- w_value: bfloat16 [2048, 2048], P(None, 'tp'), may hold values from -0.125 to 0.125
- w_out: bfloat16 [2048, 2048], P('tp'), may hold values from -0.125 to 0.125
- rel_bias: float32 [16, 15, 31], replicated, may hold values from 2 to 250
Outputs:
- updated: bfloat16 [16384, 2048], P(('sp', 'tp'))
All inputs are finite; a program needn't handle non-finite values.
Results may differ from a plain program's by a relative error of at most 0.015.
Values may be sent and summed in bfloat16 or wider, within the bound.
No kernel may reach another device: no remote copies, remote signals or barrier semaphores. Data moves between devices by JAX's collectives and lax.ppermute only.
A program may use at most 64 MiB of HBM per device.

v0:
```python
import jax
import jax.numpy as jnp
from jax import lax
from jax.sharding import Mesh
from jax.sharding import PartitionSpec as P

HEADS = 16
HEAD_DIM = 128
GRID_W = 32
WIN_H = 8
WIN_W = 16
SP = ("sp_0", "sp_1")
SP_TP = ("sp_0", "sp_1", "tp")


NORM_EPS = 1e-06
NEG_BIG = -1e30


def one_axis_at_a_time(array, axes):
    for axis in axes:
        array = lax.psum(array, axis)
    return array


def sent_to_all(array, axis):
    size = lax.axis_size(axis)
    return lax.all_to_all(
        jnp.broadcast_to(array[None], (size, *array.shape)), axis, 0, 0, tiled=True
    )


def joined_along(parts, dim):
    parts = jnp.moveaxis(parts, 0, dim)
    dims = parts.shape
    return parts.reshape(*dims[:dim], dims[dim] * dims[dim + 1], *dims[dim + 2 :])


def collect(array, axis, dim):
    parts = sent_to_all(array, axis)
    return joined_along(parts, dim)


def gathered_by_axis(array, axes, dim):
    whole = array
    for number in range(len(axes) - 1, -1, -1):
        whole = lax.all_gather(whole, axes[number], axis=dim, tiled=True)
    return whole


def padded_2(cells, sides, width):
    for axis, dim in sides:
        count = lax.axis_size(axis)
        ends = count - 1
        head = lax.slice_in_dim(cells, 0, width, axis=dim)
        tail = lax.slice_in_dim(cells, cells.shape[dim] - width, cells.shape[dim], axis=dim)
        cells = jnp.concatenate(
            [
                lax.ppermute(tail, axis, [(i, (i + 1) % count) for i in range(ends)]),
                cells,
                lax.ppermute(head, axis, [((i + 1) % count, i) for i in range(ends)]),
            ],
            axis=dim,
        )
    return cells


def in_blocks(array, dim, size):
    dims = array.shape
    parts = array.reshape(*dims[:dim], size, dims[dim] // size, *dims[dim + 1 :])
    return jnp.moveaxis(parts, dim, 0)


def summed_on_arrival(array, axis, dim):
    parts = in_blocks(array, dim, lax.axis_size(axis))
    arrived = lax.all_to_all(parts, axis, split_axis=0, concat_axis=0, tiled=True)
    return arrived.astype(jnp.float32).sum(axis=0)


def rms_mod(block, norm_gain, shifts, scales):
    block = block.astype(jnp.float32)
    normed = (
        block * lax.rsqrt(jnp.mean(block * block, axis=-1, keepdims=True) + NORM_EPS) * norm_gain
    )
    return (normed * (1.0 + scales) + shifts).astype(jnp.bfloat16)


def project(block, weights):
    return jnp.stack(
        [
            jnp.dot(block, weight, preferred_element_type=jnp.float32).astype(jnp.bfloat16)
            for weight in weights
        ]
    )


def on_device(
    latent,
    context,
    condition,
    ctx_cond,
    norm_gain,
    w_shift,
    w_scale,
    w_gate,
    w_query,
    w_key,
    w_value,
    w_out,
    rel_bias,
):
    tp_size = lax.axis_size("tp")
    sp_size = lax.axis_size(SP)
    head_dev = HEADS // tp_size
    head_cols = w_query.shape[1]
    row_part = w_shift.shape[0]
    activated = jax.nn.silu(jnp.stack([condition, ctx_cond])).astype(jnp.bfloat16)
    act_rows = lax.dynamic_slice_in_dim(activated, lax.axis_index(SP) * row_part, row_part, 1)
    partial_value = jnp.concatenate(
        [
            jnp.dot(act_rows, w_shift, preferred_element_type=jnp.float32),
            jnp.dot(act_rows, w_scale, preferred_element_type=jnp.float32),
            jnp.dot(act_rows[:1], w_gate, preferred_element_type=jnp.float32),
        ],
        axis=0,
    )
    summed = one_axis_at_a_time(partial_value, SP)
    mod_vecs = collect(summed, "tp", 1)
    normed = rms_mod(latent, norm_gain, mod_vecs[0], mod_vecs[2])
    projected = project(collect(normed, "tp", 0), (w_query, w_key, w_value))
    ctx_kv = gathered_by_axis(
        project(rms_mod(context, norm_gain, mod_vecs[1], mod_vecs[3]), (w_key, w_value)), SP, 1
    )
    ctx_key3 = ctx_kv[0].reshape(-1, head_dev, HEAD_DIM)
    ctx_val3 = ctx_kv[1].reshape(-1, head_dev, HEAD_DIM)
    grid_rows = projected.shape[1] // GRID_W
    queries = projected[0].reshape(grid_rows, GRID_W, head_dev, HEAD_DIM)
    half_win = WIN_H // 2
    padded = padded_2(projected[1:].reshape(2, grid_rows, GRID_W, head_cols), ((SP, 1),), half_win)
    total_rows = grid_rows * sp_size
    first_row = lax.axis_index(SP) * grid_rows
    local_rows = jnp.arange(grid_rows, dtype=jnp.int32)
    starts = (
        jnp.clip(first_row + local_rows - half_win, 0, total_rows - WIN_H) - first_row + half_win
    )

    def take_window(start_row):
        return lax.dynamic_slice_in_dim(padded, start_row, WIN_H, 1)

    windows = jax.vmap(take_window)(starts)
    key_win = windows[:, 0].reshape(grid_rows, WIN_H, GRID_W, head_dev, HEAD_DIM)
    val_win = windows[:, 1].reshape(grid_rows, WIN_H, GRID_W, head_dev, HEAD_DIM)
    row_off = (
        starts[:, None]
        - half_win
        + jnp.arange(WIN_H, dtype=jnp.int32)[None, :]
        - local_rows[:, None]
        + WIN_H
        - 1
    )
    col_ids = jnp.arange(GRID_W, dtype=jnp.int32)
    col_start = jnp.clip(col_ids - WIN_W // 2, 0, GRID_W - WIN_W)
    col_in = (col_ids[None, :] >= col_start[:, None]) & (
        col_ids[None, :] < col_start[:, None] + WIN_W
    )
    col_off = jnp.clip(col_ids[None, :] - col_ids[:, None], 1 - WIN_W, WIN_W - 1) + WIN_W - 1
    col_hot = (col_off[:, :, None] == jnp.arange(2 * WIN_W - 1)[None, None, :]).astype(jnp.float32)
    row_hot = (row_off[:, :, None] == jnp.arange(2 * WIN_H - 1)[None, None, :]).astype(jnp.float32)
    bias_table = lax.dynamic_slice_in_dim(rel_bias, lax.axis_index("tp") * head_dev, head_dev, 0)
    col_table = jnp.einsum("hec,qwc->heqw", bias_table, col_hot, precision=lax.Precision.HIGHEST)
    bias_win = jnp.einsum("rke,heqw->rqhkw", row_hot, col_table, precision=lax.Precision.HIGHEST)
    inv_scale = HEAD_DIM ** (-0.5)
    scores_win = (
        jnp.einsum("rqhd,rkwhd->rqhkw", queries, key_win, preferred_element_type=jnp.float32)
        * inv_scale
        + bias_win
    )
    scores_win = jnp.where(col_in[None, :, None, None, :], scores_win, NEG_BIG)
    scores_win = scores_win.reshape(grid_rows, GRID_W, head_dev, WIN_H * GRID_W)
    scores_ctx = (
        jnp.einsum("rqhd,chd->rqhc", queries, ctx_key3, preferred_element_type=jnp.float32)
        * inv_scale
    )
    row_max = jnp.maximum(jnp.max(scores_win, axis=-1), jnp.max(scores_ctx, axis=-1))
    exp_win = jnp.exp(scores_win - row_max[..., None])
    exp_ctx = jnp.exp(scores_ctx - row_max[..., None])
    row_total = jnp.sum(exp_win, axis=-1) + jnp.sum(exp_ctx, axis=-1)
    probs_win = (exp_win / row_total[..., None]).astype(jnp.bfloat16)
    probs_win = probs_win.reshape(grid_rows, GRID_W, head_dev, WIN_H, GRID_W)
    probs_ctx = (exp_ctx / row_total[..., None]).astype(jnp.bfloat16)
    attended = jnp.einsum(
        "rqhkw,rkwhd->rqhd", probs_win, val_win, preferred_element_type=jnp.float32
    )
    attended = attended + jnp.einsum(
        "rqhc,chd->rqhd", probs_ctx, ctx_val3, preferred_element_type=jnp.float32
    )
    attended = attended.astype(jnp.bfloat16).reshape(grid_rows * GRID_W, head_cols)
    branch = summed_on_arrival(
        jnp.dot(attended, w_out, preferred_element_type=jnp.float32).astype(jnp.bfloat16), "tp", 0
    )
    return (latent.astype(jnp.float32) + mod_vecs[4] * branch).astype(jnp.bfloat16)


def solution(mesh):
    torus = Mesh(mesh.devices.reshape(16, 4, mesh.shape["tp"]), ("sp_0", "sp_1", "tp"))
    return jax.shard_map(
        on_device,
        mesh=torus,
        in_specs=(
            P(SP_TP, None),
            P(SP, None),
            P(),
            P(),
            P(),
            P(SP, "tp"),
            P(SP, "tp"),
            P(SP, "tp"),
            P(None, "tp"),
            P(None, "tp"),
            P(None, "tp"),
            P("tp", None),
            P(),
        ),
        out_specs=P(SP_TP, None),
        check_vma=False,
    )
```

profile of v0, /device:TPU:1, one launch (start us, length us, event | category | flops | bytes accessed | tf_op | source)
XLA Modules:
  0.0 196.9 jit_solution(1419718682703808817)
XLA Ops:
  9.9 30.8 %psum.14 = f32[5,256]{1,0:T(8,128)S(1)} all-reduce(f32[5,256]{1,0:T(8,128)S(1)} %pad_maximum_fusion.3), channel_id=1, replica_groups=mesh['sp_0'=16,'sp_1'=4,'tp'=8] {'sp_0'}, use_global_device_ids=true, to_apply=%region_0.1 | all-reduce | flops 1280 | bytes 10240 | tf_op jit(solution)/shard_map/psum | solution.py:22
  40.7 8.8 %psum.15 = f32[5,256]{1,0:T(8,128)S(1)} all-reduce(f32[5,256]{1,0:T(8,128)S(1)} %psum.14), channel_id=1, replica_groups=mesh['sp_0'=16,'sp_1'=4,'tp'=8] {'sp_1'}, use_global_device_ids=true, to_apply=%region_1.2 | all-reduce | flops 1280 | bytes 10240 | tf_op jit(solution)/shard_map/psum | solution.py:22
  50.2 14.0 %all-to-all-start = ((f32[8,5,256]{2,1,0:T(8,128)}), f32[8,5,256]{2,1,0:T(8,128)S(1)}, u32[]{:S(2)}, u32[]{:S(2)}) async-start(f32[8,5,256]{2,1,0:T(8,128)} %broadcast_in_dim.12), calls=%async_computation | async-start | bytes 131072 | tf_op jit(solution)/shard_map/all_to_all | solution.py:28
  67.2 1.4 convolution_bitcast_fusion
  69.7 2.2 %copy.76 = f32[2,32,32,8,8]{1,2,4,0,3:T(8,128)} copy(f32[2,32,32,8,8]{2,4,3,1,0:T(8,128)S(1)} %fusion.34) | data formatting | bytes 1048576 | tf_op jit(solution)/shard_map/rke,heqw->rqhkw/dot_general | solution.py:171
  72.0 1.1 broadcast_in_dim.13
  73.2 4.8 %all-to-all-start.1 = ((bf16[8,32,2048]{2,1,0:T(8,128)(2,1)}), bf16[8,32,2048]{2,1,0:T(8,128)(2,1)S(1)}, u32[]{:S(2)}, u32[]{:S(2)}) async-start(bf16[8,32,2048]{2,1,0:T(8,128)(2,1)} %broadcast_in_dim.13), calls=%async_computation.1 | async-start | bytes 2097152 | tf_op jit(solution)/shard_map/all_to_all | solution.py:28
  78.3 1.5 fusion.7
  79.8 10.1 %all_gather.6 = bf16[2,64,256]{2,1,0:T(8,128)(2,1)} all-gather(bf16[2,16,256]{2,1,0:T(8,128)(2,1)S(1)} %pad_maximum_fusion.2), channel_id=1, replica_groups=mesh['sp_0'=16,'sp_1'=4,'tp'=8] {'sp_1'}, dimensions={1}, use_global_device_ids=true | all-gather | bytes 81920 | tf_op jit(solution)/shard_map/all_gather | solution.py:47
  89.9 3.0 %all-to-all-done.1 = bf16[8,32,2048]{2,1,0:T(8,128)(2,1)S(1)} async-done(((bf16[8,32,2048]{2,1,0:T(8,128)(2,1)}), bf16[8,32,2048]{2,1,0:T(8,128)(2,1)S(1)}, u32[]{:S(2)}, u32[]{:S(2)}) %all-to-all-start.1) | async-done | bytes 1048608 | tf_op jit(solution)/shard_map/all_to_all | solution.py:28
  94.6 1.3 collective-permute-start
  95.9 1.3 collective-permute-start.1
  99.1 2.7 %collective-permute-done.1 = bf16[2,4,32,256]{3,2,0,1:T(8,128)(2,1)} collective-permute-done((bf16[2,4,32,256]{3,2,0,1:T(8,128)(2,1)S(1)}, bf16[2,4,32,256]{3,2,0,1:T(8,128)(2,1)}, u32[]{:S(2)}, u32[]{:S(2)}) %collective-permute-start.1) | collective-permute-done | bytes 131104 | tf_op jit(solution)/shard_map/ppermute | solution.py:61
  102.8 2.0 %gather_fusion = bf16[8,2,8,32,256]{4,3,1,2,0:T(8,128)(2,1)} fusion(bf16[2,16,32,256]{3,2,0,1:T(8,128)(2,1)S(1)} %pad_maximum_fusion, s32[8]{0:T(128)S(1)} %shift-left_bitcast_fusion), kind=kCustom, calls=%fused_computation | custom fusion | bytes 4194432 | tf_op jit(solution)/shard_map/vmap()/gather | solution.py:148
  104.8 3.1 %fusion.46 = (bf16[8,1,8,32,256]{4,3,1,2,0:T(8,128)(2,1)}, bf16[8,1,8,32,256]{4,3,1,2,0:T(8,128)(2,1)}) fusion(bf16[8,2,8,32,256]{4,3,1,2,0:T(8,128)(2,1)} %gather_fusion), kind=kLoop, calls=%fused_computation.92 | loop fusion | bytes 4194304 | tf_op jit(solution)/shard_map/slice | solution.py:151
  107.9 2.3 %reshape_squeeze.13 = bf16[8,8,32,2,128]{4,3,2,1,0:T(2,128)(2,1)} reshape(bf16[8,1,8,32,256]{4,3,1,2,0:T(8,128)(2,1)} %get-tuple-element.5) | data formatting | bytes 2097152 | tf_op jit(solution)/shard_map/reshape;squeeze | solution.py:151
  110.2 2.2 %reshape_squeeze.12 = bf16[8,8,32,2,128]{4,3,2,1,0:T(2,128)(2,1)} reshape(bf16[8,1,8,32,256]{4,3,1,2,0:T(8,128)(2,1)} %get-tuple-element.6) | data formatting | bytes 2097152 | tf_op jit(solution)/shard_map/reshape;squeeze | solution.py:152
  112.4 3.2 %fusion.49 = (f32[8,32,2]{1,2,0:T(2,128)S(1)}, f32[8,32,2,8,32]{1,4,3,2,0:T(8,128)}) fusion(f32[2,32,32,8,8]{1,2,4,0,3:T(8,128)S(1)} %copy-done.1, bf16[8,32,2,128,1]{3,2,1,0,4:T(2,128)(2,1)S(1)} %bitcast.118, bf16[8,8,32,2,128]{4,3,2,1,0:T(2,128)(2,1)} %reshape_squeeze.13, pred[32,32]{0,1:T(8,128)(4,1)S(1)} %fusion.37), kind=kOutput, calls=%fused_computation.95 | convolution fusion | flops 34078208 | bytes 2231296 | tf_op jit(solution)/shard_map/rqhd,rkwhd->rqhkw/dot_general | solution.py:174
  115.5 31.5 %all-gather.2.cloned.1.call-done = bf16[2,1024,256]{2,1,0:T(8,128)(2,1)} async-done(((bf16[2,64,256]{2,1,0:T(8,128)(2,1)}), bf16[2,1024,256]{2,1,0:T(8,128)(2,1)}) %all-gather.2.cloned.1.call-update) | async-done | bytes 1048592 | tf_op jit(solution)/shard_map/all_gather | solution.py:47
  147.0 2.1 %fusion.47 = (bf16[1,1024,256]{2,1,0:T(8,128)(2,1)}, bf16[1,1024,256]{2,1,0:T(8,128)(2,1)S(1)}) fusion(bf16[2,1024,256]{2,1,0:T(8,128)(2,1)} %all-gather.2.cloned.1.call-done), kind=kLoop, calls=%fused_computation.93 | loop fusion | bytes 2097152 | tf_op jit(solution)/shard_map/slice | solution.py:135
  150.0 1.5 fusion.13
  153.5 2.0 %reshape_squeeze.15 = bf16[1024,2,128]{2,1,0:T(2,128)(2,1)} reshape(bf16[1,1024,256]{2,1,0:T(8,128)(2,1)} %get-tuple-element.7) | data formatting | bytes 1048576 | tf_op jit(solution)/shard_map/reshape;squeeze | solution.py:135
  155.5 2.5 %convolution_bitcast_fusion.2 = f32[8,32,2,128]{3,1,2,0:T(8,128)S(1)} fusion(bf16[8,8,32,2,128]{4,3,2,1,0:T(2,128)(2,1)} %reshape_squeeze.12, f32[8,32,2,8,32]{1,4,3,2,0:T(8,128)} %get-tuple-element.17, f32[8,32,2]{1,2,0:T(2,128)S(1)} %copy.82, f32[8,32,2]{1,2,0:T(2,128)S(1)} %copy.80), kind=kOutput, calls=%fused_computation.16 | convolution fusion | flops 33947648 | bytes 1839104 | tf_op jit(solution)/shard_map/rqhkw,rkwhd->rqhd/dot_general | solution.py:191
  159.2 30.0 %all_to_all.15 = bf16[8,32,2048]{2,1,0:T(8,128)(2,1)S(1)} all-to-all(bf16[8,32,2048]{2,1,0:T(8,128)(2,1)S(1)} %bitcast.117), channel_id=1, replica_groups=mesh['sp_0'=16,'sp_1'=4,'tp'=8] {'tp'}, dimensions={0} | all-to-all | bytes 2097152 | tf_op jit(solution)/shard_map/all_to_all | solution.py:76
  (70 shorter events, 18.0 us)
Async XLA Ops:
  6.5 152.2 %copy-start = (bf16[256,2048]{1,0:T(8,128)(2,1)S(1)}, bf16[256,2048]{1,0:T(8,128)(2,1)}, u32[]{:S(2)}) copy-start(bf16[256,2048]{1,0:T(8,128)(2,1)} %param.24) | copy-start | bytes 3145732
  50.2 21.7 %all-to-all-start = ((f32[8,5,256]{2,1,0:T(8,128)}), f32[8,5,256]{2,1,0:T(8,128)S(1)}, u32[]{:S(2)}, u32[]{:S(2)}) async-start(f32[8,5,256]{2,1,0:T(8,128)} %broadcast_in_dim.12), calls=%async_computation | async-start | bytes 131072 | tf_op jit(solution)/shard_map/all_to_all | solution.py:28
  69.6 2.3 %copy-start.5 = (bf16[32,2048]{1,0:T(8,128)(2,1)S(1)}, bf16[32,2048]{1,0:T(8,128)(2,1)}, u32[]{:S(2)}) copy-start(bf16[32,2048]{1,0:T(8,128)(2,1)} %param.13) | copy-start | bytes 393220
  69.6 2.3 %copy-start.11 = (f32[2048]{0:T(1024)S(1)}, f32[2048]{0:T(1024)}, u32[]{:S(2)}) copy-start(f32[2048]{0:T(1024)} %param.17) | copy-start | bytes 24580
  71.8 6.1 %copy-start.3 = (bf16[2048,256]{1,0:T(8,128)(2,1)S(1)}, bf16[2048,256]{1,0:T(8,128)(2,1)}, u32[]{:S(2)}) copy-start(bf16[2048,256]{1,0:T(8,128)(2,1)} %param.22) | copy-start | bytes 3145732
  71.8 6.1 %copy-start.7 = (bf16[16,2048]{1,0:T(8,128)(2,1)S(1)}, bf16[16,2048]{1,0:T(8,128)(2,1)}, u32[]{:S(2)}) copy-start(bf16[16,2048]{1,0:T(8,128)(2,1)} %param.14) | copy-start | bytes 196612
  73.2 19.8 %all-to-all-start.1 = ((bf16[8,32,2048]{2,1,0:T(8,128)(2,1)}), bf16[8,32,2048]{2,1,0:T(8,128)(2,1)S(1)}, u32[]{:S(2)}, u32[]{:S(2)}) async-start(bf16[8,32,2048]{2,1,0:T(8,128)(2,1)} %broadcast_in_dim.13), calls=%async_computation.1 | async-start | bytes 2097152 | tf_op jit(solution)/shard_map/all_to_all | solution.py:28
  78.0 69.1 %all-gather.2.cloned.1.call-start = ((), (), s32[]{:S(2)}) async-start(), calls=%async_computation.3 | async-start | bytes 1114112 | tf_op jit(solution)/shard_map/all_gather | solution.py:47
  92.9 1.2 copy-start.4
  92.9 4.3 %copy-start.6 = (bf16[2048,256]{1,0:T(8,128)(2,1)S(1)}, bf16[2048,256]{1,0:T(8,128)(2,1)}, u32[]{:S(2)}) copy-start(bf16[2048,256]{1,0:T(8,128)(2,1)} %param.21) | copy-start | bytes 3145732
  94.6 3.8 %collective-permute-start = (bf16[2,4,32,256]{3,2,0,1:T(8,128)(2,1)S(1)}, bf16[2,4,32,256]{3,2,0,1:T(8,128)(2,1)S(1)}, u32[]{:S(2)}, u32[]{:S(2)}) collective-permute-start(bf16[2,4,32,256]{3,2,0,1:T(8,128)(2,1)S(1)} %get-tuple-element.9), channel_id=1, source_target_pairs={{0,8},{8,16},{16,24},{24,32},{32,40},{40,48},{48,56},{56,64},{64,7... | collective-permute-start | bytes 393224 | tf_op jit(solution)/shard_map/ppermute | solution.py:59
  95.9 5.8 %collective-permute-start.1 = (bf16[2,4,32,256]{3,2,0,1:T(8,128)(2,1)S(1)}, bf16[2,4,32,256]{3,2,0,1:T(8,128)(2,1)}, u32[]{:S(2)}, u32[]{:S(2)}) collective-permute-start(bf16[2,4,32,256]{3,2,0,1:T(8,128)(2,1)S(1)} %get-tuple-element.10), channel_id=1, source_target_pairs={{8,0},{16,8},{24,16},{32,24},{40,32},{48,40},{56,48},{64,56},{72,6... | collective-permute-start | bytes 393224 | tf_op jit(solution)/shard_map/ppermute | solution.py:61
  98.4 0.7 copy-start.10
  107.9 4.5 %copy-start.1 = (f32[2,32,32,8,8]{1,2,4,0,3:T(8,128)S(1)}, f32[2,32,32,8,8]{1,2,4,0,3:T(8,128)}, u32[]{:S(2)}) copy-start(f32[2,32,32,8,8]{1,2,4,0,3:T(8,128)} %copy.76) | copy-start | bytes 1572868
  115.5 34.5 %copy-start.9 = (bf16[8,32,2,128]{3,1,0,2:T(8,128)(2,1)S(1)}, bf16[8,32,2,128]{3,1,0,2:T(8,128)(2,1)}, u32[]{:S(2)}) copy-start(bf16[8,32,2,128]{3,1,0,2:T(8,128)(2,1)} %copy.78) | copy-start | bytes 393220
  151.5 1.6 copy-start.2
  155.5 2.5 %copy-start.8 = (bf16[1024,2,128]{2,1,0:T(2,128)(2,1)S(1)}, bf16[1024,2,128]{2,1,0:T(2,128)(2,1)}, u32[]{:S(2)}) copy-start(bf16[1024,2,128]{2,1,0:T(2,128)(2,1)} %reshape_squeeze.15) | copy-start | bytes 1572868
Sparse Core Ops, SparseCore 0:
  90.0 56.9 all-gather.1
where the time goes:
time: 198 us; the launch traced here: 197 us
  blocking collectives  79.7 us (40%)
  waiting for transfers between devices  37.2 us (19%)
  local copies, waits for them, and re-layouts  22.5 us (11%)
  starting transfers between devices  21.4 us (11%)
  matrix products  16.3 us (8%)
  between operations  13.7 us (7%)
  other arithmetic  6.17 us (3%)
    psum x2, blocking collectives, one_axis_at_a_time(): array = lax.psum(array, axis)  39.6 us
    all_gather x1, waiting for transfers between devices, gathered_by_axis(): whole = lax.all_gather(whole, axes[number], axis=dim, tiled=True)  31.5 us
    all_to_all x1, blocking collectives, summed_on_arrival(): lax.all_to_all(parts, axis, split_axis=0, concat_axis=0, tiled=True)  30 us
    all_to_all x2, starting transfers between devices, sent_to_all(): lax.all_to_all(jnp.broadcast_to(array[None], (size, *array.shape)), axis,...  18.8 us
    all_gather x1, blocking collectives, gathered_by_axis(): whole = lax.all_gather(whole, axes[number], axis=dim, tiled=True)  10.1 us
  transfers between devices with their start and end apart: 5, of which 3 were waited for; matrix products, arithmetic and copies ran while one was open for 13% of the time, Pallas kernels for 0%

commit v1 on v0

v1 whole, which is shorter than its diff:
```python
import functools

import jax
import jax.numpy as jnp
from jax import lax
from jax.experimental import pallas as pl
from jax.experimental.pallas import tpu as pltpu
from jax.sharding import Mesh
from jax.sharding import PartitionSpec as P

HEADS = 16
HEAD_DIM = 128
GRID_W = 32
WIN_H = 8
WIN_W = 16
D = 2048
SP = ("z", "y")
TP = ("x", "c")
ALL = ("z", "y", "x", "c")
NORM_EPS = 1e-06
NEG_BIG = -1e30
BF = jnp.bfloat16
F32 = jnp.float32


def call(body, outs, name, scratch=(), flops=0, vmem=None):
    return pl.pallas_call(
        body,
        out_shape=outs,
        scratch_shapes=list(scratch),
        name=name,
        cost_estimate=pl.CostEstimate(flops=flops, bytes_accessed=0, transcendentals=0),
        compiler_params=pltpu.CompilerParams(vmem_limit_bytes=vmem),
    )


def shape(dims, dtype):
    return jax.ShapeDtypeStruct(dims, dtype)


def mod_partial_body(cond_ref, ctxc_ref, wsh_ref, wsc_ref, wg_ref, out_ref, pad_ref):
    sp = lax.axis_index("z") * 4 + lax.axis_index("y")
    row = sp // 4
    off = pl.multiple_of((sp % 4) * 32, 32)
    cond = cond_ref[pl.ds(row, 1), :]
    ctxc = ctxc_ref[pl.ds(row, 1), :]
    act = jnp.concatenate([cond, ctxc] * 4, axis=0)
    act = (act / (1.0 + jnp.exp(-act))).astype(BF)
    pad_ref[...] = jnp.zeros_like(pad_ref)
    pad_ref[pl.ds(off, 32), 0:256] = wsh_ref[...]
    pad_ref[pl.ds(off, 32), 256:512] = wsc_ref[...]
    pad_ref[pl.ds(off, 32), 512:768] = wg_ref[...]
    res = jnp.dot(act, pad_ref[...], preferred_element_type=F32)
    row5 = jnp.concatenate(
        [res[0:1, 0:256], res[1:2, 0:256], res[0:1, 256:512], res[1:2, 256:512], res[0:1, 512:768]],
        axis=1,
    )
    for i in range(out_ref.shape[0]):
        out_ref[i] = row5


def sum_bcast_body(in_ref, out_ref):
    total = jnp.sum(in_ref[...], axis=0)
    for i in range(out_ref.shape[0]):
        out_ref[i] = total


def mod_row(mod_ref, xc, kind):
    total = mod_ref[xc, :, kind * 256 : (kind + 1) * 256]
    for y in range(1, 4):
        total = total + mod_ref[y * 8 + xc, :, kind * 256 : (kind + 1) * 256]
    return total


def normalize(load, mod_ref, gain_ref, xn_ref, rows, which):
    x = load().astype(F32)
    inv = lax.rsqrt(jnp.mean(x * x, axis=-1, keepdims=True) + NORM_EPS)
    for xc in range(8):
        cols = slice(xc * 256, (xc + 1) * 256)
        gain = gain_ref[:, cols] * (1.0 + mod_row(mod_ref, xc, 2 + which))
        xn_ref[:, cols] = (x[:, cols] * inv * gain + mod_row(mod_ref, xc, which)).astype(BF)


def ctx_kv_body(ctx_ref, mod_ref, gain_ref, wk_ref, wv_ref, out_ref, xn_ref):
    normalize(lambda: ctx_ref[...], mod_ref, gain_ref, xn_ref, 16, 1)
    xn = xn_ref[...]
    k = jnp.dot(xn, wk_ref[...], preferred_element_type=F32).astype(BF)
    v = jnp.dot(xn, wv_ref[...], preferred_element_type=F32).astype(BF)
    for i in range(out_ref.shape[0]):
        out_ref[i, 0] = k
        out_ref[i, 1] = v


def qkv_body(
    lat_ref, mod_ref, gain_ref, wq_ref, wk_ref, wv_ref, q_ref, head_ref, tail_ref, gate_ref, xn_ref
):
    normalize(lambda: lat_ref[...].reshape(256, D), mod_ref, gain_ref, xn_ref, 256, 0)
    xn = xn_ref[...]
    k = jnp.dot(xn, wk_ref[...], preferred_element_type=F32).astype(BF)
    head_ref[0] = k[:128]
    tail_ref[0] = k[128:]
    v = jnp.dot(xn, wv_ref[...], preferred_element_type=F32).astype(BF)
    head_ref[1] = v[:128]
    tail_ref[1] = v[128:]
    q_ref[...] = jnp.dot(xn, wq_ref[...], preferred_element_type=F32).astype(BF)
    for xc in range(8):
        gate_ref[:, xc * 256 : (xc + 1) * 256] = mod_row(mod_ref, xc, 4)


def bias_body(rows_total, tab_ref, out_ref, exp_ref):
    sp = lax.axis_index("z") * 4 + lax.axis_index("y")
    tp = lax.axis_index("x") * 2 + lax.axis_index("c")
    first = sp * 8
    lane = lax.broadcasted_iota(jnp.int32, (32, 128), 1)
    col = lax.broadcasted_iota(jnp.int32, (32, 128), 0)
    key_col = lane % 32
    start = jnp.clip(col - WIN_W // 2, 0, GRID_W - WIN_W)
    col_in = (key_col >= start) & (key_col < start + WIN_W)
    quarter = lane // 32
    for h in range(2):
        tab = tab_ref[tp * 2 + h]
        for d in range(15):
            line = jnp.broadcast_to(tab[d : d + 1, :], (32, 128))
            for p in range(4):
                exp_ref[d, p] = pltpu.roll(line, (32 * p - 15) % 128, 1, stride=1, stride_axis=0)
        for r in range(8):
            a = jnp.clip(first + r - WIN_H // 2, 0, rows_total - WIN_H) - first + WIN_H // 2
            half = r // 4
            for s in range(3):
                seg = half + s
                block = jnp.full((32, 128), NEG_BIG, F32)
                for p in range(4):
                    k = seg * 4 + p
                    d = k - r + 3
                    if 0 <= d < 15:
                        ok = (k >= a) & (k < a + WIN_H)
                        block = jnp.where(
                            (quarter == p) & col_in & ok, exp_ref[d, p], block
                        )
                out_ref[h, half, s, (r % 4) * 32 : (r % 4) * 32 + 32, :] = block


def attend_body(q_ref, prev_ref, head_ref, tail_ref, next_ref, bias_ref, ctx_ref, out_ref):
    core = lax.axis_index("c")
    inv = HEAD_DIM**-0.5
    segs = (prev_ref, head_ref, tail_ref, next_ref)
    nt = (((1,), (1,)), ((), ()))
    for h in range(2):
        hc = slice(h * 128, (h + 1) * 128)
        kc = ctx_ref[:, 0, :, hc].reshape(1024, 128)
        vc = ctx_ref[:, 1, :, hc].reshape(1024, 128)
        for half in range(2):
            q = q_ref[half * 128 : (half + 1) * 128, hc]
            s_ctx = lax.dot_general(q, kc, nt, preferred_element_type=F32) * inv
            s_win = [
                lax.dot_general(q, segs[half + s][0, :, hc], nt, preferred_element_type=F32) * inv
                + bias_ref[h, half, s]
                for s in range(3)
            ]
            top = jnp.max(s_ctx, axis=-1, keepdims=True)
            peak = jnp.maximum(jnp.maximum(s_win[0], s_win[1]), s_win[2])
            top = jnp.maximum(top, jnp.max(peak, axis=-1, keepdims=True))
            e_ctx = jnp.exp(s_ctx - top)
            e_win = [jnp.exp(s - top) for s in s_win]
            total = jnp.sum(e_ctx, axis=-1, keepdims=True) + jnp.sum(
                e_win[0] + e_win[1] + e_win[2], axis=-1, keepdims=True
            )
            acc = jnp.dot(e_ctx.astype(BF), vc, preferred_element_type=F32)
            for s in range(3):
                acc = acc + jnp.dot(
                    e_win[s].astype(BF), segs[half + s][1, :, hc], preferred_element_type=F32
                )
            out = (acc / total).astype(BF)
            for i in range(4):
                block = half * 4 + i
                slot = jnp.where(core == block % 2, 0, 1)
                out_ref[slot, (block // 2) * 32 : (block // 2) * 32 + 32, hc] = out[
                    i * 32 : (i + 1) * 32
                ]


def out_proj_body(mine_ref, got_ref, w_ref, wp_ref, out_ref):
    res = jnp.dot(mine_ref[...], w_ref[...], preferred_element_type=F32)
    res = res + jnp.dot(got_ref[...], wp_ref[...], preferred_element_type=F32)
    out_ref[...] = res.astype(BF).reshape(4, 32, D)


def final_body(parts_ref, lat_ref, gate_ref, out_ref):
    branch = jnp.sum(parts_ref[...].astype(F32), axis=0)
    out_ref[...] = (lat_ref[...].astype(F32) + gate_ref[...] * branch).astype(BF)


def exchange(blocks, axes):
    return lax.all_to_all(blocks, axes, 0, 0, tiled=True)


def on_device(
    latent,
    context,
    condition,
    ctx_cond,
    norm_gain,
    w_shift,
    w_scale,
    w_gate,
    w_query,
    w_key,
    w_value,
    w_out,
    rel_bias,
):
    gain = norm_gain.reshape(1, D)
    part = call(
        mod_partial_body,
        shape((16, 1, 1280), F32),
        "mod_partial",
        [pltpu.VMEM((128, 768), BF)],
    )(condition.reshape(16, 128), ctx_cond.reshape(16, 128), w_shift, w_scale, w_gate)
    lat_all = exchange(jnp.broadcast_to(latent[None], (8, 32, D)), TP)
    got = exchange(part, "z")
    summed = call(sum_bcast_body, shape((32, 1, 1280), F32), "sum_bcast")(got)
    mod = exchange(summed, ("y", "x", "c"))

    ctx_kv = call(
        ctx_kv_body,
        shape((16, 2, 16, 256), BF),
        "ctx_kv",
        [pltpu.VMEM((16, D), BF)],
        flops=10**8,
    )(context, mod, gain, w_key, w_value)
    ctx_z = exchange(ctx_kv, "z")
    ctx_all = exchange(jnp.broadcast_to(ctx_z[None], (4, 16, 2, 16, 256)), "y")

    q, head, tail, gate = call(
        qkv_body,
        (
            shape((256, 256), BF),
            shape((2, 128, 256), BF),
            shape((2, 128, 256), BF),
            shape((1, D), F32),
        ),
        "qkv",
        [pltpu.VMEM((256, D), BF)],
        flops=10**9,
    )(lat_all, mod, gain, w_query, w_key, w_value)
    count = 64
    prev = lax.ppermute(tail, SP, [(i, i + 1) for i in range(count - 1)])
    nxt = lax.ppermute(head, SP, [(i + 1, i) for i in range(count - 1)])
    table = jnp.pad(rel_bias, ((0, 0), (0, 1), (0, 97)))
    bias = call(
        functools.partial(bias_body, 512),
        shape((2, 2, 3, 128, 128), F32),
        "bias",
        [pltpu.VMEM((15, 4, 32, 128), F32)],
        flops=10**8,
    )(table)
    att = call(attend_body, shape((2, 128, 256), BF), "attend", flops=10**9)(
        q, prev, head, tail, nxt, bias, ctx_all.reshape(64, 2, 16, 256)
    )
    swap = [(0, 1), (1, 0)]
    w_pair = lax.ppermute(w_out, "c", swap)
    other = lax.ppermute(att[1], "c", swap)
    parts = call(out_proj_body, shape((4, 32, D), BF), "out_proj", flops=10**9)(
        att[0], other, w_out, w_pair
    )
    arrived = exchange(parts, "x")
    return call(final_body, shape((32, D), BF), "final")(arrived, latent, gate)


def solution(mesh):
    torus = Mesh(mesh.devices.reshape(16, 4, 4, 2), ALL)
    return jax.shard_map(
        on_device,
        mesh=torus,
        in_specs=(
            P(ALL, None),
            P(SP, None),
            P(),
            P(),
            P(),
            P(SP, TP),
            P(SP, TP),
            P(SP, TP),
            P(None, TP),
            P(None, TP),
            P(None, TP),
            P(TP, None),
            P(),
        ),
        out_specs=P(ALL, None),
        check_vma=False,
    )
```

time: 198 us -> 145 us (0.73)
  Pallas kernels: 0 us -> 21.9 us
  waiting for transfers between devices: 37.2 us -> 15.4 us
  local copies, waits for them, and re-layouts: 22.5 us -> 6.13 us
  matrix products: 16.3 us -> 0 us
  between operations: 13.7 us -> 0.1 us
  other arithmetic: 6.17 us -> 0 us
  blocking collectives: 79.7 us -> 75.9 us
    all_to_all x1 -> x4, blocking collectives: 30 us -> 75.9 us  [exchange(): return lax.all_to_all(blocks, axes, 0, 0, tiled=True)]
    psum x2 -> x0, blocking collectives: 39.6 us -> none  [one_axis_at_a_time(): array = lax.psum(array, axis)]
    all_gather x1 -> x0, waiting for transfers between devices: 31.5 us -> none  [gathered_by_axis(): whole = lax.all_gather(whole, axes[number], axis=dim, tiled=True)]
    pallas_call x0 -> x8, Pallas kernels: none -> 21.9 us  [the longest x1 4.46 us: on_device(): call(attend_body, shape((2, 128, 256), BF), 'attend', flops=10 ** 9)]
    dot_general x14 -> x0, matrix products: 14.8 us -> none  [the longest x1 3.15 us: on_device(): jnp.einsum('rqhd,rkwhd->rqhkw', queries, key_win, preferred_element_type=...]
    ppermute x2 -> x4, starting transfers between devices: 2.59 us -> 15.4 us  [the longest x1 7.54 us: on_device(): w_pair = lax.ppermute(w_out, 'c', swap)]
    all_to_all x2, starting transfers between devices: 18.8 us -> 7.43 us  [exchange(): return lax.all_to_all(blocks, axes, 0, 0, tiled=True)]
    all_gather x1 -> x0, blocking collectives: 10.1 us -> none  [gathered_by_axis(): whole = lax.all_gather(whole, axes[number], axis=dim, tiled=True)]
  transfers between devices with their start and end apart: 5 -> 6, of which waited for: 3 -> 3; matrix products, arithmetic and copies ran while one was open for 13% -> 2% of each run, Pallas kernels for 0% -> 10%
where the time goes in v1:
time: 145 us; the launch traced here: 142 us
  blocking collectives  75.9 us (52%)
  starting transfers between devices  22.9 us (16%)
  Pallas kernels  21.9 us (15%)
  waiting for transfers between devices  15.4 us (11%)
  local copies, waits for them, and re-layouts  6.13 us (4%)
    all_to_all x4, blocking collectives, exchange(): return lax.all_to_all(blocks, axes, 0, 0, tiled=True)  75.9 us
    all_to_all x2, waiting for transfers between devices, exchange(): return lax.all_to_all(blocks, axes, 0, 0, tiled=True)  12.1 us
    ppermute x1, starting transfers between devices, on_device(): w_pair = lax.ppermute(w_out, 'c', swap)  7.54 us
    all_to_all x2, starting transfers between devices, exchange(): return lax.all_to_all(blocks, axes, 0, 0, tiled=True)  7.43 us
    pallas_call x1, Pallas kernels, on_device(): call(attend_body, shape((2, 128, 256), BF), 'attend', flops=10 ** 9)  4.46 us
    pallas_call x1, Pallas kernels, on_device(): call(qkv_body, (shape((256, 256), BF), shape((2, 128, 256), BF), shape((2...  4.23 us
    ppermute x1, starting transfers between devices, on_device(): prev = lax.ppermute(tail, SP, [(i, i + 1) for i in range(count - 1)])  3.58 us
    ppermute x1, starting transfers between devices, on_device(): other = lax.ppermute(att[1], 'c', swap)  3.03 us
  transfers between devices with their start and end apart: 6, of which 3 were waited for; matrix products, arithmetic and copies ran while one was open for 2% of the time, Pallas kernels for 10%

profile of v1, /device:TPU:1, one launch (start us, length us, event | category | flops | bytes accessed | tf_op | source)
XLA Modules:
  0.0 142.4 jit_solution(14445740827726604165)
XLA Ops:
  0.0 1.6 %mod_partial.1 = f32[16,1,1280]{2,1,0:T(1,128)} custom-call(f32[16,128]{1,0:T(8,128)} %bitcast.11, f32[16,128]{1,0:T(8,128)} %bitcast.12, bf16[32,256]{1,0:T(8,128)(2,1)} %wsh_ref.1, bf16[32,256]{1,0:T(8,128)(2,1)} %wsc_ref.1, bf16[32,256]{1,0:T(8,128)(2,1)} %wg_ref.1), custom_call_target="tpu_custom_call" | custom-call | tf_op jit(solution)/shard_map/mod_partial/pallas_call | solution.py:213
  1.6 27.6 %all_to_all.30.in_ref = f32[16,1,1280]{2,1,0:T(1,128)} all-to-all(f32[16,1,1280]{2,1,0:T(1,128)} %mod_partial.1), channel_id=1, replica_groups=mesh['z'=16,'y'=4,'x'=4,'c'=2] {'z'}, dimensions={0} | all-to-all | bytes 163840 | tf_op jit(solution)/shard_map/all_to_all | solution.py:194
  29.2 1.6 %sum_bcast.1 = f32[32,1,1280]{2,1,0:T(1,128)} custom-call(f32[16,1,1280]{2,1,0:T(1,128)} %all_to_all.30.in_ref), custom_call_target="tpu_custom_call" | custom-call | tf_op jit(solution)/shard_map/sum_bcast/pallas_call | solution.py:221
  30.8 17.6 %all_to_all.31.mod_ref = f32[32,1,1280]{2,1,0:T(1,128)} all-to-all(f32[32,1,1280]{2,1,0:T(1,128)} %sum_bcast.1), channel_id=1, replica_groups=mesh['z'=16,'y'=4,'x'=4,'c'=2] {'y','x','c'}, dimensions={0} | all-to-all | bytes 327680 | tf_op jit(solution)/shard_map/all_to_all | solution.py:194
  48.5 1.1 broadcast_in_dim.4
  49.6 3.8 %all-to-all-start = ((bf16[8,32,2048]{2,1,0:T(8,128)(2,1)}), bf16[8,32,2048]{2,1,0:T(8,128)(2,1)S(1)}, u32[]{:S(2)}, u32[]{:S(2)}) async-start(bf16[8,32,2048]{2,1,0:T(8,128)(2,1)} %broadcast_in_dim.4), calls=%async_computation | async-start | bytes 2097152 | tf_op jit(solution)/shard_map/all_to_all | solution.py:194
  53.4 2.9 %ctx_kv.1 = bf16[16,2,16,256]{3,2,1,0:T(8,128)(2,1)} custom-call(bf16[16,2048]{1,0:T(8,128)(2,1)} %ctx_ref.1, f32[32,1,1280]{2,1,0:T(1,128)} %all_to_all.31.mod_ref, f32[1,2048]{1,0:T(1,128)} %bitcast.9, bf16[2048,256]{1,0:T(8,128)(2,1)} %wk_ref.3, bf16[2048,256]{1,0:T(8,128)(2,1)} %wv_ref.3), custom_call_target="tpu_custom_call" | custom-call | flops 100000000 | tf_op jit(solution)/shard_map/ctx_kv/pallas_call | solution.py:224
  56.2 12.1 %all-to-all-done.lat_ref = bf16[8,32,2048]{2,1,0:T(8,128)(2,1)S(1)} async-done(((bf16[8,32,2048]{2,1,0:T(8,128)(2,1)}), bf16[8,32,2048]{2,1,0:T(8,128)(2,1)S(1)}, u32[]{:S(2)}, u32[]{:S(2)}) %all-to-all-start) | async-done | bytes 1048608 | tf_op jit(solution)/shard_map/all_to_all | solution.py:194
  68.4 17.3 %all_to_all.32 = bf16[16,2,16,256]{3,2,1,0:T(8,128)(2,1)S(1)} all-to-all(bf16[16,2,16,256]{3,2,1,0:T(8,128)(2,1)} %ctx_kv.1), channel_id=1, replica_groups=mesh['z'=16,'y'=4,'x'=4,'c'=2] {'z'}, dimensions={0} | all-to-all | bytes 524288 | tf_op jit(solution)/shard_map/all_to_all | solution.py:194
  85.6 1.1 broadcast_in_dim.5
  86.8 3.6 %all-to-all-start.4 = ((bf16[4,16,2,16,256]{4,3,2,1,0:T(8,128)(2,1)}), bf16[4,16,2,16,256]{4,3,2,1,0:T(8,128)(2,1)S(1)}, u32[]{:S(2)}, u32[]{:S(2)}) async-start(bf16[4,16,2,16,256]{4,3,2,1,0:T(8,128)(2,1)} %broadcast_in_dim.5), calls=%async_computation.4 | async-start | bytes 2097152 | tf_op jit(solution)/shard_map/all_to_all | solution.py:194
  90.4 7.5 %collective-permute-start.3 = (bf16[256,2048]{1,0:T(8,128)(2,1)S(1)}, bf16[256,2048]{1,0:T(8,128)(2,1)}, u32[]{:S(2)}, u32[]{:S(2)}) collective-permute-start(bf16[256,2048]{1,0:T(8,128)(2,1)S(1)} %copy-done.4), channel_id=1, source_target_pairs={{0,1},{1,0},{2,3},{3,2},{4,5},{5,4},{6,7},{7,6},{8,9},{9,8},{10,11... | collective-permute-start | bytes 3145736 | tf_op jit(solution)/shard_map/ppermute | solution.py:261
  98.0 4.2 %qkv.1 = (bf16[256,256]{1,0:T(8,128)(2,1)}, bf16[2,128,256]{2,1,0:T(8,128)(2,1)}, bf16[2,128,256]{2,1,0:T(8,128)(2,1)}, f32[1,2048]{1,0:T(1,128)}) custom-call(bf16[8,32,2048]{2,1,0:T(8,128)(2,1)} %copy-done, f32[32,1,1280]{2,1,0:T(1,128)} %all_to_all.31.mod_ref, f32[1,2048]{1,0:T(1,128)} %bitcast.10, bf16[2048,256]{1,0:T(8,128)(2,1)} %wq_ref.1, ...), custom_call_target="tpu_custom_call" | custom-call | flops 1000000000 | tf_op jit(solution)/shard_map/qkv/pallas_call | solution.py:234
  102.2 3.6 %collective-permute-start = (bf16[2,128,256]{2,1,0:T(8,128)(2,1)}, bf16[2,128,256]{2,1,0:T(8,128)(2,1)S(1)}, u32[]{:S(2)}, u32[]{:S(2)}) collective-permute-start(bf16[2,128,256]{2,1,0:T(8,128)(2,1)} %get-tuple-element.10.tail_ref), channel_id=1, source_target_pairs={{0,8},{8,16},{16,24},{24,32},{32,40},{40,48},{48,56},{56,64},{64,7... | collective-permute-start | bytes 393224 | tf_op jit(solution)/shard_map/ppermute | solution.py:247
  105.8 1.3 collective-permute-start.1
  107.8 2.4 %bias.1.bias_ref = f32[2,2,3,128,128]{4,3,2,1,0:T(8,128)} custom-call(f32[16,16,128]{2,1,0:T(8,128)} %pad.4.tab_ref), custom_call_target="tpu_custom_call" | custom-call | flops 100000000 | tf_op jit(solution)/shard_map/bias/pallas_call | solution.py:250
  110.2 2.5 %collective-permute-done.1.next_ref = bf16[2,128,256]{2,1,0:T(8,128)(2,1)S(1)} collective-permute-done((bf16[2,128,256]{2,1,0:T(8,128)(2,1)}, bf16[2,128,256]{2,1,0:T(8,128)(2,1)S(1)}, u32[]{:S(2)}, u32[]{:S(2)}) %collective-permute-start.1) | collective-permute-done | bytes 131104 | tf_op jit(solution)/shard_map/ppermute | solution.py:248
  113.7 4.5 %attend.1 = bf16[2,128,256]{2,1,0:T(8,128)(2,1)} custom-call(bf16[256,256]{1,0:T(8,128)(2,1)} %get-tuple-element.9.q_ref, bf16[2,128,256]{2,1,0:T(8,128)(2,1)} %copy-done.5, bf16[2,128,256]{2,1,0:T(8,128)(2,1)} %get-tuple-element.11.head_ref, bf16[2,128,256]{2,1,0:T(8,128)(2,1)} %get-tuple-element.10.tail_ref, bf16[2,128,256]{2,1,0:T(8,128)(2,1)} %copy-done.6, ...), custom_call_target="tpu_custom_call" | custom-call | flops 1000000000 | tf_op jit(solution)/shard_map/attend/pallas_call | solution.py:257
  118.2 1.5 %slice_bitcast_fusion = (bf16[128,256]{1,0:T(8,128)(2,1)S(1)}, bf16[128,256]{1,0:T(8,128)(2,1)}) fusion(bf16[2,128,256]{2,1,0:T(8,128)(2,1)} %attend.1), kind=kLoop, calls=%fused_computation | loop fusion | bytes 262144 | tf_op jit(solution)/shard_map/squeeze | solution.py:262
  119.7 3.0 %collective-permute-start.2 = (bf16[128,256]{1,0:T(8,128)(2,1)S(1)}, bf16[128,256]{1,0:T(8,128)(2,1)S(1)}, u32[]{:S(2)}, u32[]{:S(2)}) collective-permute-start(bf16[128,256]{1,0:T(8,128)(2,1)S(1)} %get-tuple-element.13), channel_id=1, source_target_pairs={{0,1},{1,0},{2,3},{3,2},{4,5},{5,4},{6,7},{7,6},{8,9},{9,8},{10,11... | collective-permute-start | bytes 196616 | tf_op jit(solution)/shard_map/ppermute | solution.py:262
  122.8 0.9 collective-permute-done.2.got_ref
  124.3 2.9 %out_proj.1 = bf16[4,32,2048]{2,1,0:T(8,128)(2,1)} custom-call(bf16[128,256]{1,0:T(8,128)(2,1)} %get-tuple-element.14.mine_ref, bf16[128,256]{1,0:T(8,128)(2,1)} %copy-done.7, bf16[256,2048]{1,0:T(8,128)(2,1)} %w_ref.1, bf16[256,2048]{1,0:T(8,128)(2,1)} %collective-permute-done.3.wp_ref), custom_call_target="tpu_custom_call" | custom-call | flops 1000000000 | tf_op jit(solution)/shard_map/out_proj/pallas_call | solution.py:263
  127.1 13.4 %all_to_all.33.parts_ref = bf16[4,32,2048]{2,1,0:T(8,128)(2,1)} all-to-all(bf16[4,32,2048]{2,1,0:T(8,128)(2,1)} %out_proj.1), channel_id=1, replica_groups=mesh['z'=16,'y'=4,'x'=4,'c'=2] {'x'}, dimensions={0} | all-to-all | bytes 1048576 | tf_op jit(solution)/shard_map/all_to_all | solution.py:194
  140.6 1.9 %final.1 = bf16[32,2048]{1,0:T(8,128)(2,1)} custom-call(bf16[4,32,2048]{2,1,0:T(8,128)(2,1)} %all_to_all.33.parts_ref, bf16[32,2048]{1,0:T(8,128)(2,1)} %lat_ref.1, f32[1,2048]{1,0:T(1,128)} %get-tuple-element.12.gate_ref), custom_call_target="tpu_custom_call" | custom-call | tf_op jit(solution)/shard_map/final/pallas_call | solution.py:267
  (21 shorter events, 2.4 us)
Async XLA Ops:
  30.8 17.6 %copy-start.2 = (bf16[32,2048]{1,0:T(8,128)(2,1)S(1)}, bf16[32,2048]{1,0:T(8,128)(2,1)}, u32[]{:S(2)}) copy-start(bf16[32,2048]{1,0:T(8,128)(2,1)} %lat_ref.1) | copy-start | bytes 393220
  49.6 18.8 %all-to-all-start = ((bf16[8,32,2048]{2,1,0:T(8,128)(2,1)}), bf16[8,32,2048]{2,1,0:T(8,128)(2,1)S(1)}, u32[]{:S(2)}, u32[]{:S(2)}) async-start(bf16[8,32,2048]{2,1,0:T(8,128)(2,1)} %broadcast_in_dim.4), calls=%async_computation | async-start | bytes 2097152 | tf_op jit(solution)/shard_map/all_to_all | solution.py:194
  68.4 18.4 %copy-start = (bf16[8,32,2048]{2,1,0:T(8,128)(2,1)}, bf16[8,32,2048]{2,1,0:T(8,128)(2,1)S(1)}, u32[]{:S(2)}) copy-start(bf16[8,32,2048]{2,1,0:T(8,128)(2,1)S(1)} %all-to-all-done.lat_ref) | copy-start | bytes 3145732
  86.8 3.7 %copy-start.4 = (bf16[256,2048]{1,0:T(8,128)(2,1)S(1)}, bf16[256,2048]{1,0:T(8,128)(2,1)}, u32[]{:S(2)}) copy-start(bf16[256,2048]{1,0:T(8,128)(2,1)} %w_ref.1) | copy-start | bytes 3145732
  86.8 25.9 %all-to-all-start.4 = ((bf16[4,16,2,16,256]{4,3,2,1,0:T(8,128)(2,1)}), bf16[4,16,2,16,256]{4,3,2,1,0:T(8,128)(2,1)S(1)}, u32[]{:S(2)}, u32[]{:S(2)}) async-start(bf16[4,16,2,16,256]{4,3,2,1,0:T(8,128)(2,1)} %broadcast_in_dim.5), calls=%async_computation.4 | async-start | bytes 2097152 | tf_op jit(solution)/shard_map/all_to_all | solution.py:194
  90.4 16.7 %copy-start.3 = (f32[16,15,31]{2,0,1:T(8,128)S(1)}, f32[16,15,31]{2,0,1:T(8,128)}, u32[]{:S(2)}) copy-start(f32[16,15,31]{2,0,1:T(8,128)} %param.25) | copy-start | bytes 89284
  90.4 32.3 %collective-permute-start.3 = (bf16[256,2048]{1,0:T(8,128)(2,1)S(1)}, bf16[256,2048]{1,0:T(8,128)(2,1)}, u32[]{:S(2)}, u32[]{:S(2)}) collective-permute-start(bf16[256,2048]{1,0:T(8,128)(2,1)S(1)} %copy-done.4), channel_id=1, source_target_pairs={{0,1},{1,0},{2,3},{3,2},{4,5},{5,4},{6,7},{7,6},{8,9},{9,8},{10,11... | collective-permute-start | bytes 3145736 | tf_op jit(solution)/shard_map/ppermute | solution.py:261
  102.2 8.0 %collective-permute-start = (bf16[2,128,256]{2,1,0:T(8,128)(2,1)}, bf16[2,128,256]{2,1,0:T(8,128)(2,1)S(1)}, u32[]{:S(2)}, u32[]{:S(2)}) collective-permute-start(bf16[2,128,256]{2,1,0:T(8,128)(2,1)} %get-tuple-element.10.tail_ref), channel_id=1, source_target_pairs={{0,8},{8,16},{16,24},{24,32},{32,40},{40,48},{48,56},{56,64},{64,7... | collective-permute-start | bytes 393224 | tf_op jit(solution)/shard_map/ppermute | solution.py:247
  105.8 6.9 %collective-permute-start.1 = (bf16[2,128,256]{2,1,0:T(8,128)(2,1)}, bf16[2,128,256]{2,1,0:T(8,128)(2,1)S(1)}, u32[]{:S(2)}, u32[]{:S(2)}) collective-permute-start(bf16[2,128,256]{2,1,0:T(8,128)(2,1)} %get-tuple-element.11.head_ref), channel_id=1, source_target_pairs={{8,0},{16,8},{24,16},{32,24},{40,32},{48,40},{56,48},{64,56},{72,6... | collective-permute-start | bytes 393224 | tf_op jit(solution)/shard_map/ppermute | solution.py:248
  110.2 2.5 %copy-start.5 = (bf16[2,128,256]{2,1,0:T(8,128)(2,1)}, bf16[2,128,256]{2,1,0:T(8,128)(2,1)S(1)}, u32[]{:S(2)}) copy-start(bf16[2,128,256]{2,1,0:T(8,128)(2,1)S(1)} %collective-permute-done.prev_ref) | copy-start | bytes 393220
  112.7 0.7 copy-start.6
  112.7 1.1 copy-start.1
  119.7 3.9 %collective-permute-start.2 = (bf16[128,256]{1,0:T(8,128)(2,1)S(1)}, bf16[128,256]{1,0:T(8,128)(2,1)S(1)}, u32[]{:S(2)}, u32[]{:S(2)}) collective-permute-start(bf16[128,256]{1,0:T(8,128)(2,1)S(1)} %get-tuple-element.13), channel_id=1, source_target_pairs={{0,1},{1,0},{2,3},{3,2},{4,5},{5,4},{6,7},{7,6},{8,9},{9,8},{10,11... | collective-permute-start | bytes 196616 | tf_op jit(solution)/shard_map/ppermute | solution.py:262
  123.6 0.6 copy-start.7

commit v2 on v1

--- a/solution.py
+++ b/solution.py
@@ -8,7 +8,7 @@
 from jax.sharding import Mesh
 from jax.sharding import PartitionSpec as P
 
-HEADS = 16
+
 HEAD_DIM = 128
 GRID_W = 32
 WIN_H = 8
@@ -23,12 +23,16 @@
 F32 = jnp.float32
 
 
-def call(body, outs, name, scratch=(), flops=0, vmem=None):
+VMEM_SPEC = pl.BlockSpec(memory_space=pltpu.VMEM)
+HBM_SPEC = pl.BlockSpec(memory_space=pltpu.HBM)
+
+
+def call(body, outs, scratch=(), flops=0, vmem=8 << 20, **specs):
     return pl.pallas_call(
         body,
         out_shape=outs,
+        **specs,
         scratch_shapes=list(scratch),
-        name=name,
         cost_estimate=pl.CostEstimate(flops=flops, bytes_accessed=0, transcendentals=0),
         compiler_params=pltpu.CompilerParams(vmem_limit_bytes=vmem),
     )
@@ -38,51 +42,90 @@
     return jax.ShapeDtypeStruct(dims, dtype)
 
 
-def mod_partial_body(cond_ref, ctxc_ref, wsh_ref, wsc_ref, wg_ref, out_ref, pad_ref):
+def mod_partial_body(
+    cond_hbm, ctxc_hbm, wsh_hbm, wsc_hbm, wg_hbm, ctx_hbm, out_ref, pad_ref, act_ref, ctx_ref, sems
+):
     sp = lax.axis_index("z") * 4 + lax.axis_index("y")
+    tp = lax.axis_index("x") * 2 + lax.axis_index("c")
     row = sp // 4
     off = pl.multiple_of((sp % 4) * 32, 32)
-    cond = cond_ref[pl.ds(row, 1), :]
-    ctxc = ctxc_ref[pl.ds(row, 1), :]
+    zero = jnp.zeros((32, 768), BF)
+    for i in range(4):
+        pad_ref[i * 32 : (i + 1) * 32] = zero
+    cols = pl.ds(pl.multiple_of(tp * 256, 256), 256)
+    copies = [
+        pltpu.make_async_copy(src, dst, sems.at[i])
+        for i, (src, dst) in enumerate(
+            (
+                (cond_hbm, act_ref.at[0]),
+                (ctxc_hbm, act_ref.at[1]),
+                (wsh_hbm, pad_ref.at[pl.ds(off, 32), 0:256]),
+                (wsc_hbm, pad_ref.at[pl.ds(off, 32), 256:512]),
+                (wg_hbm, pad_ref.at[pl.ds(off, 32), 512:768]),
+                (ctx_hbm.at[:, cols], ctx_ref),
+            )
+        )
+    ]
+    for copy in copies:
+        copy.start()
+    for copy in copies:
+        copy.wait()
+    cond = act_ref[0, pl.ds(row, 1), :]
+    ctxc = act_ref[1, pl.ds(row, 1), :]
     act = jnp.concatenate([cond, ctxc] * 4, axis=0)
     act = (act / (1.0 + jnp.exp(-act))).astype(BF)
-    pad_ref[...] = jnp.zeros_like(pad_ref)
-    pad_ref[pl.ds(off, 32), 0:256] = wsh_ref[...]
-    pad_ref[pl.ds(off, 32), 256:512] = wsc_ref[...]
-    pad_ref[pl.ds(off, 32), 512:768] = wg_ref[...]
     res = jnp.dot(act, pad_ref[...], preferred_element_type=F32)
-    row5 = jnp.concatenate(
-        [res[0:1, 0:256], res[1:2, 0:256], res[0:1, 256:512], res[1:2, 256:512], res[0:1, 512:768]],
-        axis=1,
+    rows = jnp.concatenate(
+        [
+            res[0:2, 0:256],
+            res[0:2, 256:512],
+            res[0:1, 512:768],
+            jnp.zeros((3, 256), F32),
+        ],
+        axis=0,
     )
+    high = rows.astype(BF)
+    low = (rows - high.astype(F32)).astype(BF)
+    packed = jnp.concatenate([high.astype(F32), low.astype(F32)], axis=0).astype(BF)
+    ctx = ctx_ref[...]
     for i in range(out_ref.shape[0]):
-        out_ref[i] = row5
-
-
-def sum_bcast_body(in_ref, out_ref):
-    total = jnp.sum(in_ref[...], axis=0)
-    for i in range(out_ref.shape[0]):
-        out_ref[i] = total
+        out_ref[i, 0:16] = ctx
+        out_ref[i, 16:32] = packed
+
+
+def relay_body(in_ref, mod_ref, ctx_ref):
+    total = jnp.sum(in_ref[:, 16:32, :].astype(F32), axis=0)
+    total = total[0:8] + total[8:16]
+    for i in range(mod_ref.shape[0]):
+        mod_ref[i] = total
+    ctx_ref[...] = in_ref[:, 0:16, :].reshape(256, 256)
 
 
 def mod_row(mod_ref, xc, kind):
-    total = mod_ref[xc, :, kind * 256 : (kind + 1) * 256]
+    total = mod_ref[xc, kind : kind + 1, :]
     for y in range(1, 4):
-        total = total + mod_ref[y * 8 + xc, :, kind * 256 : (kind + 1) * 256]
+        total = total + mod_ref[y * 8 + xc, kind : kind + 1, :]
     return total
 
 
-def normalize(load, mod_ref, gain_ref, xn_ref, rows, which):
-    x = load().astype(F32)
-    inv = lax.rsqrt(jnp.mean(x * x, axis=-1, keepdims=True) + NORM_EPS)
-    for xc in range(8):
-        cols = slice(xc * 256, (xc + 1) * 256)
-        gain = gain_ref[:, cols] * (1.0 + mod_row(mod_ref, xc, 2 + which))
-        xn_ref[:, cols] = (x[:, cols] * inv * gain + mod_row(mod_ref, xc, which)).astype(BF)
-
-
-def ctx_kv_body(ctx_ref, mod_ref, gain_ref, wk_ref, wv_ref, out_ref, xn_ref):
-    normalize(lambda: ctx_ref[...], mod_ref, gain_ref, xn_ref, 16, 1)
+def gather_x_body(own_ref, p1_ref, p2_ref, p3_ref, out_ref):
+    x = lax.axis_index("x")
+    for d, ref in enumerate((own_ref, p1_ref, p2_ref, p3_ref)):
+        out_ref[lax.rem(x - d + 4, 4)] = ref[...]
+
+
+def ctx_kv_body(mine_ref, theirs_ref, mod_ref, gain_ref, wk_ref, wv_ref, out_ref, xn_ref):
+    core = lax.axis_index("c")
+    blocks = [(ref, j, 2 * j + c) for j in range(4) for ref, c in ((mine_ref, core), (theirs_ref, 1 - core))]
+    square = jnp.zeros((256, 256), F32)
+    for ref, j, _ in blocks:
+        x = ref[j].astype(F32)
+        square = square + x * x
+    inv = lax.rsqrt(jnp.sum(square, axis=-1, keepdims=True) * (1.0 / D) + NORM_EPS)
+    for ref, j, xc in blocks:
+        cols = pl.ds(pl.multiple_of(xc * 256, 256), 256)
+        gain = gain_ref[:, cols] * (1.0 + mod_row(mod_ref, xc, 3))
+        xn_ref[:, cols] = (ref[j].astype(F32) * inv * gain + mod_row(mod_ref, xc, 1)).astype(BF)
     xn = xn_ref[...]
     k = jnp.dot(xn, wk_ref[...], preferred_element_type=F32).astype(BF)
     v = jnp.dot(xn, wv_ref[...], preferred_element_type=F32).astype(BF)
@@ -92,9 +135,20 @@
 
 
 def qkv_body(
-    lat_ref, mod_ref, gain_ref, wq_ref, wk_ref, wv_ref, q_ref, head_ref, tail_ref, gate_ref, xn_ref
+    mine_ref, theirs_ref, mod_ref, gain_ref, wq_ref, wk_ref, wv_ref,
+    q_ref, head_ref, tail_ref, gate_ref, xn_ref,
 ):
-    normalize(lambda: lat_ref[...].reshape(256, D), mod_ref, gain_ref, xn_ref, 256, 0)
+    core = lax.axis_index("c")
+    gains = [gain_ref[:, i * 256 : (i + 1) * 256] * (1.0 + mod_row(mod_ref, i, 2)) for i in range(8)]
+    shifts = [mod_row(mod_ref, i, 0) for i in range(8)]
+    gain = jnp.concatenate(gains, axis=1)
+    shift = jnp.concatenate(shifts, axis=1)
+    for ref, c in ((mine_ref, core), (theirs_ref, 1 - core)):
+        for j in range(4):
+            x = ref[j].astype(F32)
+            inv = lax.rsqrt(jnp.sum(x * x, axis=-1, keepdims=True) * (1.0 / D) + NORM_EPS)
+            rows = pl.ds(pl.multiple_of((2 * j + c) * 32, 32), 32)
+            xn_ref[rows, :] = (x * inv * gain + shift).astype(BF)
     xn = xn_ref[...]
     k = jnp.dot(xn, wk_ref[...], preferred_element_type=F32).astype(BF)
     head_ref[0] = k[:128]
@@ -140,7 +194,7 @@
                 out_ref[h, half, s, (r % 4) * 32 : (r % 4) * 32 + 32, :] = block
 
 
-def attend_body(q_ref, prev_ref, head_ref, tail_ref, next_ref, bias_ref, ctx_ref, out_ref):
+def attend_body(q_ref, prev_ref, head_ref, tail_ref, next_ref, bias_ref, ctx_ref, mine_ref, other_ref):
     core = lax.axis_index("c")
     inv = HEAD_DIM**-0.5
     segs = (prev_ref, head_ref, tail_ref, next_ref)
@@ -171,12 +225,12 @@
                     e_win[s].astype(BF), segs[half + s][1, :, hc], preferred_element_type=F32
                 )
             out = (acc / total).astype(BF)
-            for i in range(4):
-                block = half * 4 + i
-                slot = jnp.where(core == block % 2, 0, 1)
-                out_ref[slot, (block // 2) * 32 : (block // 2) * 32 + 32, hc] = out[
-                    i * 32 : (i + 1) * 32
-                ]
+            for i in range(2):
+                even = out[i * 64 : i * 64 + 32]
+                odd = out[i * 64 + 32 : i * 64 + 64]
+                rows = slice((half * 2 + i) * 32, (half * 2 + i + 1) * 32)
+                mine_ref[rows, hc] = jnp.where(core == 0, even, odd)
+                other_ref[rows, hc] = jnp.where(core == 0, odd, even)
 
 
 def out_proj_body(mine_ref, got_ref, w_ref, wp_ref, out_ref):
@@ -192,6 +246,16 @@
 
 def exchange(blocks, axes):
     return lax.all_to_all(blocks, axes, 0, 0, tiled=True)
+
+
+SWAP = [(0, 1), (1, 0)]
+
+
+def along_x(own):
+    parts = [own]
+    for d in (1, 2, 3):
+        parts.append(lax.ppermute(own, "x", [(i, (i + d) % 4) for i in range(4)]))
+    return parts
 
 
 def on_device(
@@ -212,24 +276,33 @@
     gain = norm_gain.reshape(1, D)
     part = call(
         mod_partial_body,
-        shape((16, 1, 1280), F32),
-        "mod_partial",
-        [pltpu.VMEM((128, 768), BF)],
-    )(condition.reshape(16, 128), ctx_cond.reshape(16, 128), w_shift, w_scale, w_gate)
-    lat_all = exchange(jnp.broadcast_to(latent[None], (8, 32, D)), TP)
+        shape((16, 32, 256), BF),
+        [
+            pltpu.VMEM((128, 768), BF),
+            pltpu.VMEM((2, 16, 128), F32),
+            pltpu.VMEM((16, 256), BF),
+            pltpu.SemaphoreType.DMA((6,)),
+        ],
+        flops=10**7,
+        in_specs=[HBM_SPEC] * 6,
+        out_specs=VMEM_SPEC,
+    )(condition.reshape(16, 128), ctx_cond.reshape(16, 128), w_shift, w_scale, w_gate, context)
     got = exchange(part, "z")
-    summed = call(sum_bcast_body, shape((32, 1, 1280), F32), "sum_bcast")(got)
+    lat_parts = along_x(latent)
+    w_pair = lax.ppermute(w_out, "c", SWAP)
+    summed, ctx_own = call(
+        relay_body, (shape((32, 8, 256), F32), shape((256, 256), BF)), flops=10**7
+    )(got)
     mod = exchange(summed, ("y", "x", "c"))
-
+    ctx_parts = along_x(ctx_own)
+    lat_mine = call(gather_x_body, shape((4, 32, D), BF), flops=10**8)(*lat_parts)
+    lat_theirs = lax.ppermute(lat_mine, "c", SWAP)
+    ctx_mine = call(gather_x_body, shape((4, 256, 256), BF), flops=10**8)(*ctx_parts)
+    ctx_theirs = lax.ppermute(ctx_mine, "c", SWAP)
     ctx_kv = call(
-        ctx_kv_body,
-        shape((16, 2, 16, 256), BF),
-        "ctx_kv",
-        [pltpu.VMEM((16, D), BF)],
-        flops=10**8,
-    )(context, mod, gain, w_key, w_value)
-    ctx_z = exchange(ctx_kv, "z")
-    ctx_all = exchange(jnp.broadcast_to(ctx_z[None], (4, 16, 2, 16, 256)), "y")
+        ctx_kv_body, shape((4, 2, 256, 256), BF), [pltpu.VMEM((256, D), BF)], flops=10**9
+    )(ctx_mine, ctx_theirs, mod, gain, w_key, w_value)
+    ctx_all = exchange(ctx_kv, "y")
 
     q, head, tail, gate = call(
         qkv_body,
@@ -239,10 +312,9 @@
             shape((2, 128, 256), BF),
             shape((1, D), F32),
         ),
-        "qkv",
         [pltpu.VMEM((256, D), BF)],
         flops=10**9,
-    )(lat_all, mod, gain, w_query, w_key, w_value)
+    )(lat_mine, lat_theirs, mod, gain, w_query, w_key, w_value)
     count = 64
     prev = lax.ppermute(tail, SP, [(i, i + 1) for i in range(count - 1)])
     nxt = lax.ppermute(head, SP, [(i + 1, i) for i in range(count - 1)])
@@ -250,21 +322,16 @@
     bias = call(
         functools.partial(bias_body, 512),
         shape((2, 2, 3, 128, 128), F32),
-        "bias",
         [pltpu.VMEM((15, 4, 32, 128), F32)],
         flops=10**8,
     )(table)
-    att = call(attend_body, shape((2, 128, 256), BF), "attend", flops=10**9)(
-        q, prev, head, tail, nxt, bias, ctx_all.reshape(64, 2, 16, 256)
-    )
-    swap = [(0, 1), (1, 0)]
-    w_pair = lax.ppermute(w_out, "c", swap)
-    other = lax.ppermute(att[1], "c", swap)
-    parts = call(out_proj_body, shape((4, 32, D), BF), "out_proj", flops=10**9)(
-        att[0], other, w_out, w_pair
-    )
+    att, away = call(
+        attend_body, (shape((128, 256), BF), shape((128, 256), BF)), flops=10**9
+    )(q, prev, head, tail, nxt, bias, ctx_all)
+    other = lax.ppermute(away, "c", SWAP)
+    parts = call(out_proj_body, shape((4, 32, D), BF), flops=10**9)(att, other, w_out, w_pair)
     arrived = exchange(parts, "x")
-    return call(final_body, shape((32, D), BF), "final")(arrived, latent, gate)
+    return call(final_body, shape((32, D), BF))(arrived, latent, gate)
 
 
 def solution(mesh):

time: 145 us -> 126 us (0.87)
  blocking collectives: 75.9 us -> 41.1 us
  starting transfers between devices: 22.9 us -> 55 us
  Pallas kernels: 21.9 us -> 10.3 us
  waiting for transfers between devices: 15.4 us -> 9.41 us
  local copies, waits for them, and re-layouts: 6.13 us -> 7.63 us
    all_to_all x4 -> x2, blocking collectives: 75.9 us -> 41.1 us  [exchange(): return lax.all_to_all(blocks, axes, 0, 0, tiled=True)]
    ppermute x2 -> x10, starting transfers between devices: 10.6 us -> 39.2 us  [the longest x6 21.2 us: along_x(): parts.append(lax.ppermute(own, 'x', [(i, (i + d) % 4) for i in range(4)]))]
    all_to_all x2, waiting for transfers between devices: 12.1 us -> 0.01 us  [exchange(): return lax.all_to_all(blocks, axes, 0, 0, tiled=True)]
    pallas_call x6 -> x8, Pallas kernels: 15.3 us -> 8.14 us  [the longest x1 2.11 us: on_device(): call(ctx_kv_body, shape((4, 2, 256, 256), BF), [pltpu.VMEM((256, D), BF)]...]
    unnamed x17 -> x41, local copies, waits for them, and re-layouts: 1.72 us -> 7.62 us
    ppermute x2 -> x10, waiting for transfers between devices: 0.87 us -> 5.14 us  [the longest x6 2.67 us: along_x(): parts.append(lax.ppermute(own, 'x', [(i, (i + d) % 4) for i in range(4)]))]
    all_to_all x2, starting transfers between devices: 7.43 us -> 10.9 us  [exchange(): return lax.all_to_all(blocks, axes, 0, 0, tiled=True)]
    pallas_call x1, Pallas kernels: 4.23 us -> 1.53 us  [on_device(): call(qkv_body, (shape((256, 256), BF), shape((2, 128, 256), BF), shape((2...]
  transfers between devices with their start and end apart: 6 -> 14, of which waited for: 3 -> 5; matrix products, arithmetic and copies ran while one was open for 2% -> 0% of each run, Pallas kernels for 10% -> 6%
where the time goes in v2:
time: 126 us; the launch traced here: 124 us
  starting transfers between devices  55 us (44%)
  blocking collectives  41.1 us (33%)
  Pallas kernels  10.3 us (8%)
  waiting for transfers between devices  9.41 us (7%)
  local copies, waits for them, and re-layouts  7.63 us (6%)
    all_to_all x2, blocking collectives, exchange(): return lax.all_to_all(blocks, axes, 0, 0, tiled=True)  41.1 us
    ppermute x6, starting transfers between devices, along_x(): parts.append(lax.ppermute(own, 'x', [(i, (i + d) % 4) for i in range(4)]))  21.2 us
    all_to_all x2, starting transfers between devices, exchange(): return lax.all_to_all(blocks, axes, 0, 0, tiled=True)  10.9 us
    ppermute x1, starting transfers between devices, on_device(): ctx_theirs = lax.ppermute(ctx_mine, 'c', SWAP)  9.15 us
    unnamed x41, local copies, waits for them, and re-layouts  7.62 us
    ppermute x1, starting transfers between devices, on_device(): prev = lax.ppermute(tail, SP, [(i, i + 1) for i in range(count - 1)])  3.56 us
    ppermute x1, starting transfers between devices, on_device(): other = lax.ppermute(away, 'c', SWAP)  3.42 us
    ppermute x1, starting transfers between devices, on_device(): w_pair = lax.ppermute(w_out, 'c', SWAP)  3.15 us
  transfers between devices with their start and end apart: 14, of which 5 were waited for; matrix products, arithmetic and copies ran while one was open for 0% of the time, Pallas kernels for 6%

profile of v2, /device:TPU:1, one launch (start us, length us, event | category | flops | bytes accessed | tf_op | source)
XLA Modules:
  0.0 123.7 jit_solution(15578749385430760899)
XLA Ops:
  4.7 29.4 %all_to_all.20.in_ref = bf16[16,32,256]{2,1,0:T(8,128)(2,1)S(1)} all-to-all(bf16[16,32,256]{2,1,0:T(8,128)(2,1)S(1)} %shard_map.128), channel_id=1, replica_groups=mesh['z'=16,'y'=4,'x'=4,'c'=2] {'z'}, dimensions={0} | all-to-all | bytes 524288 | tf_op jit(solution)/shard_map/all_to_all | solution.py:248
  34.9 3.1 %collective-permute-start.6 = (bf16[256,256]{1,0:T(8,128)(2,1)S(1)}, bf16[256,256]{1,0:T(8,128)(2,1)S(1)}, u32[]{:S(2)}, u32[]{:S(2)}) collective-permute-start(bf16[256,256]{1,0:T(8,128)(2,1)S(1)} %get-tuple-element.17.own_ref), channel_id=1, source_target_pairs={{0,2},{2,4},{4,6},{6,0},{1,3},{3,5},{5,7},{7,1},{8,10},{10,12},{12... | collective-permute-start | bytes 393224 | tf_op jit(solution)/shard_map/ppermute | solution.py:257
  38.0 4.4 %collective-permute-start.7 = (bf16[256,256]{1,0:T(8,128)(2,1)S(1)}, bf16[256,256]{1,0:T(8,128)(2,1)S(1)}, u32[]{:S(2)}, u32[]{:S(2)}) collective-permute-start(bf16[256,256]{1,0:T(8,128)(2,1)S(1)} %get-tuple-element.17.own_ref), channel_id=1, source_target_pairs={{0,4},{2,6},{4,0},{6,2},{1,5},{3,7},{5,1},{7,3},{8,12},{10,14},{12... | collective-permute-start | bytes 393224 | tf_op jit(solution)/shard_map/ppermute | solution.py:257
  42.4 3.1 %collective-permute-start.8 = (bf16[256,256]{1,0:T(8,128)(2,1)S(1)}, bf16[256,256]{1,0:T(8,128)(2,1)S(1)}, u32[]{:S(2)}, u32[]{:S(2)}) collective-permute-start(bf16[256,256]{1,0:T(8,128)(2,1)S(1)} %get-tuple-element.17.own_ref), channel_id=1, source_target_pairs={{0,6},{2,0},{4,2},{6,4},{1,7},{3,1},{5,3},{7,5},{8,14},{10,8},{12,... | collective-permute-start | bytes 393224 | tf_op jit(solution)/shard_map/ppermute | solution.py:257
  45.5 2.7 %collective-permute-done.8.p3_ref = bf16[256,256]{1,0:T(8,128)(2,1)S(1)} collective-permute-done((bf16[256,256]{1,0:T(8,128)(2,1)S(1)}, bf16[256,256]{1,0:T(8,128)(2,1)S(1)}, u32[]{:S(2)}, u32[]{:S(2)}) %collective-permute-start.8) | collective-permute-done | bytes 131104 | tf_op jit(solution)/shard_map/ppermute | solution.py:257
  48.2 9.1 %collective-permute-start.9 = (bf16[4,256,256]{2,1,0:T(8,128)(2,1)S(1)}, bf16[4,256,256]{2,1,0:T(8,128)(2,1)S(1)}, u32[]{:S(2)}, u32[]{:S(2)}) collective-permute-start(bf16[4,256,256]{2,1,0:T(8,128)(2,1)S(1)} %shard_map.132.mine_ref), channel_id=1, source_target_pairs={{0,1},{1,0},{2,3},{3,2},{4,5},{5,4},{6,7},{7,6},{8,9},{9,8},{10,11... | collective-permute-start | bytes 1572872 | tf_op jit(solution)/shard_map/ppermute | solution.py:301
  57.3 7.0 %all-to-all-start.1 = ((f32[32,8,256]{2,1,0:T(8,128)}), f32[32,8,256]{2,1,0:T(8,128)S(1)}, u32[]{:S(2)}, u32[]{:S(2)}) async-start(f32[32,8,256]{2,1,0:T(8,128)} %copy-done.4), calls=%async_computation.1 | async-start | bytes 524288 | tf_op jit(solution)/shard_map/all_to_all | solution.py:248
  64.3 3.3 %collective-permute-start = (bf16[32,2048]{1,0:T(8,128)(2,1)S(1)}, bf16[32,2048]{1,0:T(8,128)(2,1)}, u32[]{:S(2)}, u32[]{:S(2)}) collective-permute-start(bf16[32,2048]{1,0:T(8,128)(2,1)S(1)} %copy-done.3), channel_id=1, source_target_pairs={{0,2},{2,4},{4,6},{6,0},{1,3},{3,5},{5,7},{7,1},{8,10},{10,12},{12... | collective-permute-start | bytes 393224 | tf_op jit(solution)/shard_map/ppermute | solution.py:257
  67.6 4.3 %collective-permute-start.1 = (bf16[32,2048]{1,0:T(8,128)(2,1)S(1)}, bf16[32,2048]{1,0:T(8,128)(2,1)}, u32[]{:S(2)}, u32[]{:S(2)}) collective-permute-start(bf16[32,2048]{1,0:T(8,128)(2,1)S(1)} %copy-done.3), channel_id=1, source_target_pairs={{0,4},{2,6},{4,0},{6,2},{1,5},{3,7},{5,1},{7,3},{8,12},{10,14},{12... | collective-permute-start | bytes 393224 | tf_op jit(solution)/shard_map/ppermute | solution.py:257
  71.9 3.1 %collective-permute-start.2 = (bf16[32,2048]{1,0:T(8,128)(2,1)S(1)}, bf16[32,2048]{1,0:T(8,128)(2,1)}, u32[]{:S(2)}, u32[]{:S(2)}) collective-permute-start(bf16[32,2048]{1,0:T(8,128)(2,1)S(1)} %copy-done.3), channel_id=1, source_target_pairs={{0,6},{2,0},{4,2},{6,4},{1,7},{3,1},{5,3},{7,5},{8,14},{10,8},{12,... | collective-permute-start | bytes 393224 | tf_op jit(solution)/shard_map/ppermute | solution.py:257
  75.0 3.1 %collective-permute-start.11 = (bf16[256,2048]{1,0:T(8,128)(2,1)}, bf16[256,2048]{1,0:T(8,128)(2,1)}, u32[]{:S(2)}, u32[]{:S(2)}) collective-permute-start(bf16[256,2048]{1,0:T(8,128)(2,1)} %w_ref.1), channel_id=1, source_target_pairs={{0,1},{1,0},{2,3},{3,2},{4,5},{5,4},{6,7},{7,6},{8,9},{9,8},{10,11... | collective-permute-start | bytes 3145736 | tf_op jit(solution)/shard_map/ppermute | solution.py:292
  78.2 2.1 %shard_map.133 = bf16[4,2,256,256]{3,2,1,0:T(8,128)(2,1)} custom-call(bf16[4,256,256]{2,1,0:T(8,128)(2,1)S(1)} %shard_map.132.mine_ref, bf16[4,256,256]{2,1,0:T(8,128)(2,1)S(1)} %collective-permute-done.9.theirs_ref, f32[32,8,256]{2,1,0:T(8,128)S(1)} %all-to-all-done.1.mod_ref, f32[1,2048]{1,0:T(1,128)S(1)} %bitcast.3, bf16[2048,256]{1,0:T(8,128)(2,1)S(1)} %copy-done, ...), custom_call_target="tpu_custom_call" | custom-call | flops 1000000000 | tf_op jit(solution)/shard_map/pallas_call | solution.py:302
  80.3 4.0 %all-to-all-start.2 = ((bf16[4,2,256,256]{3,2,1,0:T(8,128)(2,1)}), bf16[4,2,256,256]{3,2,1,0:T(8,128)(2,1)S(1)}, u32[]{:S(2)}, u32[]{:S(2)}) async-start(bf16[4,2,256,256]{3,2,1,0:T(8,128)(2,1)} %shard_map.133), calls=%async_computation.2 | async-start | bytes 2097152 | tf_op jit(solution)/shard_map/all_to_all | solution.py:248
  85.5 2.3 %collective-permute-start.3 = (bf16[4,32,2048]{2,1,0:T(8,128)(2,1)S(1)}, bf16[4,32,2048]{2,1,0:T(8,128)(2,1)S(1)}, u32[]{:S(2)}, u32[]{:S(2)}) collective-permute-start(bf16[4,32,2048]{2,1,0:T(8,128)(2,1)S(1)} %shard_map.127.mine_ref), channel_id=1, source_target_pairs={{0,1},{1,0},{2,3},{3,2},{4,5},{5,4},{6,7},{7,6},{8,9},{9,8},{10,11... | collective-permute-start | bytes 1572872 | tf_op jit(solution)/shard_map/ppermute | solution.py:299
  87.8 1.6 %collective-permute-done.3.theirs_ref = bf16[4,32,2048]{2,1,0:T(8,128)(2,1)S(1)} collective-permute-done((bf16[4,32,2048]{2,1,0:T(8,128)(2,1)S(1)}, bf16[4,32,2048]{2,1,0:T(8,128)(2,1)S(1)}, u32[]{:S(2)}, u32[]{:S(2)}) %collective-permute-start.3) | collective-permute-done | bytes 524320 | tf_op jit(solution)/shard_map/ppermute | solution.py:299
  89.4 1.5 %shard_map.130 = (bf16[256,256]{1,0:T(8,128)(2,1)S(1)}, bf16[2,128,256]{2,1,0:T(8,128)(2,1)S(1)}, bf16[2,128,256]{2,1,0:T(8,128)(2,1)S(1)}, f32[1,2048]{1,0:T(1,128)S(1)}) custom-call(bf16[4,32,2048]{2,1,0:T(8,128)(2,1)S(1)} %shard_map.127.mine_ref, bf16[4,32,2048]{2,1,0:T(8,128)(2,1)S(1)} %collective-permute-done.3.theirs_ref, ...), custom_call_target="tpu_custom_call" | custom-call | flops 1000000000 | tf_op jit(solution)/shard_map/pallas_call | solution.py:307
  91.6 3.6 %collective-permute-start.4 = (bf16[2,128,256]{2,1,0:T(8,128)(2,1)S(1)}, bf16[2,128,256]{2,1,0:T(8,128)(2,1)S(1)}, u32[]{:S(2)}, u32[]{:S(2)}) collective-permute-start(bf16[2,128,256]{2,1,0:T(8,128)(2,1)S(1)} %get-tuple-element.15.tail_ref), channel_id=1, source_target_pairs={{0,8},{8,16},{16,24},{24,32},{32,40},{40,48},{48,56},{56,64},{64,7... | collective-permute-start | bytes 393224 | tf_op jit(solution)/shard_map/ppermute | solution.py:319
  95.2 1.3 %collective-permute-start.5 = (bf16[2,128,256]{2,1,0:T(8,128)(2,1)S(1)}, bf16[2,128,256]{2,1,0:T(8,128)(2,1)S(1)}, u32[]{:S(2)}, u32[]{:S(2)}) collective-permute-start(bf16[2,128,256]{2,1,0:T(8,128)(2,1)S(1)} %get-tuple-element.16.head_ref), channel_id=1, source_target_pairs={{8,0},{16,8},{24,16},{32,24},{40,32},{48,40},{56,48},{64,56},{72,6... | collective-permute-start | bytes 393224 | tf_op jit(solution)/shard_map/ppermute | solution.py:320
  97.2 1.4 %collective-permute-done.4.prev_ref = bf16[2,128,256]{2,1,0:T(8,128)(2,1)S(1)} collective-permute-done((bf16[2,128,256]{2,1,0:T(8,128)(2,1)S(1)}, bf16[2,128,256]{2,1,0:T(8,128)(2,1)S(1)}, u32[]{:S(2)}, u32[]{:S(2)}) %collective-permute-start.4) | collective-permute-done | bytes 131104 | tf_op jit(solution)/shard_map/ppermute | solution.py:319
  98.6 2.9 %collective-permute-done.5.next_ref = bf16[2,128,256]{2,1,0:T(8,128)(2,1)S(1)} collective-permute-done((bf16[2,128,256]{2,1,0:T(8,128)(2,1)S(1)}, bf16[2,128,256]{2,1,0:T(8,128)(2,1)S(1)}, u32[]{:S(2)}, u32[]{:S(2)}) %collective-permute-start.5) | collective-permute-done | bytes 131104 | tf_op jit(solution)/shard_map/ppermute | solution.py:320
  103.3 2.1 %shard_map.134 = (bf16[128,256]{1,0:T(8,128)(2,1)S(1)}, bf16[128,256]{1,0:T(8,128)(2,1)S(1)}) custom-call(bf16[256,256]{1,0:T(8,128)(2,1)S(1)} %copy-done.14, bf16[2,128,256]{2,1,0:T(8,128)(2,1)S(1)} %collective-permute-done.4.prev_ref, bf16[2,128,256]{2,1,0:T(8,128)(2,1)S(1)} %copy-done.16, bf16[2,128,256]{2,1,0:T(8,128)(2,1)S(1)} %copy-done.18, ...), custom_call_target="tpu_custom_call" | custom-call | flops 1000000000 | tf_op jit(solution)/shard_map/pallas_call | solution.py:328
  105.4 3.4 %collective-permute-start.10 = (bf16[128,256]{1,0:T(8,128)(2,1)S(1)}, bf16[128,256]{1,0:T(8,128)(2,1)S(1)}, u32[]{:S(2)}, u32[]{:S(2)}) collective-permute-start(bf16[128,256]{1,0:T(8,128)(2,1)S(1)} %get-tuple-element.19), channel_id=1, source_target_pairs={{0,1},{1,0},{2,3},{3,2},{4,5},{5,4},{6,7},{7,6},{8,9},{9,8},{10,11... | collective-permute-start | bytes 196616 | tf_op jit(solution)/shard_map/ppermute | solution.py:331
  109.7 1.7 %shard_map.135 = bf16[4,32,2048]{2,1,0:T(8,128)(2,1)S(1)} custom-call(bf16[128,256]{1,0:T(8,128)(2,1)S(1)} %get-tuple-element.18.mine_ref, bf16[128,256]{1,0:T(8,128)(2,1)S(1)} %collective-permute-done.10.got_ref, bf16[256,2048]{1,0:T(8,128)(2,1)S(1)} %copy-done.12, bf16[256,2048]{1,0:T(8,128)(2,1)} %collective-permute-done.11.wp_ref), custom_call_target="tpu_custom_call" | custom-call | flops 1000000000 | tf_op jit(solution)/shard_map/pallas_call | solution.py:332
  111.4 11.6 %all_to_all.21.parts_ref = bf16[4,32,2048]{2,1,0:T(8,128)(2,1)S(1)} all-to-all(bf16[4,32,2048]{2,1,0:T(8,128)(2,1)S(1)} %shard_map.135), channel_id=1, replica_groups=mesh['z'=16,'y'=4,'x'=4,'c'=2] {'x'}, dimensions={0} | all-to-all | bytes 1048576 | tf_op jit(solution)/shard_map/all_to_all | solution.py:248
  (58 shorter events, 11.4 us)
Async XLA Ops:
  4.7 73.5 %copy-start.1 = (bf16[2048,256]{1,0:T(8,128)(2,1)S(1)}, bf16[2048,256]{1,0:T(8,128)(2,1)}, u32[]{:S(2)}) copy-start(bf16[2048,256]{1,0:T(8,128)(2,1)} %wv_ref.3) | copy-start | bytes 3145732
  34.1 44.0 %copy-start = (bf16[2048,256]{1,0:T(8,128)(2,1)S(1)}, bf16[2048,256]{1,0:T(8,128)(2,1)}, u32[]{:S(2)}) copy-start(bf16[2048,256]{1,0:T(8,128)(2,1)} %wk_ref.3) | copy-start | bytes 3145732
  34.9 10.6 %collective-permute-start.6 = (bf16[256,256]{1,0:T(8,128)(2,1)S(1)}, bf16[256,256]{1,0:T(8,128)(2,1)S(1)}, u32[]{:S(2)}, u32[]{:S(2)}) collective-permute-start(bf16[256,256]{1,0:T(8,128)(2,1)S(1)} %get-tuple-element.17.own_ref), channel_id=1, source_target_pairs={{0,2},{2,4},{4,6},{6,0},{1,3},{3,5},{5,7},{7,1},{8,10},{10,12},{12... | collective-permute-start | bytes 393224 | tf_op jit(solution)/shard_map/ppermute | solution.py:257
  38.0 7.4 %collective-permute-start.7 = (bf16[256,256]{1,0:T(8,128)(2,1)S(1)}, bf16[256,256]{1,0:T(8,128)(2,1)S(1)}, u32[]{:S(2)}, u32[]{:S(2)}) collective-permute-start(bf16[256,256]{1,0:T(8,128)(2,1)S(1)} %get-tuple-element.17.own_ref), channel_id=1, source_target_pairs={{0,4},{2,6},{4,0},{6,2},{1,5},{3,7},{5,1},{7,3},{8,12},{10,14},{12... | collective-permute-start | bytes 393224 | tf_op jit(solution)/shard_map/ppermute | solution.py:257
  42.4 5.7 %collective-permute-start.8 = (bf16[256,256]{1,0:T(8,128)(2,1)S(1)}, bf16[256,256]{1,0:T(8,128)(2,1)S(1)}, u32[]{:S(2)}, u32[]{:S(2)}) collective-permute-start(bf16[256,256]{1,0:T(8,128)(2,1)S(1)} %get-tuple-element.17.own_ref), channel_id=1, source_target_pairs={{0,6},{2,0},{4,2},{6,4},{1,7},{3,1},{5,3},{7,5},{8,14},{10,8},{12,... | collective-permute-start | bytes 393224 | tf_op jit(solution)/shard_map/ppermute | solution.py:257
  48.2 30.0 %collective-permute-start.9 = (bf16[4,256,256]{2,1,0:T(8,128)(2,1)S(1)}, bf16[4,256,256]{2,1,0:T(8,128)(2,1)S(1)}, u32[]{:S(2)}, u32[]{:S(2)}) collective-permute-start(bf16[4,256,256]{2,1,0:T(8,128)(2,1)S(1)} %shard_map.132.mine_ref), channel_id=1, source_target_pairs={{0,1},{1,0},{2,3},{3,2},{4,5},{5,4},{6,7},{7,6},{8,9},{9,8},{10,11... | collective-permute-start | bytes 1572872 | tf_op jit(solution)/shard_map/ppermute | solution.py:301
  57.3 7.0 %copy-start.3 = (bf16[32,2048]{1,0:T(8,128)(2,1)S(1)}, bf16[32,2048]{1,0:T(8,128)(2,1)}, u32[]{:S(2)}) copy-start(bf16[32,2048]{1,0:T(8,128)(2,1)} %lat_ref.1) | copy-start | bytes 393220
  57.3 20.9 %copy-start.6 = (f32[2048]{0:T(1024)S(1)}, f32[2048]{0:T(1024)}, u32[]{:S(2)}) copy-start(f32[2048]{0:T(1024)} %param.17) | copy-start | bytes 24580
  57.3 20.8 %all-to-all-start.1 = ((f32[32,8,256]{2,1,0:T(8,128)}), f32[32,8,256]{2,1,0:T(8,128)S(1)}, u32[]{:S(2)}, u32[]{:S(2)}) async-start(f32[32,8,256]{2,1,0:T(8,128)} %copy-done.4), calls=%async_computation.1 | async-start | bytes 524288 | tf_op jit(solution)/shard_map/all_to_all | solution.py:248
  64.3 20.0 %collective-permute-start = (bf16[32,2048]{1,0:T(8,128)(2,1)S(1)}, bf16[32,2048]{1,0:T(8,128)(2,1)}, u32[]{:S(2)}, u32[]{:S(2)}) collective-permute-start(bf16[32,2048]{1,0:T(8,128)(2,1)S(1)} %copy-done.3), channel_id=1, source_target_pairs={{0,2},{2,4},{4,6},{6,0},{1,3},{3,5},{5,7},{7,1},{8,10},{10,12},{12... | collective-permute-start | bytes 393224 | tf_op jit(solution)/shard_map/ppermute | solution.py:257
  67.6 16.7 %collective-permute-start.1 = (bf16[32,2048]{1,0:T(8,128)(2,1)S(1)}, bf16[32,2048]{1,0:T(8,128)(2,1)}, u32[]{:S(2)}, u32[]{:S(2)}) collective-permute-start(bf16[32,2048]{1,0:T(8,128)(2,1)S(1)} %copy-done.3), channel_id=1, source_target_pairs={{0,4},{2,6},{4,0},{6,2},{1,5},{3,7},{5,1},{7,3},{8,12},{10,14},{12... | collective-permute-start | bytes 393224 | tf_op jit(solution)/shard_map/ppermute | solution.py:257
  71.9 12.4 %collective-permute-start.2 = (bf16[32,2048]{1,0:T(8,128)(2,1)S(1)}, bf16[32,2048]{1,0:T(8,128)(2,1)}, u32[]{:S(2)}, u32[]{:S(2)}) collective-permute-start(bf16[32,2048]{1,0:T(8,128)(2,1)S(1)} %copy-done.3), channel_id=1, source_target_pairs={{0,6},{2,0},{4,2},{6,4},{1,7},{3,1},{5,3},{7,5},{8,14},{10,8},{12,... | collective-permute-start | bytes 393224 | tf_op jit(solution)/shard_map/ppermute | solution.py:257
  75.0 33.8 %collective-permute-start.11 = (bf16[256,2048]{1,0:T(8,128)(2,1)}, bf16[256,2048]{1,0:T(8,128)(2,1)}, u32[]{:S(2)}, u32[]{:S(2)}) collective-permute-start(bf16[256,2048]{1,0:T(8,128)(2,1)} %w_ref.1), channel_id=1, source_target_pairs={{0,1},{1,0},{2,3},{3,2},{4,5},{5,4},{6,7},{7,6},{8,9},{9,8},{10,11... | collective-permute-start | bytes 3145736 | tf_op jit(solution)/shard_map/ppermute | solution.py:292
  80.3 21.2 %all-to-all-start.2 = ((bf16[4,2,256,256]{3,2,1,0:T(8,128)(2,1)}), bf16[4,2,256,256]{3,2,1,0:T(8,128)(2,1)S(1)}, u32[]{:S(2)}, u32[]{:S(2)}) async-start(bf16[4,2,256,256]{3,2,1,0:T(8,128)(2,1)} %shard_map.133), calls=%async_computation.2 | async-start | bytes 2097152 | tf_op jit(solution)/shard_map/all_to_all | solution.py:248
  84.3 5.1 %copy-start.2 = (bf16[2048,256]{1,0:T(8,128)(2,1)S(1)}, bf16[2048,256]{1,0:T(8,128)(2,1)}, u32[]{:S(2)}) copy-start(bf16[2048,256]{1,0:T(8,128)(2,1)} %wq_ref.1) | copy-start | bytes 3145732
  85.5 11.0 %copy-start.19 = (f32[16,15,31]{2,0,1:T(8,128)S(1)}, f32[16,15,31]{2,0,1:T(8,128)}, u32[]{:S(2)}) copy-start(f32[16,15,31]{2,0,1:T(8,128)} %param.25) | copy-start | bytes 89284
  85.5 3.9 %collective-permute-start.3 = (bf16[4,32,2048]{2,1,0:T(8,128)(2,1)S(1)}, bf16[4,32,2048]{2,1,0:T(8,128)(2,1)S(1)}, u32[]{:S(2)}, u32[]{:S(2)}) collective-permute-start(bf16[4,32,2048]{2,1,0:T(8,128)(2,1)S(1)} %shard_map.127.mine_ref), channel_id=1, source_target_pairs={{0,1},{1,0},{2,3},{3,2},{4,5},{5,4},{6,7},{7,6},{8,9},{9,8},{10,11... | collective-permute-start | bytes 1572872 | tf_op jit(solution)/shard_map/ppermute | solution.py:299
  91.6 5.0 %copy-start.15 = (bf16[2,128,256]{2,1,0:T(8,128)(2,1)}, bf16[2,128,256]{2,1,0:T(8,128)(2,1)S(1)}, u32[]{:S(2)}) copy-start(bf16[2,128,256]{2,1,0:T(8,128)(2,1)S(1)} %get-tuple-element.16.head_ref) | copy-start | bytes 393220
  91.6 5.0 %copy-start.17 = (bf16[2,128,256]{2,1,0:T(8,128)(2,1)}, bf16[2,128,256]{2,1,0:T(8,128)(2,1)S(1)}, u32[]{:S(2)}) copy-start(bf16[2,128,256]{2,1,0:T(8,128)(2,1)S(1)} %get-tuple-element.15.tail_ref) | copy-start | bytes 393220
  91.6 7.0 %collective-permute-start.4 = (bf16[2,128,256]{2,1,0:T(8,128)(2,1)S(1)}, bf16[2,128,256]{2,1,0:T(8,128)(2,1)S(1)}, u32[]{:S(2)}, u32[]{:S(2)}) collective-permute-start(bf16[2,128,256]{2,1,0:T(8,128)(2,1)S(1)} %get-tuple-element.15.tail_ref), channel_id=1, source_target_pairs={{0,8},{8,16},{16,24},{24,32},{32,40},{40,48},{48,56},{56,64},{64,7... | collective-permute-start | bytes 393224 | tf_op jit(solution)/shard_map/ppermute | solution.py:319
  95.2 6.3 %collective-permute-start.5 = (bf16[2,128,256]{2,1,0:T(8,128)(2,1)S(1)}, bf16[2,128,256]{2,1,0:T(8,128)(2,1)S(1)}, u32[]{:S(2)}, u32[]{:S(2)}) collective-permute-start(bf16[2,128,256]{2,1,0:T(8,128)(2,1)S(1)} %get-tuple-element.16.head_ref), channel_id=1, source_target_pairs={{8,0},{16,8},{24,16},{32,24},{40,32},{48,40},{56,48},{64,56},{72,6... | collective-permute-start | bytes 393224 | tf_op jit(solution)/shard_map/ppermute | solution.py:320
  96.6 4.9 %copy-start.14 = (bf16[256,256]{1,0:T(8,128)(2,1)S(1)}, bf16[256,256]{1,0:T(8,128)(2,1)}, u32[]{:S(2)}) copy-start(bf16[256,256]{1,0:T(8,128)(2,1)} %copy-done.13) | copy-start | bytes 393220
  103.3 6.4 %copy-start.12 = (bf16[256,2048]{1,0:T(8,128)(2,1)S(1)}, bf16[256,2048]{1,0:T(8,128)(2,1)}, u32[]{:S(2)}) copy-start(bf16[256,2048]{1,0:T(8,128)(2,1)} %w_ref.1) | copy-start | bytes 3145732
  105.4 4.3 %collective-permute-start.10 = (bf16[128,256]{1,0:T(8,128)(2,1)S(1)}, bf16[128,256]{1,0:T(8,128)(2,1)S(1)}, u32[]{:S(2)}, u32[]{:S(2)}) collective-permute-start(bf16[128,256]{1,0:T(8,128)(2,1)S(1)} %get-tuple-element.19), channel_id=1, source_target_pairs={{0,1},{1,0},{2,3},{3,2},{4,5},{5,4},{6,7},{7,6},{8,9},{9,8},{10,11... | collective-permute-start | bytes 196616 | tf_op jit(solution)/shard_map/ppermute | solution.py:331
  (10 other events, 7.5 us)

commit v3 on v2

v3 whole, which is shorter than its diff:
```python
import functools

import jax
import jax.numpy as jnp
from jax import lax
from jax.experimental import pallas as pl
from jax.experimental.pallas import tpu as pltpu
from jax.sharding import Mesh
from jax.sharding import PartitionSpec as P


HEAD_DIM = 128
GRID_W = 32
WIN_H = 8
WIN_W = 16
D = 2048
SP = ("z", "y")
TP = ("x", "c")
ALL = ("z", "y", "x", "c")
NORM_EPS = 1e-06
NEG_BIG = -1e30
LOG2E = 1.4426950408889634
BF = jnp.bfloat16
F32 = jnp.float32


VMEM_SPEC = pl.BlockSpec(memory_space=pltpu.VMEM)
HBM_SPEC = pl.BlockSpec(memory_space=pltpu.HBM)


def call(body, outs, scratch=(), flops=0, vmem=8 << 20, **specs):
    return pl.pallas_call(
        body,
        out_shape=outs,
        **specs,
        scratch_shapes=list(scratch),
        cost_estimate=pl.CostEstimate(flops=flops, bytes_accessed=0, transcendentals=0),
        compiler_params=pltpu.CompilerParams(vmem_limit_bytes=vmem),
    )


def in_hbm(array):
    return pltpu.with_memory_space_constraint(array, pltpu.HBM)


def shape(dims, dtype):
    return jax.ShapeDtypeStruct(dims, dtype)


def pack_rows(rows):
    high = [row.astype(BF).astype(F32) for row in rows]
    low = [rows[i] - high[i] for i in (0, 2, 4)]
    return jnp.concatenate(high + low, axis=0).astype(BF)


def unpack_rows(total):
    rows = [total[i : i + 1, :] for i in range(8)]
    return [rows[0] + rows[5], rows[1], rows[2] + rows[6], rows[3], rows[4] + rows[7]]


def mod_partial_body(
    cond_hbm, ctxc_hbm, wsh_hbm, wsc_hbm, wg_hbm, ctx_hbm, out_ref, pad_ref, act_ref, ctx_ref, sems
):
    sp = lax.axis_index("z") * 4 + lax.axis_index("y")
    tp = lax.axis_index("x") * 2 + lax.axis_index("c")
    row = sp // 4
    off = pl.multiple_of((sp % 4) * 32, 32)
    zero = jnp.zeros((32, 768), BF)
    for i in range(4):
        pad_ref[i * 32 : (i + 1) * 32] = zero
    cols = pl.ds(pl.multiple_of(tp * 256, 256), 256)
    copies = [
        pltpu.make_async_copy(src, dst, sems.at[i])
        for i, (src, dst) in enumerate(
            (
                (cond_hbm, act_ref.at[0]),
                (ctxc_hbm, act_ref.at[1]),
                (wsh_hbm, pad_ref.at[pl.ds(off, 32), 0:256]),
                (wsc_hbm, pad_ref.at[pl.ds(off, 32), 256:512]),
                (wg_hbm, pad_ref.at[pl.ds(off, 32), 512:768]),
                (ctx_hbm.at[:, cols], ctx_ref),
            )
        )
    ]
    for copy in copies:
        copy.start()
    for copy in copies:
        copy.wait()
    cond = act_ref[0, pl.ds(row, 1), :]
    ctxc = act_ref[1, pl.ds(row, 1), :]
    act = jnp.concatenate([cond, ctxc] * 4, axis=0)
    act = (act / (1.0 + jnp.exp(-act))).astype(BF)
    res = jnp.dot(act, pad_ref[...], preferred_element_type=F32)
    packed = pack_rows(
        [res[0:1, 0:256], res[1:2, 0:256], res[0:1, 256:512], res[1:2, 256:512], res[0:1, 512:768]]
    )
    ctx = ctx_ref[...]
    for i in range(out_ref.shape[0]):
        out_ref[i, 0:16] = ctx
        out_ref[i, 16:24] = packed


def relay_body(in_ref, out_ref):
    total = pack_rows(unpack_rows(jnp.sum(in_ref[:, 16:24, :].astype(F32), axis=0)))
    ctx = in_ref[:, 0:16, :].reshape(256, 256)
    for i in range(out_ref.shape[0]):
        out_ref[i, 0:256] = ctx
        out_ref[i, 256:264] = total


def relay_mod_body(in_ref, out_ref):
    total = jnp.concatenate([in_ref[x, 256:264, :] for x in range(4)], axis=1)
    for i in range(out_ref.shape[0]):
        out_ref[i] = total


def mod_row(mod_ref, x, c, kind):
    cols = slice(x * 256, (x + 1) * 256)
    total = mod_ref[c, :, cols].astype(F32)
    for y in range(1, 4):
        total = total + mod_ref[y * 2 + c, :, cols].astype(F32)
    return unpack_rows(total)[kind]


def gather_x_body(own_ref, p1_ref, p2_ref, p3_ref, out_ref):
    x = lax.axis_index("x")
    for d, ref in enumerate((own_ref, p1_ref, p2_ref, p3_ref)):
        out_ref[lax.rem(x - d + 4, 4)] = ref[...]


def ctx_kv_body(mine_ref, theirs_ref, mod_ref, gain_ref, wk_ref, wv_ref, out_ref, xn_ref):
    core = lax.axis_index("c")
    square = jnp.zeros((256, 256), F32)
    for ref in (mine_ref, theirs_ref):
        for j in range(4):
            x = ref[j, 0:256].astype(F32)
            square = square + x * x
    inv = lax.rsqrt(jnp.sum(square, axis=-1, keepdims=True) * (1.0 / D) + NORM_EPS)
    for ref, c in ((mine_ref, core), (theirs_ref, 1 - core)):
        total = mod_ref[c].astype(F32)
        for y in range(1, 4):
            total = total + mod_ref[y * 2 + c].astype(F32)
        for j in range(4):
            cols = pl.ds(pl.multiple_of((2 * j + c) * 256, 256), 256)
            part = total[:, j * 256 : (j + 1) * 256]
            gain = gain_ref[:, cols] * (1.0 + part[3:4])
            x = ref[j, 0:256].astype(F32)
            xn_ref[:, cols] = (x * inv * gain + part[1:2]).astype(BF)
    xn = xn_ref[...]
    k = jnp.dot(xn, wk_ref[...], preferred_element_type=F32).astype(BF)
    for i in range(out_ref.shape[0]):
        out_ref[i, 0] = k
    v = jnp.dot(xn, wv_ref[...], preferred_element_type=F32).astype(BF)
    for i in range(out_ref.shape[0]):
        out_ref[i, 1] = v


def table_body(in_ref, out_ref):
    out_ref[...] = jnp.zeros_like(out_ref)
    out_ref[:, 0:15, 0:31] = in_ref[...]


def qkv_body(
    mine_ref, theirs_ref, mod_ref, gain_ref, wq_hbm, wk_ref, wv_ref,
    q_ref, head_ref, tail_ref, gate_ref, xn_ref, wq_ref, sem,
):
    copy = pltpu.make_async_copy(wq_hbm, wq_ref, sem)
    copy.start()
    core = lax.axis_index("c")
    mods = [[mod_row(mod_ref, i // 2, i % 2, kind) for i in range(8)] for kind in (0, 2, 4)]
    shift, scale, gate = (jnp.concatenate(rows, axis=1) for rows in mods)
    gain = gain_ref[...] * (1.0 + scale)
    gate_ref[...] = gate
    for ref, c in ((mine_ref, core), (theirs_ref, 1 - core)):
        for j in range(4):
            x = ref[j].astype(F32)
            inv = lax.rsqrt(jnp.sum(x * x, axis=-1, keepdims=True) * (1.0 / D) + NORM_EPS)
            rows = pl.ds(pl.multiple_of((2 * j + c) * 32, 32), 32)
            xn_ref[rows, :] = (x * inv * gain + shift).astype(BF)
    xn = xn_ref[...]
    for i, w_ref in enumerate((wk_ref, wv_ref)):
        res = jnp.dot(xn, w_ref[...], preferred_element_type=F32).astype(BF)
        head_ref[i] = res[:128]
        tail_ref[i] = res[128:]
    copy.wait()
    q = jnp.dot(xn_ref[...], wq_ref[...], preferred_element_type=F32)
    q_ref[...] = (q * (LOG2E * HEAD_DIM**-0.5)).astype(BF)


def bias_body(rows_total, tab_ref, out_ref, exp_ref):
    sp = lax.axis_index("z") * 4 + lax.axis_index("y")
    tp = lax.axis_index("x") * 2 + lax.axis_index("c")
    first = sp * 8
    lane = lax.broadcasted_iota(jnp.int32, (32, 128), 1)
    col = lax.broadcasted_iota(jnp.int32, (32, 128), 0)
    key_col = lane % 32
    start = jnp.clip(col - WIN_W // 2, 0, GRID_W - WIN_W)
    col_in = (key_col >= start) & (key_col < start + WIN_W)
    quarter = lane // 32
    for h in range(2):
        tab = tab_ref[tp * 2 + h] * LOG2E
        for d in range(15):
            line = jnp.broadcast_to(tab[d : d + 1, :], (32, 128))
            for p in range(4):
                exp_ref[d, p] = pltpu.roll(line, (32 * p - 15) % 128, 1, stride=1, stride_axis=0)
        for r in range(8):
            a = jnp.clip(first + r - WIN_H // 2, 0, rows_total - WIN_H) - first + WIN_H // 2
            half = r // 4
            for s in range(3):
                seg = half + s
                block = jnp.full((32, 128), NEG_BIG, F32)
                for p in range(4):
                    k = seg * 4 + p
                    d = k - r + 3
                    if 0 <= d < 15:
                        ok = (k >= a) & (k < a + WIN_H)
                        block = jnp.where(
                            (quarter == p) & col_in & ok, exp_ref[d, p], block
                        )
                out_ref[h, half, s, (r % 4) * 32 : (r % 4) * 32 + 32, :] = block


def attend_body(
    q_hbm, prev_ref, head_hbm, tail_hbm, next_ref, bias_hbm, ctx_ref,
    mine_ref, other_ref, q_ref, kv_ref, bias_ref, sems,
):
    copies = [
        pltpu.make_async_copy(src, dst, sems.at[i])
        for i, (src, dst) in enumerate(
            (
                (q_hbm, q_ref),
                (head_hbm, kv_ref.at[0]),
                (tail_hbm, kv_ref.at[1]),
                (bias_hbm, bias_ref),
            )
        )
    ]
    for copy in copies:
        copy.start()
    segs = (prev_ref, kv_ref.at[0], kv_ref.at[1], next_ref)
    core = lax.axis_index("c")
    nt = (((1,), (1,)), ((), ()))
    copies[0].wait()
    for h in range(2):
        hc = slice(h * 128, (h + 1) * 128)
        kc = ctx_ref[:, 0, :, hc].reshape(1024, 128)
        vc = ctx_ref[:, 1, :, hc].reshape(1024, 128)
        s_ctx = lax.dot_general(q_ref[:, hc], kc, nt, preferred_element_type=F32)
        if h == 0:
            for copy in copies[1:]:
                copy.wait()
        s_win = [
            [
                lax.dot_general(
                    q_ref[half * 128 : (half + 1) * 128, hc],
                    segs[half + s][0, :, hc],
                    nt,
                    preferred_element_type=F32,
                )
                + bias_ref[h, half, s]
                for half in range(2)
            ]
            for s in range(3)
        ]
        s_win = [jnp.concatenate(pair, axis=0) for pair in s_win]
        peak = jnp.maximum(jnp.maximum(s_win[0], s_win[1]), s_win[2])
        for i in range(8):
            peak = jnp.maximum(peak, s_ctx[:, i * 128 : (i + 1) * 128])
        top = jnp.max(peak, axis=-1, keepdims=True)
        e_ctx = jnp.exp2(s_ctx - top)
        e_win = [jnp.exp2(s - top) for s in s_win]
        part = e_win[0] + e_win[1] + e_win[2]
        for i in range(8):
            part = part + e_ctx[:, i * 128 : (i + 1) * 128]
        total = jnp.sum(part, axis=-1, keepdims=True)
        acc = jnp.dot(e_ctx.astype(BF), vc, preferred_element_type=F32)
        for half in range(2):
            rows = slice(half * 128, (half + 1) * 128)
            acc_half = acc[rows]
            for s in range(3):
                acc_half = acc_half + jnp.dot(
                    e_win[s][rows].astype(BF),
                    segs[half + s][1, :, hc],
                    preferred_element_type=F32,
                )
            out = (acc_half / total[rows]).astype(BF)
            for i in range(2):
                even = out[i * 64 : i * 64 + 32]
                odd = out[i * 64 + 32 : i * 64 + 64]
                rows = slice((half * 2 + i) * 32, (half * 2 + i + 1) * 32)
                mine_ref[rows, hc] = jnp.where(core == 0, even, odd)
                other_ref[rows, hc] = jnp.where(core == 0, odd, even)


def out_own_body(mine_ref, w_ref, out_ref):
    out_ref[...] = jnp.dot(mine_ref[...], w_ref[...], preferred_element_type=F32)


def out_proj_body(own_ref, got_ref, wp_ref, out_ref):
    res = own_ref[...] + jnp.dot(got_ref[...], wp_ref[...], preferred_element_type=F32)
    out_ref[...] = res.astype(BF).reshape(4, 32, D)


def final_body(parts_ref, lat_ref, gate_ref, out_ref):
    branch = jnp.sum(parts_ref[...].astype(F32), axis=0)
    out_ref[...] = (lat_ref[...].astype(F32) + gate_ref[...] * branch).astype(BF)


def exchange(blocks, axes):
    return lax.all_to_all(blocks, axes, 0, 0, tiled=True)


SWAP = [(0, 1), (1, 0)]


def along_x(own):
    parts = [own]
    for d in (1, 2, 3):
        parts.append(lax.ppermute(own, "x", [(i, (i + d) % 4) for i in range(4)]))
    return parts


def on_device(
    latent,
    context,
    condition,
    ctx_cond,
    norm_gain,
    w_shift,
    w_scale,
    w_gate,
    w_query,
    w_key,
    w_value,
    w_out,
    rel_bias,
):
    gain = norm_gain.reshape(1, D)
    part = call(
        mod_partial_body,
        shape((16, 24, 256), BF),
        [
            pltpu.VMEM((128, 768), BF),
            pltpu.VMEM((2, 16, 128), F32),
            pltpu.VMEM((16, 256), BF),
            pltpu.SemaphoreType.DMA((6,)),
        ],
        flops=10**7,
        in_specs=[HBM_SPEC] * 6,
        out_specs=VMEM_SPEC,
    )(*map(in_hbm, (condition.reshape(16, 128), ctx_cond.reshape(16, 128), w_shift, w_scale, w_gate, context)))
    got = exchange(part, "z")
    lat_parts = along_x(latent)
    table = call(table_body, shape((16, 16, 128), F32), flops=10**7)(rel_bias)
    w_pair = lax.ppermute(w_out, "c", SWAP)
    relayed = call(relay_body, shape((4, 264, 256), BF), flops=10**7)(got)
    ctx_mine = exchange(relayed, "x")
    lat_mine = call(gather_x_body, shape((4, 32, D), BF), flops=10**8)(*lat_parts)
    lat_theirs = lax.ppermute(lat_mine, "c", SWAP)
    mod_own = call(relay_mod_body, shape((8, 8, 1024), BF), flops=10**7)(ctx_mine)
    mod = exchange(mod_own, ("y", "c"))
    ctx_theirs = lax.ppermute(ctx_mine, "c", SWAP)
    ctx_kv = call(
        ctx_kv_body, shape((4, 2, 256, 256), BF), [pltpu.VMEM((256, D), BF)], flops=10**9
    )(ctx_mine, ctx_theirs, mod, gain, w_key, w_value)
    ctx_all = exchange(ctx_kv, "y")

    q, head, tail, gate = call(
        qkv_body,
        (
            shape((256, 256), BF),
            shape((2, 128, 256), BF),
            shape((2, 128, 256), BF),
            shape((1, D), F32),
        ),
        [pltpu.VMEM((256, D), BF), pltpu.VMEM((D, 256), BF), pltpu.SemaphoreType.DMA],
        flops=2 * 10**9,
        in_specs=[VMEM_SPEC] * 4 + [HBM_SPEC] + [VMEM_SPEC] * 2,
        out_specs=[VMEM_SPEC] * 4,
        vmem=16 << 20,
    )(lat_mine, lat_theirs, mod, gain, in_hbm(w_query), w_key, w_value)
    prev = lax.ppermute(tail, SP, [(i, i + 1) for i in range(63)])
    nxt = lax.ppermute(head, SP, [(i + 1, i) for i in range(63)])
    bias = call(
        functools.partial(bias_body, 512),
        shape((2, 2, 3, 128, 128), F32),
        [pltpu.VMEM((15, 4, 32, 128), F32)],
        flops=10**8,
    )(table)
    att, away = call(
        attend_body,
        (shape((128, 256), BF), shape((128, 256), BF)),
        [
            pltpu.VMEM((256, 256), BF),
            pltpu.VMEM((2, 2, 128, 256), BF),
            pltpu.VMEM((2, 2, 3, 128, 128), F32),
            pltpu.SemaphoreType.DMA((4,)),
        ],
        flops=10**9,
        in_specs=[HBM_SPEC, VMEM_SPEC, HBM_SPEC, HBM_SPEC, VMEM_SPEC, HBM_SPEC, VMEM_SPEC],
        out_specs=[VMEM_SPEC] * 2,
    )(in_hbm(q), prev, in_hbm(head), in_hbm(tail), nxt, in_hbm(bias), ctx_all)
    other = lax.ppermute(away, "c", SWAP)
    own = call(out_own_body, shape((128, D), F32), flops=10**9)(att, w_out)
    parts = call(out_proj_body, shape((4, 32, D), BF), flops=10**9)(own, other, w_pair)
    arrived = exchange(parts, "x")
    return call(final_body, shape((32, D), BF))(arrived, latent, gate)


def solution(mesh):
    torus = Mesh(mesh.devices.reshape(16, 4, 4, 2), ALL)
    return jax.shard_map(
        on_device,
        mesh=torus,
        in_specs=(
            P(ALL, None),
            P(SP, None),
            P(),
            P(),
            P(),
            P(SP, TP),
            P(SP, TP),
            P(SP, TP),
            P(None, TP),
            P(None, TP),
            P(None, TP),
            P(TP, None),
            P(),
        ),
        out_specs=P(ALL, None),
        check_vma=False,
    )
```

time: 126 us -> 117 us (0.929)
  the two profiles are of different devices: /device:TPU:1 before, /device:TPU:32 now
where the time goes in v3:
time: 117 us; the launch traced here: 116 us
  blocking collectives  57.5 us (49%)
  starting transfers between devices  34.4 us (29%)
  Pallas kernels  16.4 us (14%)
  waiting for transfers between devices  6.46 us (6%)
    all_to_all x3, blocking collectives, exchange(): return lax.all_to_all(blocks, axes, 0, 0, tiled=True)  57.5 us
    ppermute x3, starting transfers between devices, along_x(): parts.append(lax.ppermute(own, 'x', [(i, (i + d) % 4) for i in range(4)]))  9.48 us
    all_to_all x2, starting transfers between devices, exchange(): return lax.all_to_all(blocks, axes, 0, 0, tiled=True)  8.52 us
    pallas_call x1, Pallas kernels, on_device(): call(qkv_body, (shape((256, 256), BF), shape((2, 128, 256), BF), shape((2...  4.41 us
    ppermute x1, starting transfers between devices, on_device(): nxt = lax.ppermute(head, SP, [(i + 1, i) for i in range(63)])  4.02 us
    ppermute x1, starting transfers between devices, on_device(): prev = lax.ppermute(tail, SP, [(i, i + 1) for i in range(63)])  3.93 us
    pallas_call x1, Pallas kernels, on_device(): call(ctx_kv_body, shape((4, 2, 256, 256), BF), [pltpu.VMEM((256, D), BF)]...  3.16 us
    pallas_call x1, Pallas kernels, on_device(): call(attend_body, (shape((128, 256), BF), shape((128, 256), BF)), [pltpu....  2.99 us
  transfers between devices with their start and end apart: 11, of which 5 were waited for; matrix products, arithmetic and copies ran while one was open for 0% of the time, Pallas kernels for 11%

profile of v3, /device:TPU:32, one launch (start us, length us, event | category | flops | bytes accessed | tf_op | source)
XLA Modules:
  0.0 115.9 jit_solution(2002539130373334158)
XLA Ops:
  0.0 1.0 shard_map.128
  1.0 30.9 %all_to_all.25.in_ref = bf16[16,24,256]{2,1,0:T(8,128)(2,1)S(1)} all-to-all(bf16[16,24,256]{2,1,0:T(8,128)(2,1)S(1)} %shard_map.128), channel_id=1, replica_groups=mesh['z'=16,'y'=4,'x'=4,'c'=2] {'z'}, dimensions={0} | all-to-all | bytes 393216 | tf_op jit(solution)/shard_map/all_to_all | solution.py:310
  32.0 13.3 %all_to_all.26.in_ref.mine_ref = bf16[4,264,256]{2,1,0:T(8,128)(2,1)S(1)} all-to-all(bf16[4,264,256]{2,1,0:T(8,128)(2,1)S(1)} %shard_map.129), channel_id=1, replica_groups=mesh['z'=16,'y'=4,'x'=4,'c'=2] {'x'}, dimensions={0} | all-to-all | bytes 1081344 | tf_op jit(solution)/shard_map/all_to_all | solution.py:310
  45.3 2.0 %collective-permute-start.6 = (bf16[4,264,256]{2,1,0:T(8,128)(2,1)S(1)}, bf16[4,264,256]{2,1,0:T(8,128)(2,1)}, u32[]{:S(2)}, u32[]{:S(2)}) collective-permute-start(bf16[4,264,256]{2,1,0:T(8,128)(2,1)S(1)} %all_to_all.26.in_ref.mine_ref), channel_id=1, source_target_pairs={{0,1},{1,0},{2,3},{3,2},{4,5},{5,4},{6,7},{7,6},{8,9},{9,8},{10,11... | collective-permute-start | bytes 1622024 | tf_op jit(solution)/shard_map/ppermute | solution.py:362
  47.4 2.5 %collective-permute-start = (bf16[32,2048]{1,0:T(8,128)(2,1)S(1)}, bf16[32,2048]{1,0:T(8,128)(2,1)S(1)}, u32[]{:S(2)}, u32[]{:S(2)}) collective-permute-start(bf16[32,2048]{1,0:T(8,128)(2,1)S(1)} %copy-done.3), channel_id=1, source_target_pairs={{0,2},{2,4},{4,6},{6,0},{1,3},{3,5},{5,7},{7,1},{8,10},{10,12},{12... | collective-permute-start | bytes 393224 | tf_op jit(solution)/shard_map/ppermute | solution.py:319
  49.9 4.0 %collective-permute-start.1 = (bf16[32,2048]{1,0:T(8,128)(2,1)S(1)}, bf16[32,2048]{1,0:T(8,128)(2,1)S(1)}, u32[]{:S(2)}, u32[]{:S(2)}) collective-permute-start(bf16[32,2048]{1,0:T(8,128)(2,1)S(1)} %copy-done.3), channel_id=1, source_target_pairs={{0,4},{2,6},{4,0},{6,2},{1,5},{3,7},{5,1},{7,3},{8,12},{10,14},{12... | collective-permute-start | bytes 393224 | tf_op jit(solution)/shard_map/ppermute | solution.py:319
  53.8 3.0 %collective-permute-start.2 = (bf16[32,2048]{1,0:T(8,128)(2,1)S(1)}, bf16[32,2048]{1,0:T(8,128)(2,1)S(1)}, u32[]{:S(2)}, u32[]{:S(2)}) collective-permute-start(bf16[32,2048]{1,0:T(8,128)(2,1)S(1)} %copy-done.3), channel_id=1, source_target_pairs={{0,6},{2,0},{4,2},{6,4},{1,7},{3,1},{5,3},{7,5},{8,14},{10,8},{12,... | collective-permute-start | bytes 393224 | tf_op jit(solution)/shard_map/ppermute | solution.py:319
  57.6 4.5 %all-to-all-start.2 = ((bf16[8,8,1024]{2,1,0:T(8,128)(2,1)}), bf16[8,8,1024]{2,1,0:T(8,128)(2,1)S(1)}, u32[]{:S(2)}, u32[]{:S(2)}) async-start(bf16[8,8,1024]{2,1,0:T(8,128)(2,1)} %shard_map.130), calls=%async_computation.2 | async-start | bytes 262144 | tf_op jit(solution)/shard_map/all_to_all | solution.py:310
  62.0 2.5 %collective-permute-start.8 = (bf16[256,2048]{1,0:T(8,128)(2,1)}, bf16[256,2048]{1,0:T(8,128)(2,1)}, u32[]{:S(2)}, u32[]{:S(2)}) collective-permute-start(bf16[256,2048]{1,0:T(8,128)(2,1)} %w_ref.1), channel_id=1, source_target_pairs={{0,1},{1,0},{2,3},{3,2},{4,5},{5,4},{6,7},{7,6},{8,9},{9,8},{10,11... | collective-permute-start | bytes 3145736 | tf_op jit(solution)/shard_map/ppermute | solution.py:355
  64.6 0.8 shard_map.127.mine_ref
  65.4 1.9 %collective-permute-start.3 = (bf16[4,32,2048]{2,1,0:T(8,128)(2,1)}, bf16[4,32,2048]{2,1,0:T(8,128)(2,1)}, u32[]{:S(2)}, u32[]{:S(2)}) collective-permute-start(bf16[4,32,2048]{2,1,0:T(8,128)(2,1)} %shard_map.127.mine_ref), channel_id=1, source_target_pairs={{0,1},{1,0},{2,3},{3,2},{4,5},{5,4},{6,7},{7,6},{8,9},{9,8},{10,11... | collective-permute-start | bytes 1572872 | tf_op jit(solution)/shard_map/ppermute | solution.py:359
  68.1 3.2 %shard_map.134 = bf16[4,2,256,256]{3,2,1,0:T(8,128)(2,1)} custom-call(bf16[4,264,256]{2,1,0:T(8,128)(2,1)S(1)} %all_to_all.26.in_ref.mine_ref, bf16[4,264,256]{2,1,0:T(8,128)(2,1)} %collective-permute-done.6.theirs_ref, bf16[8,8,1024]{2,1,0:T(8,128)(2,1)S(1)} %all-to-all-done.2.mod_ref, f32[1,2048]{1,0:T(1,128)S(1)} %bitcast.3, ...), custom_call_target="tpu_custom_call" | custom-call | flops 1000000000 | tf_op jit(solution)/shard_map/pallas_call | solution.py:363
  71.3 4.1 %all-to-all-start.3 = ((bf16[4,2,256,256]{3,2,1,0:T(8,128)(2,1)}), bf16[4,2,256,256]{3,2,1,0:T(8,128)(2,1)S(1)}, u32[]{:S(2)}, u32[]{:S(2)}) async-start(bf16[4,2,256,256]{3,2,1,0:T(8,128)(2,1)} %shard_map.134), calls=%async_computation.3 | async-start | bytes 2097152 | tf_op jit(solution)/shard_map/all_to_all | solution.py:310
  75.4 4.4 %shard_map.131 = (bf16[256,256]{1,0:T(8,128)(2,1)S(1)}, bf16[2,128,256]{2,1,0:T(8,128)(2,1)S(1)}, bf16[2,128,256]{2,1,0:T(8,128)(2,1)S(1)}, f32[1,2048]{1,0:T(1,128)S(1)}) custom-call(bf16[4,32,2048]{2,1,0:T(8,128)(2,1)} %shard_map.127.mine_ref, bf16[4,32,2048]{2,1,0:T(8,128)(2,1)} %collective-permute-done.3.theirs_ref, ...), custom_call_target="tpu_custom_call" | custom-call | flops 2000000000 | tf_op jit(solution)/shard_map/pallas_call | solution.py:368
  79.8 3.9 %collective-permute-start.4 = (bf16[2,128,256]{2,1,0:T(8,128)(2,1)S(1)}, bf16[2,128,256]{2,1,0:T(8,128)(2,1)S(1)}, u32[]{:S(2)}, u32[]{:S(2)}) collective-permute-start(bf16[2,128,256]{2,1,0:T(8,128)(2,1)S(1)} %get-tuple-element.12.tail_hbm), channel_id=1, source_target_pairs={{0,8},{8,16},{16,24},{24,32},{32,40},{40,48},{48,56},{56,64},{64,7... | collective-permute-start | bytes 393224 | tf_op jit(solution)/shard_map/ppermute | solution.py:382
  83.8 4.0 %collective-permute-start.5 = (bf16[2,128,256]{2,1,0:T(8,128)(2,1)S(1)}, bf16[2,128,256]{2,1,0:T(8,128)(2,1)S(1)}, u32[]{:S(2)}, u32[]{:S(2)}) collective-permute-start(bf16[2,128,256]{2,1,0:T(8,128)(2,1)S(1)} %get-tuple-element.13.head_hbm), channel_id=1, source_target_pairs={{8,0},{16,8},{24,16},{32,24},{40,32},{48,40},{56,48},{64,56},{72,6... | collective-permute-start | bytes 393224 | tf_op jit(solution)/shard_map/ppermute | solution.py:383
  88.5 0.9 copy-done.2
  89.4 2.5 %collective-permute-done.4.prev_ref = bf16[2,128,256]{2,1,0:T(8,128)(2,1)S(1)} collective-permute-done((bf16[2,128,256]{2,1,0:T(8,128)(2,1)S(1)}, bf16[2,128,256]{2,1,0:T(8,128)(2,1)S(1)}, u32[]{:S(2)}, u32[]{:S(2)}) %collective-permute-start.4) | collective-permute-done | bytes 131104 | tf_op jit(solution)/shard_map/ppermute | solution.py:382
  92.0 2.2 %all-to-all-done.3.ctx_ref = bf16[4,2,256,256]{3,2,1,0:T(8,128)(2,1)S(1)} async-done(((bf16[4,2,256,256]{3,2,1,0:T(8,128)(2,1)}), bf16[4,2,256,256]{3,2,1,0:T(8,128)(2,1)S(1)}, u32[]{:S(2)}, u32[]{:S(2)}) %all-to-all-start.3) | async-done | bytes 1048608 | tf_op jit(solution)/shard_map/all_to_all | solution.py:310
  94.2 3.0 %shard_map.135 = (bf16[128,256]{1,0:T(8,128)(2,1)S(1)}, bf16[128,256]{1,0:T(8,128)(2,1)S(1)}) custom-call(bf16[256,256]{1,0:T(8,128)(2,1)} %copy-done.8, bf16[2,128,256]{2,1,0:T(8,128)(2,1)S(1)} %collective-permute-done.4.prev_ref, bf16[2,128,256]{2,1,0:T(8,128)(2,1)} %copy-done.6, bf16[2,128,256]{2,1,0:T(8,128)(2,1)} %copy-done.7, ...), custom_call_target="tpu_custom_call" | custom-call | flops 1000000000 | tf_op jit(solution)/shard_map/pallas_call | solution.py:390
  97.2 1.9 %collective-permute-start.7 = (bf16[128,256]{1,0:T(8,128)(2,1)S(1)}, bf16[128,256]{1,0:T(8,128)(2,1)S(1)}, u32[]{:S(2)}, u32[]{:S(2)}) collective-permute-start(bf16[128,256]{1,0:T(8,128)(2,1)S(1)} %get-tuple-element.15), channel_id=1, source_target_pairs={{0,1},{1,0},{2,3},{3,2},{4,5},{5,4},{6,7},{7,6},{8,9},{9,8},{10,11... | collective-permute-start | bytes 196616 | tf_op jit(solution)/shard_map/ppermute | solution.py:403
  99.5 0.9 collective-permute-done.7.got_ref
  100.3 1.5 %shard_map.137 = bf16[4,32,2048]{2,1,0:T(8,128)(2,1)S(1)} custom-call(f32[128,2048]{1,0:T(8,128)S(1)} %shard_map.136.own_ref, bf16[128,256]{1,0:T(8,128)(2,1)S(1)} %collective-permute-done.7.got_ref, bf16[256,2048]{1,0:T(8,128)(2,1)} %collective-permute-done.8.wp_ref), custom_call_target="tpu_custom_call" | custom-call | flops 1000000000 | tf_op jit(solution)/shard_map/pallas_call | solution.py:405
  101.9 13.3 %all_to_all.27.parts_ref = bf16[4,32,2048]{2,1,0:T(8,128)(2,1)S(1)} all-to-all(bf16[4,32,2048]{2,1,0:T(8,128)(2,1)S(1)} %shard_map.137), channel_id=1, replica_groups=mesh['z'=16,'y'=4,'x'=4,'c'=2] {'x'}, dimensions={0} | all-to-all | bytes 1048576 | tf_op jit(solution)/shard_map/all_to_all | solution.py:310
  (34 shorter events, 3.4 us)
Async XLA Ops:
  31.9 15.5 %copy-start.3 = (bf16[32,2048]{1,0:T(8,128)(2,1)S(1)}, bf16[32,2048]{1,0:T(8,128)(2,1)}, u32[]{:S(2)}) copy-start(bf16[32,2048]{1,0:T(8,128)(2,1)} %lat_ref.1) | copy-start | bytes 393220
  32.0 36.2 %copy-start.1 = (bf16[2048,256]{1,0:T(8,128)(2,1)S(1)}, bf16[2048,256]{1,0:T(8,128)(2,1)}, u32[]{:S(2)}) copy-start(bf16[2048,256]{1,0:T(8,128)(2,1)} %wv_ref.3) | copy-start | bytes 3145732
  45.3 22.8 %copy-start = (bf16[2048,256]{1,0:T(8,128)(2,1)S(1)}, bf16[2048,256]{1,0:T(8,128)(2,1)}, u32[]{:S(2)}) copy-start(bf16[2048,256]{1,0:T(8,128)(2,1)} %wk_ref.3) | copy-start | bytes 3145732
  45.3 22.8 %collective-permute-start.6 = (bf16[4,264,256]{2,1,0:T(8,128)(2,1)S(1)}, bf16[4,264,256]{2,1,0:T(8,128)(2,1)}, u32[]{:S(2)}, u32[]{:S(2)}) collective-permute-start(bf16[4,264,256]{2,1,0:T(8,128)(2,1)S(1)} %all_to_all.26.in_ref.mine_ref), channel_id=1, source_target_pairs={{0,1},{1,0},{2,3},{3,2},{4,5},{5,4},{6,7},{7,6},{8,9},{9,8},{10,11... | collective-permute-start | bytes 1622024 | tf_op jit(solution)/shard_map/ppermute | solution.py:362
  47.4 17.2 %collective-permute-start = (bf16[32,2048]{1,0:T(8,128)(2,1)S(1)}, bf16[32,2048]{1,0:T(8,128)(2,1)S(1)}, u32[]{:S(2)}, u32[]{:S(2)}) collective-permute-start(bf16[32,2048]{1,0:T(8,128)(2,1)S(1)} %copy-done.3), channel_id=1, source_target_pairs={{0,2},{2,4},{4,6},{6,0},{1,3},{3,5},{5,7},{7,1},{8,10},{10,12},{12... | collective-permute-start | bytes 393224 | tf_op jit(solution)/shard_map/ppermute | solution.py:319
  49.9 14.7 %collective-permute-start.1 = (bf16[32,2048]{1,0:T(8,128)(2,1)S(1)}, bf16[32,2048]{1,0:T(8,128)(2,1)S(1)}, u32[]{:S(2)}, u32[]{:S(2)}) collective-permute-start(bf16[32,2048]{1,0:T(8,128)(2,1)S(1)} %copy-done.3), channel_id=1, source_target_pairs={{0,4},{2,6},{4,0},{6,2},{1,5},{3,7},{5,1},{7,3},{8,12},{10,14},{12... | collective-permute-start | bytes 393224 | tf_op jit(solution)/shard_map/ppermute | solution.py:319
  53.8 10.7 %collective-permute-start.2 = (bf16[32,2048]{1,0:T(8,128)(2,1)S(1)}, bf16[32,2048]{1,0:T(8,128)(2,1)S(1)}, u32[]{:S(2)}, u32[]{:S(2)}) collective-permute-start(bf16[32,2048]{1,0:T(8,128)(2,1)S(1)} %copy-done.3), channel_id=1, source_target_pairs={{0,6},{2,0},{4,2},{6,4},{1,7},{3,1},{5,3},{7,5},{8,14},{10,8},{12,... | collective-permute-start | bytes 393224 | tf_op jit(solution)/shard_map/ppermute | solution.py:319
  57.6 10.6 %all-to-all-start.2 = ((bf16[8,8,1024]{2,1,0:T(8,128)(2,1)}), bf16[8,8,1024]{2,1,0:T(8,128)(2,1)S(1)}, u32[]{:S(2)}, u32[]{:S(2)}) async-start(bf16[8,8,1024]{2,1,0:T(8,128)(2,1)} %shard_map.130), calls=%async_computation.2 | async-start | bytes 262144 | tf_op jit(solution)/shard_map/all_to_all | solution.py:310
  62.0 6.1 %copy-start.4 = (f32[2048]{0:T(1024)S(1)}, f32[2048]{0:T(1024)}, u32[]{:S(2)}) copy-start(f32[2048]{0:T(1024)} %param.17) | copy-start | bytes 24580
  62.0 37.4 %collective-permute-start.8 = (bf16[256,2048]{1,0:T(8,128)(2,1)}, bf16[256,2048]{1,0:T(8,128)(2,1)}, u32[]{:S(2)}, u32[]{:S(2)}) collective-permute-start(bf16[256,2048]{1,0:T(8,128)(2,1)} %w_ref.1), channel_id=1, source_target_pairs={{0,1},{1,0},{2,3},{3,2},{4,5},{5,4},{6,7},{7,6},{8,9},{9,8},{10,11... | collective-permute-start | bytes 3145736 | tf_op jit(solution)/shard_map/ppermute | solution.py:355
  65.4 9.9 %collective-permute-start.3 = (bf16[4,32,2048]{2,1,0:T(8,128)(2,1)}, bf16[4,32,2048]{2,1,0:T(8,128)(2,1)}, u32[]{:S(2)}, u32[]{:S(2)}) collective-permute-start(bf16[4,32,2048]{2,1,0:T(8,128)(2,1)} %shard_map.127.mine_ref), channel_id=1, source_target_pairs={{0,1},{1,0},{2,3},{3,2},{4,5},{5,4},{6,7},{7,6},{8,9},{9,8},{10,11... | collective-permute-start | bytes 1572872 | tf_op jit(solution)/shard_map/ppermute | solution.py:359
  71.3 22.9 %all-to-all-start.3 = ((bf16[4,2,256,256]{3,2,1,0:T(8,128)(2,1)}), bf16[4,2,256,256]{3,2,1,0:T(8,128)(2,1)S(1)}, u32[]{:S(2)}, u32[]{:S(2)}) async-start(bf16[4,2,256,256]{3,2,1,0:T(8,128)(2,1)} %shard_map.134), calls=%async_computation.3 | async-start | bytes 2097152 | tf_op jit(solution)/shard_map/all_to_all | solution.py:310
  75.4 12.4 %copy-start.9 = (f32[16,15,31]{2,0,1:T(8,128)S(1)}, f32[16,15,31]{2,0,1:T(8,128)}, u32[]{:S(2)}) copy-start(f32[16,15,31]{2,0,1:T(8,128)} %param.25) | copy-start | bytes 89284
  79.8 8.1 %copy-start.6 = (bf16[2,128,256]{2,1,0:T(8,128)(2,1)}, bf16[2,128,256]{2,1,0:T(8,128)(2,1)S(1)}, u32[]{:S(2)}) copy-start(bf16[2,128,256]{2,1,0:T(8,128)(2,1)S(1)} %get-tuple-element.13.head_hbm) | copy-start | bytes 393220
  79.8 8.1 %copy-start.7 = (bf16[2,128,256]{2,1,0:T(8,128)(2,1)}, bf16[2,128,256]{2,1,0:T(8,128)(2,1)S(1)}, u32[]{:S(2)}) copy-start(bf16[2,128,256]{2,1,0:T(8,128)(2,1)S(1)} %get-tuple-element.12.tail_hbm) | copy-start | bytes 393220
  79.8 8.1 %copy-start.8 = (bf16[256,256]{1,0:T(8,128)(2,1)}, bf16[256,256]{1,0:T(8,128)(2,1)S(1)}, u32[]{:S(2)}) copy-start(bf16[256,256]{1,0:T(8,128)(2,1)S(1)} %get-tuple-element.11.q_hbm) | copy-start | bytes 393220
  79.8 12.1 %collective-permute-start.4 = (bf16[2,128,256]{2,1,0:T(8,128)(2,1)S(1)}, bf16[2,128,256]{2,1,0:T(8,128)(2,1)S(1)}, u32[]{:S(2)}, u32[]{:S(2)}) collective-permute-start(bf16[2,128,256]{2,1,0:T(8,128)(2,1)S(1)} %get-tuple-element.12.tail_hbm), channel_id=1, source_target_pairs={{0,8},{8,16},{16,24},{24,32},{32,40},{40,48},{48,56},{56,64},{64,7... | collective-permute-start | bytes 393224 | tf_op jit(solution)/shard_map/ppermute | solution.py:382
  83.8 8.3 %collective-permute-start.5 = (bf16[2,128,256]{2,1,0:T(8,128)(2,1)S(1)}, bf16[2,128,256]{2,1,0:T(8,128)(2,1)S(1)}, u32[]{:S(2)}, u32[]{:S(2)}) collective-permute-start(bf16[2,128,256]{2,1,0:T(8,128)(2,1)S(1)} %get-tuple-element.13.head_hbm), channel_id=1, source_target_pairs={{8,0},{16,8},{24,16},{32,24},{40,32},{48,40},{56,48},{64,56},{72,6... | collective-permute-start | bytes 393224 | tf_op jit(solution)/shard_map/ppermute | solution.py:383
  88.5 0.9 copy-start.2
  94.2 4.9 %copy-start.5 = (bf16[256,2048]{1,0:T(8,128)(2,1)S(1)}, bf16[256,2048]{1,0:T(8,128)(2,1)}, u32[]{:S(2)}) copy-start(bf16[256,2048]{1,0:T(8,128)(2,1)} %w_ref.1) | copy-start | bytes 3145732
  97.2 3.1 %collective-permute-start.7 = (bf16[128,256]{1,0:T(8,128)(2,1)S(1)}, bf16[128,256]{1,0:T(8,128)(2,1)S(1)}, u32[]{:S(2)}, u32[]{:S(2)}) collective-permute-start(bf16[128,256]{1,0:T(8,128)(2,1)S(1)} %get-tuple-element.15), channel_id=1, source_target_pairs={{0,1},{1,0},{2,3},{3,2},{4,5},{5,4},{6,7},{7,6},{8,9},{9,8},{10,11... | collective-permute-start | bytes 196616 | tf_op jit(solution)/shard_map/ppermute | solution.py:403

commit v4 on v3

--- a/solution.py
+++ b/solution.py
@@ -14,9 +14,10 @@
 WIN_H = 8
 WIN_W = 16
 D = 2048
-SP = ("z", "y")
+Z = ("zh", "zl")
+SP = ("zh", "zl", "y")
 TP = ("x", "c")
-ALL = ("z", "y", "x", "c")
+ALL = ("zh", "zl", "y", "x", "c")
 NORM_EPS = 1e-06
 NEG_BIG = -1e30
 LOG2E = 1.4426950408889634
@@ -50,7 +51,7 @@
 def pack_rows(rows):
     high = [row.astype(BF).astype(F32) for row in rows]
     low = [rows[i] - high[i] for i in (0, 2, 4)]
-    return jnp.concatenate(high + low, axis=0).astype(BF)
+    return jnp.concatenate(high + low, axis=0)
 
 
 def unpack_rows(total):
@@ -61,7 +62,7 @@
 def mod_partial_body(
     cond_hbm, ctxc_hbm, wsh_hbm, wsc_hbm, wg_hbm, ctx_hbm, out_ref, pad_ref, act_ref, ctx_ref, sems
 ):
-    sp = lax.axis_index("z") * 4 + lax.axis_index("y")
+    sp = lax.axis_index(SP)
     tp = lax.axis_index("x") * 2 + lax.axis_index("c")
     row = sp // 4
     off = pl.multiple_of((sp % 4) * 32, 32)
@@ -94,32 +95,38 @@
     packed = pack_rows(
         [res[0:1, 0:256], res[1:2, 0:256], res[0:1, 256:512], res[1:2, 256:512], res[0:1, 512:768]]
     )
-    ctx = ctx_ref[...]
+    ctx = ctx_ref[...].astype(F32)
+    blocks = [jnp.concatenate([ctx[i * 8 : i * 8 + 8], packed], axis=0).astype(BF) for i in range(2)]
     for i in range(out_ref.shape[0]):
-        out_ref[i, 0:16] = ctx
-        out_ref[i, 16:24] = packed
+        out_ref[i] = blocks[i % 2]
 
 
 def relay_body(in_ref, out_ref):
-    total = pack_rows(unpack_rows(jnp.sum(in_ref[:, 16:24, :].astype(F32), axis=0)))
-    ctx = in_ref[:, 0:16, :].reshape(256, 256)
+    got = in_ref[...].astype(F32)
+    total = pack_rows(unpack_rows(jnp.sum(got[:, 8:16, :], axis=0)))
+    block = jnp.concatenate([got[:, 0:8, :].reshape(128, 256), total], axis=0).astype(BF)
     for i in range(out_ref.shape[0]):
-        out_ref[i, 0:256] = ctx
-        out_ref[i, 256:264] = total
-
-
-def relay_mod_body(in_ref, out_ref):
-    total = jnp.concatenate([in_ref[x, 256:264, :] for x in range(4)], axis=1)
-    for i in range(out_ref.shape[0]):
-        out_ref[i] = total
-
-
-def mod_row(mod_ref, x, c, kind):
-    cols = slice(x * 256, (x + 1) * 256)
-    total = mod_ref[c, :, cols].astype(F32)
+        out_ref[i] = block
+
+
+def column_block(x, c):
+    return pl.ds(pl.multiple_of((2 * x + c) * 256, 256), 256)
+
+
+def relay_mod_body(mine_ref, theirs_ref, out_ref):
+    core = lax.axis_index("c")
+    for ref, c in ((mine_ref, core), (theirs_ref, 1 - core)):
+        for x in range(4):
+            block = ref[x, 128:136, :]
+            for i in range(out_ref.shape[0]):
+                out_ref[i, :, column_block(x, c)] = block
+
+
+def sum_over_y(mod_ref, cols):
+    total = mod_ref[0, :, cols].astype(F32)
     for y in range(1, 4):
-        total = total + mod_ref[y * 2 + c, :, cols].astype(F32)
-    return unpack_rows(total)[kind]
+        total = total + mod_ref[y, :, cols].astype(F32)
+    return total
 
 
 def gather_x_body(own_ref, p1_ref, p2_ref, p3_ref, out_ref):
@@ -128,23 +135,23 @@
         out_ref[lax.rem(x - d + 4, 4)] = ref[...]
 
 
-def ctx_kv_body(mine_ref, theirs_ref, mod_ref, gain_ref, wk_ref, wv_ref, out_ref, xn_ref):
+def ctx_kv_body(mine_ref, theirs_ref, mod_ref, gain_hbm, wk_ref, wv_ref, out_ref, xn_ref, gain_ref, sem):
+    copy = pltpu.make_async_copy(gain_hbm, gain_ref, sem)
+    copy.start()
     core = lax.axis_index("c")
-    square = jnp.zeros((256, 256), F32)
+    square = jnp.zeros((128, 256), F32)
     for ref in (mine_ref, theirs_ref):
         for j in range(4):
-            x = ref[j, 0:256].astype(F32)
+            x = ref[j, 0:128].astype(F32)
             square = square + x * x
     inv = lax.rsqrt(jnp.sum(square, axis=-1, keepdims=True) * (1.0 / D) + NORM_EPS)
+    copy.wait()
     for ref, c in ((mine_ref, core), (theirs_ref, 1 - core)):
-        total = mod_ref[c].astype(F32)
-        for y in range(1, 4):
-            total = total + mod_ref[y * 2 + c].astype(F32)
         for j in range(4):
-            cols = pl.ds(pl.multiple_of((2 * j + c) * 256, 256), 256)
-            part = total[:, j * 256 : (j + 1) * 256]
+            cols = column_block(j, c)
+            part = sum_over_y(mod_ref, cols)
             gain = gain_ref[:, cols] * (1.0 + part[3:4])
-            x = ref[j, 0:256].astype(F32)
+            x = ref[j, 0:128].astype(F32)
             xn_ref[:, cols] = (x * inv * gain + part[1:2]).astype(BF)
     xn = xn_ref[...]
     k = jnp.dot(xn, wk_ref[...], preferred_element_type=F32).astype(BF)
@@ -160,20 +167,25 @@
     out_ref[:, 0:15, 0:31] = in_ref[...]
 
 
-def qkv_body(
-    mine_ref, theirs_ref, mod_ref, gain_ref, wq_hbm, wk_ref, wv_ref,
-    q_ref, head_ref, tail_ref, gate_ref, xn_ref, wq_ref, sem,
+def kv_body(
+    mine_hbm, theirs_hbm, mod_ref, gain_hbm, wk_ref, wv_ref,
+    head_ref, tail_ref, gate_ref, xn_ref, lat_ref, gain_ref, sems,
 ):
-    copy = pltpu.make_async_copy(wq_hbm, wq_ref, sem)
-    copy.start()
+    copies = [
+        pltpu.make_async_copy(src, lat_ref.at[i], sems.at[i])
+        for i, src in enumerate((mine_hbm, theirs_hbm))
+    ] + [pltpu.make_async_copy(gain_hbm, gain_ref, sems.at[2])]
+    for copy in copies:
+        copy.start()
     core = lax.axis_index("c")
-    mods = [[mod_row(mod_ref, i // 2, i % 2, kind) for i in range(8)] for kind in (0, 2, 4)]
-    shift, scale, gate = (jnp.concatenate(rows, axis=1) for rows in mods)
+    shift, _, scale, _, gate = unpack_rows(sum_over_y(mod_ref, slice(None)))
+    gate_ref[...] = gate
+    copies[2].wait()
     gain = gain_ref[...] * (1.0 + scale)
-    gate_ref[...] = gate
-    for ref, c in ((mine_ref, core), (theirs_ref, 1 - core)):
+    for i, c in enumerate((core, 1 - core)):
+        copies[i].wait()
         for j in range(4):
-            x = ref[j].astype(F32)
+            x = lat_ref[i, j].astype(F32)
             inv = lax.rsqrt(jnp.sum(x * x, axis=-1, keepdims=True) * (1.0 / D) + NORM_EPS)
             rows = pl.ds(pl.multiple_of((2 * j + c) * 32, 32), 32)
             xn_ref[rows, :] = (x * inv * gain + shift).astype(BF)
@@ -182,13 +194,15 @@
         res = jnp.dot(xn, w_ref[...], preferred_element_type=F32).astype(BF)
         head_ref[i] = res[:128]
         tail_ref[i] = res[128:]
-    copy.wait()
+
+
+def query_body(xn_ref, wq_ref, q_ref):
     q = jnp.dot(xn_ref[...], wq_ref[...], preferred_element_type=F32)
     q_ref[...] = (q * (LOG2E * HEAD_DIM**-0.5)).astype(BF)
 
 
 def bias_body(rows_total, tab_ref, out_ref, exp_ref):
-    sp = lax.axis_index("z") * 4 + lax.axis_index("y")
+    sp = lax.axis_index(SP)
     tp = lax.axis_index("x") * 2 + lax.axis_index("c")
     first = sp * 8
     lane = lax.broadcasted_iota(jnp.int32, (32, 128), 1)
@@ -221,8 +235,8 @@
 
 
 def attend_body(
-    q_hbm, prev_ref, head_hbm, tail_hbm, next_ref, bias_hbm, ctx_ref,
-    mine_ref, other_ref, q_ref, kv_ref, bias_ref, sems,
+    q_hbm, prev_ref, head_hbm, tail_hbm, next_ref, bias_hbm, ctx_ref, w_hbm, wp_hbm,
+    mine_ref, other_ref, w_ref, q_ref, kv_ref, bias_ref, sems,
 ):
     copies = [
         pltpu.make_async_copy(src, dst, sems.at[i])
@@ -232,6 +246,8 @@
                 (head_hbm, kv_ref.at[0]),
                 (tail_hbm, kv_ref.at[1]),
                 (bias_hbm, bias_ref),
+                (w_hbm, w_ref.at[0]),
+                (wp_hbm, w_ref.at[1]),
             )
         )
     ]
@@ -247,7 +263,7 @@
         vc = ctx_ref[:, 1, :, hc].reshape(1024, 128)
         s_ctx = lax.dot_general(q_ref[:, hc], kc, nt, preferred_element_type=F32)
         if h == 0:
-            for copy in copies[1:]:
+            for copy in copies[1:4]:
                 copy.wait()
         s_win = [
             [
@@ -290,14 +306,16 @@
                 rows = slice((half * 2 + i) * 32, (half * 2 + i + 1) * 32)
                 mine_ref[rows, hc] = jnp.where(core == 0, even, odd)
                 other_ref[rows, hc] = jnp.where(core == 0, odd, even)
+    for copy in copies[4:]:
+        copy.wait()
 
 
 def out_own_body(mine_ref, w_ref, out_ref):
-    out_ref[...] = jnp.dot(mine_ref[...], w_ref[...], preferred_element_type=F32)
-
-
-def out_proj_body(own_ref, got_ref, wp_ref, out_ref):
-    res = own_ref[...] + jnp.dot(got_ref[...], wp_ref[...], preferred_element_type=F32)
+    out_ref[...] = jnp.dot(mine_ref[...], w_ref[0], preferred_element_type=F32)
+
+
+def out_proj_body(own_ref, got_ref, w_ref, out_ref):
+    res = own_ref[...] + jnp.dot(got_ref[...], w_ref[1], preferred_element_type=F32)
     out_ref[...] = res.astype(BF).reshape(4, 32, D)
 
 
@@ -335,10 +353,10 @@
     w_out,
     rel_bias,
 ):
-    gain = norm_gain.reshape(1, D)
+    gain = in_hbm(norm_gain.reshape(1, D))
     part = call(
         mod_partial_body,
-        shape((16, 24, 256), BF),
+        shape((16, 16, 256), BF),
         [
             pltpu.VMEM((128, 768), BF),
             pltpu.VMEM((2, 16, 128), F32),
@@ -349,36 +367,42 @@
         in_specs=[HBM_SPEC] * 6,
         out_specs=VMEM_SPEC,
     )(*map(in_hbm, (condition.reshape(16, 128), ctx_cond.reshape(16, 128), w_shift, w_scale, w_gate, context)))
-    got = exchange(part, "z")
+    got = exchange(part, Z)
     lat_parts = along_x(latent)
     table = call(table_body, shape((16, 16, 128), F32), flops=10**7)(rel_bias)
     w_pair = lax.ppermute(w_out, "c", SWAP)
-    relayed = call(relay_body, shape((4, 264, 256), BF), flops=10**7)(got)
+    relayed = call(relay_body, shape((4, 136, 256), BF), flops=10**7)(got)
     ctx_mine = exchange(relayed, "x")
     lat_mine = call(gather_x_body, shape((4, 32, D), BF), flops=10**8)(*lat_parts)
     lat_theirs = lax.ppermute(lat_mine, "c", SWAP)
-    mod_own = call(relay_mod_body, shape((8, 8, 1024), BF), flops=10**7)(ctx_mine)
-    mod = exchange(mod_own, ("y", "c"))
     ctx_theirs = lax.ppermute(ctx_mine, "c", SWAP)
+    mod_own = call(relay_mod_body, shape((4, 8, D), BF), flops=10**7)(ctx_mine, ctx_theirs)
+    mod = exchange(mod_own, "y")
     ctx_kv = call(
-        ctx_kv_body, shape((4, 2, 256, 256), BF), [pltpu.VMEM((256, D), BF)], flops=10**9
+        ctx_kv_body,
+        shape((8, 2, 128, 256), BF),
+        [pltpu.VMEM((128, D), BF), pltpu.VMEM((1, D), F32), pltpu.SemaphoreType.DMA],
+        flops=10**9,
+        in_specs=[VMEM_SPEC] * 3 + [HBM_SPEC] + [VMEM_SPEC] * 2,
+        out_specs=VMEM_SPEC,
     )(ctx_mine, ctx_theirs, mod, gain, w_key, w_value)
-    ctx_all = exchange(ctx_kv, "y")
-
-    q, head, tail, gate = call(
-        qkv_body,
+    ctx_all = exchange(ctx_kv, ("zl", "y"))
+
+    head, tail, gate, xn = call(
+        kv_body,
         (
-            shape((256, 256), BF),
             shape((2, 128, 256), BF),
             shape((2, 128, 256), BF),
             shape((1, D), F32),
+            shape((256, D), BF),
         ),
-        [pltpu.VMEM((256, D), BF), pltpu.VMEM((D, 256), BF), pltpu.SemaphoreType.DMA],
+        [pltpu.VMEM((2, 4, 32, D), BF), pltpu.VMEM((1, D), F32), pltpu.SemaphoreType.DMA((3,))],
         flops=2 * 10**9,
-        in_specs=[VMEM_SPEC] * 4 + [HBM_SPEC] + [VMEM_SPEC] * 2,
+        in_specs=[HBM_SPEC] * 2 + [VMEM_SPEC, HBM_SPEC] + [VMEM_SPEC] * 2,
         out_specs=[VMEM_SPEC] * 4,
         vmem=16 << 20,
-    )(lat_mine, lat_theirs, mod, gain, in_hbm(w_query), w_key, w_value)
+    )(in_hbm(lat_mine), in_hbm(lat_theirs), mod, gain, w_key, w_value)
+    q = call(query_body, shape((256, 256), BF), flops=10**9)(xn, w_query)
     prev = lax.ppermute(tail, SP, [(i, i + 1) for i in range(63)])
     nxt = lax.ppermute(head, SP, [(i + 1, i) for i in range(63)])
     bias = call(
@@ -387,28 +411,28 @@
         [pltpu.VMEM((15, 4, 32, 128), F32)],
         flops=10**8,
     )(table)
-    att, away = call(
+    att, away, w_near = call(
         attend_body,
-        (shape((128, 256), BF), shape((128, 256), BF)),
+        (shape((128, 256), BF), shape((128, 256), BF), shape((2, 256, D), BF)),
         [
             pltpu.VMEM((256, 256), BF),
             pltpu.VMEM((2, 2, 128, 256), BF),
             pltpu.VMEM((2, 2, 3, 128, 128), F32),
-            pltpu.SemaphoreType.DMA((4,)),
+            pltpu.SemaphoreType.DMA((6,)),
         ],
         flops=10**9,
-        in_specs=[HBM_SPEC, VMEM_SPEC, HBM_SPEC, HBM_SPEC, VMEM_SPEC, HBM_SPEC, VMEM_SPEC],
-        out_specs=[VMEM_SPEC] * 2,
-    )(in_hbm(q), prev, in_hbm(head), in_hbm(tail), nxt, in_hbm(bias), ctx_all)
+        in_specs=[HBM_SPEC, VMEM_SPEC, HBM_SPEC, HBM_SPEC, VMEM_SPEC, HBM_SPEC, VMEM_SPEC, HBM_SPEC, HBM_SPEC],
+        out_specs=[VMEM_SPEC] * 3,
+    )(in_hbm(q), prev, in_hbm(head), in_hbm(tail), nxt, in_hbm(bias), ctx_all, in_hbm(w_out), in_hbm(w_pair))
     other = lax.ppermute(away, "c", SWAP)
-    own = call(out_own_body, shape((128, D), F32), flops=10**9)(att, w_out)
-    parts = call(out_proj_body, shape((4, 32, D), BF), flops=10**9)(own, other, w_pair)
+    own = call(out_own_body, shape((128, D), F32), flops=10**9)(att, w_near)
+    parts = call(out_proj_body, shape((4, 32, D), BF), flops=10**9)(own, other, w_near)
     arrived = exchange(parts, "x")
     return call(final_body, shape((32, D), BF))(arrived, latent, gate)
 
 
 def solution(mesh):
-    torus = Mesh(mesh.devices.reshape(16, 4, 4, 2), ALL)
+    torus = Mesh(mesh.devices.reshape(8, 2, 4, 4, 2), ALL)
     return jax.shard_map(
         on_device,
         mesh=torus,

time: 117 us -> 119 us (1.017)
  the two profiles are of different devices: /device:TPU:32 before, /device:TPU:1 now
where the time goes in v4:
time: 119 us; the launch traced here: 116 us
  blocking collectives  57.2 us (48%)
  starting transfers between devices  33.9 us (28%)
  Pallas kernels  11.3 us (9%)
  waiting for transfers between devices  10.2 us (9%)
  local copies, waits for them, and re-layouts  3.37 us (3%)
    all_to_all x4, blocking collectives, exchange(): return lax.all_to_all(blocks, axes, 0, 0, tiled=True)  57.2 us
    ppermute x3, starting transfers between devices, along_x(): parts.append(lax.ppermute(own, 'x', [(i, (i + d) % 4) for i in range(4)]))  7.81 us
    ppermute x1, starting transfers between devices, on_device(): ctx_theirs = lax.ppermute(ctx_mine, 'c', SWAP)  7.09 us
    ppermute x3, waiting for transfers between devices, along_x(): parts.append(lax.ppermute(own, 'x', [(i, (i + d) % 4) for i in range(4)]))  5.66 us
    ppermute x1, starting transfers between devices, on_device(): w_pair = lax.ppermute(w_out, 'c', SWAP)  3.72 us
    all_to_all x1, starting transfers between devices, exchange(): return lax.all_to_all(blocks, axes, 0, 0, tiled=True)  3.57 us
    ppermute x1, starting transfers between devices, on_device(): prev = lax.ppermute(tail, SP, [(i, i + 1) for i in range(63)])  3.54 us
    ppermute x1, starting transfers between devices, on_device(): lat_theirs = lax.ppermute(lat_mine, 'c', SWAP)  3.47 us
  transfers between devices with their start and end apart: 10, of which 6 were waited for; matrix products, arithmetic and copies ran while one was open for 0% of the time, Pallas kernels for 3%

profile of v4, /device:TPU:1, one launch (start us, length us, event | category | flops | bytes accessed | tf_op | source)
XLA Modules:
  0.0 116.2 jit_solution(1212844447552950712)
XLA Ops:
  0.0 1.2 shard_map.128
  1.2 27.5 %all_to_all.25.in_ref = bf16[16,16,256]{2,1,0:T(8,128)(2,1)S(1)} all-to-all(bf16[16,16,256]{2,1,0:T(8,128)(2,1)S(1)} %shard_map.128), channel_id=1, replica_groups=mesh['zh'=8,'zl'=2,'y'=4,'x'=4,'c'=2] {'zh','zl'}, dimensions={0} | all-to-all | bytes 262144 | tf_op jit(solution)/shard_map/all_to_all | solution.py:328
  28.7 9.4 %all_to_all.26.mine_ref = bf16[4,136,256]{2,1,0:T(8,128)(2,1)S(1)} all-to-all(bf16[4,136,256]{2,1,0:T(8,128)(2,1)S(1)} %shard_map.129), channel_id=1, replica_groups=mesh['zh'=8,'zl'=2,'y'=4,'x'=4,'c'=2] {'x'}, dimensions={0} | all-to-all | bytes 557056 | tf_op jit(solution)/shard_map/all_to_all | solution.py:328
  38.1 7.1 %collective-permute-start.4 = (bf16[4,136,256]{2,1,0:T(8,128)(2,1)S(1)}, bf16[4,136,256]{2,1,0:T(8,128)(2,1)S(1)}, u32[]{:S(2)}, u32[]{:S(2)}) collective-permute-start(bf16[4,136,256]{2,1,0:T(8,128)(2,1)S(1)} %all_to_all.26.mine_ref), channel_id=1, source_target_pairs={{0,1},{1,0},{2,3},{3,2},{4,5},{5,4},{6,7},{7,6},{8,9},{9,8},{10,11... | collective-permute-start | bytes 835592 | tf_op jit(solution)/shard_map/ppermute | solution.py:378
  45.2 1.2 %collective-permute-done.4.theirs_ref = bf16[4,136,256]{2,1,0:T(8,128)(2,1)S(1)} collective-permute-done((bf16[4,136,256]{2,1,0:T(8,128)(2,1)S(1)}, bf16[4,136,256]{2,1,0:T(8,128)(2,1)S(1)}, u32[]{:S(2)}, u32[]{:S(2)}) %collective-permute-start.4) | collective-permute-done | bytes 278560 | tf_op jit(solution)/shard_map/ppermute | solution.py:378
  46.4 8.8 %all_to_all.27.mod_ref = bf16[4,8,2048]{2,1,0:T(8,128)(2,1)S(1)} all-to-all(bf16[4,8,2048]{2,1,0:T(8,128)(2,1)S(1)} %shard_map.130), channel_id=1, replica_groups=mesh['zh'=8,'zl'=2,'y'=4,'x'=4,'c'=2] {'y'}, dimensions={0} | all-to-all | bytes 262144 | tf_op jit(solution)/shard_map/all_to_all | solution.py:328
  55.2 2.4 %shard_map.135 = bf16[8,2,128,256]{3,2,1,0:T(8,128)(2,1)} custom-call(bf16[4,136,256]{2,1,0:T(8,128)(2,1)S(1)} %all_to_all.26.mine_ref, bf16[4,136,256]{2,1,0:T(8,128)(2,1)S(1)} %collective-permute-done.4.theirs_ref, bf16[4,8,2048]{2,1,0:T(8,128)(2,1)S(1)} %all_to_all.27.mod_ref, f32[1,2048]{1,0:T(1,128)} %bitcast.3, bf16[2048,256]{1,0:T(8,128)(2,1)S(1)} %copy-done.1, ...), custom_call_target="tpu_custom_call" | custom-call | flops 1000000000 | tf_op jit(solution)/shard_map/pallas_call | solution.py:381
  57.7 3.6 %all-to-all-start.3 = ((bf16[8,2,128,256]{3,2,1,0:T(8,128)(2,1)}), bf16[8,2,128,256]{3,2,1,0:T(8,128)(2,1)S(1)}, u32[]{:S(2)}, u32[]{:S(2)}) async-start(bf16[8,2,128,256]{3,2,1,0:T(8,128)(2,1)} %shard_map.135), calls=%async_computation.3 | async-start | bytes 2097152 | tf_op jit(solution)/shard_map/all_to_all | solution.py:328
  61.2 3.7 %collective-permute-start.7 = (bf16[256,2048]{1,0:T(8,128)(2,1)}, bf16[256,2048]{1,0:T(8,128)(2,1)S(1)}, u32[]{:S(2)}, u32[]{:S(2)}) collective-permute-start(bf16[256,2048]{1,0:T(8,128)(2,1)} %w_hbm.1), channel_id=1, source_target_pairs={{0,1},{1,0},{2,3},{3,2},{4,5},{5,4},{6,7},{7,6},{8,9},{9,8},{10,11... | collective-permute-start | bytes 3145736 | tf_op jit(solution)/shard_map/ppermute | solution.py:373
  65.0 2.8 %collective-permute-start.2 = (bf16[32,2048]{1,0:T(8,128)(2,1)S(1)}, bf16[32,2048]{1,0:T(8,128)(2,1)S(1)}, u32[]{:S(2)}, u32[]{:S(2)}) collective-permute-start(bf16[32,2048]{1,0:T(8,128)(2,1)S(1)} %copy-done.4), channel_id=1, source_target_pairs={{0,6},{2,0},{4,2},{6,4},{1,7},{3,1},{5,3},{7,5},{8,14},{10,8},{12,... | collective-permute-start | bytes 393224 | tf_op jit(solution)/shard_map/ppermute | solution.py:337
  67.8 3.1 %collective-permute-start.1 = (bf16[32,2048]{1,0:T(8,128)(2,1)S(1)}, bf16[32,2048]{1,0:T(8,128)(2,1)S(1)}, u32[]{:S(2)}, u32[]{:S(2)}) collective-permute-start(bf16[32,2048]{1,0:T(8,128)(2,1)S(1)} %copy-done.4), channel_id=1, source_target_pairs={{0,4},{2,6},{4,0},{6,2},{1,5},{3,7},{5,1},{7,3},{8,12},{10,14},{12... | collective-permute-start | bytes 393224 | tf_op jit(solution)/shard_map/ppermute | solution.py:337
  70.9 1.9 %collective-permute-start = (bf16[32,2048]{1,0:T(8,128)(2,1)S(1)}, bf16[32,2048]{1,0:T(8,128)(2,1)S(1)}, u32[]{:S(2)}, u32[]{:S(2)}) collective-permute-start(bf16[32,2048]{1,0:T(8,128)(2,1)S(1)} %copy-done.4), channel_id=1, source_target_pairs={{0,2},{2,4},{4,6},{6,0},{1,3},{3,5},{5,7},{7,1},{8,10},{10,12},{12... | collective-permute-start | bytes 393224 | tf_op jit(solution)/shard_map/ppermute | solution.py:337
  72.8 3.1 %collective-permute-done.1.p2_ref = bf16[32,2048]{1,0:T(8,128)(2,1)S(1)} collective-permute-done((bf16[32,2048]{1,0:T(8,128)(2,1)S(1)}, bf16[32,2048]{1,0:T(8,128)(2,1)S(1)}, u32[]{:S(2)}, u32[]{:S(2)}) %collective-permute-start.1) | collective-permute-done | bytes 131104 | tf_op jit(solution)/shard_map/ppermute | solution.py:337
  75.9 2.5 %collective-permute-done.p1_ref = bf16[32,2048]{1,0:T(8,128)(2,1)S(1)} collective-permute-done((bf16[32,2048]{1,0:T(8,128)(2,1)S(1)}, bf16[32,2048]{1,0:T(8,128)(2,1)S(1)}, u32[]{:S(2)}, u32[]{:S(2)}) %collective-permute-start) | collective-permute-done | bytes 131104 | tf_op jit(solution)/shard_map/ppermute | solution.py:337
  78.6 3.5 %collective-permute-start.3 = (bf16[4,32,2048]{2,1,0:T(8,128)(2,1)S(1)}, bf16[4,32,2048]{2,1,0:T(8,128)(2,1)S(1)}, u32[]{:S(2)}, u32[]{:S(2)}) collective-permute-start(bf16[4,32,2048]{2,1,0:T(8,128)(2,1)S(1)} %shard_map.127.mine_hbm), channel_id=1, source_target_pairs={{0,1},{1,0},{2,3},{3,2},{4,5},{5,4},{6,7},{7,6},{8,9},{9,8},{10,11... | collective-permute-start | bytes 1572872 | tf_op jit(solution)/shard_map/ppermute | solution.py:377
  82.0 1.5 %collective-permute-done.3.theirs_hbm = bf16[4,32,2048]{2,1,0:T(8,128)(2,1)S(1)} collective-permute-done((bf16[4,32,2048]{2,1,0:T(8,128)(2,1)S(1)}, bf16[4,32,2048]{2,1,0:T(8,128)(2,1)S(1)}, u32[]{:S(2)}, u32[]{:S(2)}) %collective-permute-start.3) | collective-permute-done | bytes 524320 | tf_op jit(solution)/shard_map/ppermute | solution.py:377
  84.4 2.2 %shard_map.131 = (bf16[2,128,256]{2,1,0:T(8,128)(2,1)S(1)}, bf16[2,128,256]{2,1,0:T(8,128)(2,1)S(1)}, f32[1,2048]{1,0:T(1,128)S(1)}, bf16[256,2048]{1,0:T(8,128)(2,1)S(1)}) custom-call(bf16[4,32,2048]{2,1,0:T(8,128)(2,1)} %copy-done.3, bf16[4,32,2048]{2,1,0:T(8,128)(2,1)} %copy-done.11, bf16[4,8,2048]{2,1,0:T(8,128)(2,1)S(1)} %all_to_all.27.mod_ref, ...), custom_call_target="tpu_custom_call" | custom-call | flops 2000000000 | tf_op jit(solution)/shard_map/pallas_call | solution.py:391
  86.6 3.5 %collective-permute-start.5 = (bf16[2,128,256]{2,1,0:T(8,128)(2,1)S(1)}, bf16[2,128,256]{2,1,0:T(8,128)(2,1)S(1)}, u32[]{:S(2)}, u32[]{:S(2)}) collective-permute-start(bf16[2,128,256]{2,1,0:T(8,128)(2,1)S(1)} %get-tuple-element.13.tail_hbm), channel_id=1, source_target_pairs={{0,8},{8,16},{16,24},{24,32},{32,40},{40,48},{48,56},{56,64},{64,7... | collective-permute-start | bytes 393224 | tf_op jit(solution)/shard_map/ppermute | solution.py:406
  90.2 1.3 %collective-permute-start.6 = (bf16[2,128,256]{2,1,0:T(8,128)(2,1)S(1)}, bf16[2,128,256]{2,1,0:T(8,128)(2,1)S(1)}, u32[]{:S(2)}, u32[]{:S(2)}) collective-permute-start(bf16[2,128,256]{2,1,0:T(8,128)(2,1)S(1)} %get-tuple-element.14.head_hbm), channel_id=1, source_target_pairs={{8,0},{16,8},{24,16},{32,24},{40,32},{48,40},{56,48},{64,56},{72,6... | collective-permute-start | bytes 393224 | tf_op jit(solution)/shard_map/ppermute | solution.py:407
  94.2 1.0 copy-done.9
  95.1 1.3 %collective-permute-done.6.next_ref = bf16[2,128,256]{2,1,0:T(8,128)(2,1)S(1)} collective-permute-done((bf16[2,128,256]{2,1,0:T(8,128)(2,1)S(1)}, bf16[2,128,256]{2,1,0:T(8,128)(2,1)S(1)}, u32[]{:S(2)}, u32[]{:S(2)}) %collective-permute-start.6) | collective-permute-done | bytes 131104 | tf_op jit(solution)/shard_map/ppermute | solution.py:407
  96.5 2.9 %shard_map.136 = (bf16[128,256]{1,0:T(8,128)(2,1)S(1)}, bf16[128,256]{1,0:T(8,128)(2,1)S(1)}, bf16[2,256,2048]{2,1,0:T(8,128)(2,1)S(1)}) custom-call(bf16[256,256]{1,0:T(8,128)(2,1)} %copy-done.7, bf16[2,128,256]{2,1,0:T(8,128)(2,1)S(1)} %collective-permute-done.5.prev_ref, bf16[2,128,256]{2,1,0:T(8,128)(2,1)} %copy-done.5, bf16[2,128,256]{2,1,0:T(8,128)(2,1)} %copy-done.6, ...), custom_call_target="tpu_custom_call" | custom-call | flops 1000000000 | tf_op jit(solution)/shard_map/pallas_call | solution.py:414
  99.4 3.4 %collective-permute-start.8 = (bf16[128,256]{1,0:T(8,128)(2,1)S(1)}, bf16[128,256]{1,0:T(8,128)(2,1)S(1)}, u32[]{:S(2)}, u32[]{:S(2)}) collective-permute-start(bf16[128,256]{1,0:T(8,128)(2,1)S(1)} %get-tuple-element.17), channel_id=1, source_target_pairs={{0,1},{1,0},{2,3},{3,2},{4,5},{5,4},{6,7},{7,6},{8,9},{9,8},{10,11... | collective-permute-start | bytes 196616 | tf_op jit(solution)/shard_map/ppermute | solution.py:427
  104.0 11.4 %all_to_all.28.parts_ref = bf16[4,32,2048]{2,1,0:T(8,128)(2,1)S(1)} all-to-all(bf16[4,32,2048]{2,1,0:T(8,128)(2,1)S(1)} %shard_map.138), channel_id=1, replica_groups=mesh['zh'=8,'zl'=2,'y'=4,'x'=4,'c'=2] {'x'}, dimensions={0} | all-to-all | bytes 1048576 | tf_op jit(solution)/shard_map/all_to_all | solution.py:328
  (38 shorter events, 5.5 us)
Async XLA Ops:
  0.0 55.2 %copy-start.2 = (bf16[2048,256]{1,0:T(8,128)(2,1)S(1)}, bf16[2048,256]{1,0:T(8,128)(2,1)}, u32[]{:S(2)}) copy-start(bf16[2048,256]{1,0:T(8,128)(2,1)} %wv_ref.3) | copy-start | bytes 3145732
  0.0 55.2 %copy-start.1 = (bf16[2048,256]{1,0:T(8,128)(2,1)S(1)}, bf16[2048,256]{1,0:T(8,128)(2,1)}, u32[]{:S(2)}) copy-start(bf16[2048,256]{1,0:T(8,128)(2,1)} %wk_ref.3) | copy-start | bytes 3145732
  38.1 8.3 %collective-permute-start.4 = (bf16[4,136,256]{2,1,0:T(8,128)(2,1)S(1)}, bf16[4,136,256]{2,1,0:T(8,128)(2,1)S(1)}, u32[]{:S(2)}, u32[]{:S(2)}) collective-permute-start(bf16[4,136,256]{2,1,0:T(8,128)(2,1)S(1)} %all_to_all.26.mine_ref), channel_id=1, source_target_pairs={{0,1},{1,0},{2,3},{3,2},{4,5},{5,4},{6,7},{7,6},{8,9},{9,8},{10,11... | collective-permute-start | bytes 835592 | tf_op jit(solution)/shard_map/ppermute | solution.py:378
  55.2 9.7 %copy-start.4 = (bf16[32,2048]{1,0:T(8,128)(2,1)S(1)}, bf16[32,2048]{1,0:T(8,128)(2,1)}, u32[]{:S(2)}) copy-start(bf16[32,2048]{1,0:T(8,128)(2,1)} %lat_ref.1) | copy-start | bytes 393220
  57.7 38.8 %all-to-all-start.3 = ((bf16[8,2,128,256]{3,2,1,0:T(8,128)(2,1)}), bf16[8,2,128,256]{3,2,1,0:T(8,128)(2,1)S(1)}, u32[]{:S(2)}, u32[]{:S(2)}) async-start(bf16[8,2,128,256]{3,2,1,0:T(8,128)(2,1)} %shard_map.135), calls=%async_computation.3 | async-start | bytes 2097152 | tf_op jit(solution)/shard_map/all_to_all | solution.py:328
  61.2 32.9 %collective-permute-start.7 = (bf16[256,2048]{1,0:T(8,128)(2,1)}, bf16[256,2048]{1,0:T(8,128)(2,1)S(1)}, u32[]{:S(2)}, u32[]{:S(2)}) collective-permute-start(bf16[256,2048]{1,0:T(8,128)(2,1)} %w_hbm.1), channel_id=1, source_target_pairs={{0,1},{1,0},{2,3},{3,2},{4,5},{5,4},{6,7},{7,6},{8,9},{9,8},{10,11... | collective-permute-start | bytes 3145736 | tf_op jit(solution)/shard_map/ppermute | solution.py:373
  65.0 7.8 %collective-permute-start.2 = (bf16[32,2048]{1,0:T(8,128)(2,1)S(1)}, bf16[32,2048]{1,0:T(8,128)(2,1)S(1)}, u32[]{:S(2)}, u32[]{:S(2)}) collective-permute-start(bf16[32,2048]{1,0:T(8,128)(2,1)S(1)} %copy-done.4), channel_id=1, source_target_pairs={{0,6},{2,0},{4,2},{6,4},{1,7},{3,1},{5,3},{7,5},{8,14},{10,8},{12,... | collective-permute-start | bytes 393224 | tf_op jit(solution)/shard_map/ppermute | solution.py:337
  67.8 8.2 %collective-permute-start.1 = (bf16[32,2048]{1,0:T(8,128)(2,1)S(1)}, bf16[32,2048]{1,0:T(8,128)(2,1)S(1)}, u32[]{:S(2)}, u32[]{:S(2)}) collective-permute-start(bf16[32,2048]{1,0:T(8,128)(2,1)S(1)} %copy-done.4), channel_id=1, source_target_pairs={{0,4},{2,6},{4,0},{6,2},{1,5},{3,7},{5,1},{7,3},{8,12},{10,14},{12... | collective-permute-start | bytes 393224 | tf_op jit(solution)/shard_map/ppermute | solution.py:337
  70.9 7.6 %collective-permute-start = (bf16[32,2048]{1,0:T(8,128)(2,1)S(1)}, bf16[32,2048]{1,0:T(8,128)(2,1)S(1)}, u32[]{:S(2)}, u32[]{:S(2)}) collective-permute-start(bf16[32,2048]{1,0:T(8,128)(2,1)S(1)} %copy-done.4), channel_id=1, source_target_pairs={{0,2},{2,4},{4,6},{6,0},{1,3},{3,5},{5,7},{7,1},{8,10},{10,12},{12... | collective-permute-start | bytes 393224 | tf_op jit(solution)/shard_map/ppermute | solution.py:337
  78.5 5.0 %copy-start.3 = (bf16[4,32,2048]{2,1,0:T(8,128)(2,1)}, bf16[4,32,2048]{2,1,0:T(8,128)(2,1)S(1)}, u32[]{:S(2)}) copy-start(bf16[4,32,2048]{2,1,0:T(8,128)(2,1)S(1)} %shard_map.127.mine_hbm) | copy-start | bytes 1572868
  78.5 12.9 %copy-start.10 = (f32[16,15,31]{2,0,1:T(8,128)S(1)}, f32[16,15,31]{2,0,1:T(8,128)}, u32[]{:S(2)}) copy-start(f32[16,15,31]{2,0,1:T(8,128)} %param.25) | copy-start | bytes 89284
  78.6 14.5 %copy-start.8 = (bf16[2048,256]{1,0:T(8,128)(2,1)S(1)}, bf16[2048,256]{1,0:T(8,128)(2,1)}, u32[]{:S(2)}) copy-start(bf16[2048,256]{1,0:T(8,128)(2,1)} %wq_ref.1) | copy-start | bytes 3145732
  78.6 5.0 %collective-permute-start.3 = (bf16[4,32,2048]{2,1,0:T(8,128)(2,1)S(1)}, bf16[4,32,2048]{2,1,0:T(8,128)(2,1)S(1)}, u32[]{:S(2)}, u32[]{:S(2)}) collective-permute-start(bf16[4,32,2048]{2,1,0:T(8,128)(2,1)S(1)} %shard_map.127.mine_hbm), channel_id=1, source_target_pairs={{0,1},{1,0},{2,3},{3,2},{4,5},{5,4},{6,7},{7,6},{8,9},{9,8},{10,11... | collective-permute-start | bytes 1572872 | tf_op jit(solution)/shard_map/ppermute | solution.py:377
  83.6 0.8 copy-start.11
  86.6 6.9 %copy-start.5 = (bf16[2,128,256]{2,1,0:T(8,128)(2,1)}, bf16[2,128,256]{2,1,0:T(8,128)(2,1)S(1)}, u32[]{:S(2)}) copy-start(bf16[2,128,256]{2,1,0:T(8,128)(2,1)S(1)} %get-tuple-element.14.head_hbm) | copy-start | bytes 393220
  86.6 6.9 %copy-start.6 = (bf16[2,128,256]{2,1,0:T(8,128)(2,1)}, bf16[2,128,256]{2,1,0:T(8,128)(2,1)S(1)}, u32[]{:S(2)}) copy-start(bf16[2,128,256]{2,1,0:T(8,128)(2,1)S(1)} %get-tuple-element.13.tail_hbm) | copy-start | bytes 393220
  86.6 7.6 %collective-permute-start.5 = (bf16[2,128,256]{2,1,0:T(8,128)(2,1)S(1)}, bf16[2,128,256]{2,1,0:T(8,128)(2,1)S(1)}, u32[]{:S(2)}, u32[]{:S(2)}) collective-permute-start(bf16[2,128,256]{2,1,0:T(8,128)(2,1)S(1)} %get-tuple-element.13.tail_hbm), channel_id=1, source_target_pairs={{0,8},{8,16},{16,24},{24,32},{32,40},{40,48},{48,56},{56,64},{64,7... | collective-permute-start | bytes 393224 | tf_op jit(solution)/shard_map/ppermute | solution.py:406
  90.2 6.3 %collective-permute-start.6 = (bf16[2,128,256]{2,1,0:T(8,128)(2,1)S(1)}, bf16[2,128,256]{2,1,0:T(8,128)(2,1)S(1)}, u32[]{:S(2)}, u32[]{:S(2)}) collective-permute-start(bf16[2,128,256]{2,1,0:T(8,128)(2,1)S(1)} %get-tuple-element.14.head_hbm), channel_id=1, source_target_pairs={{8,0},{16,8},{24,16},{32,24},{40,32},{48,40},{56,48},{64,56},{72,6... | collective-permute-start | bytes 393224 | tf_op jit(solution)/shard_map/ppermute | solution.py:407
  92.2 0.9 copy-start
  93.5 0.7 copy-start.7
  94.2 1.0 copy-start.9
  99.4 4.3 %collective-permute-start.8 = (bf16[128,256]{1,0:T(8,128)(2,1)S(1)}, bf16[128,256]{1,0:T(8,128)(2,1)S(1)}, u32[]{:S(2)}, u32[]{:S(2)}) collective-permute-start(bf16[128,256]{1,0:T(8,128)(2,1)S(1)} %get-tuple-element.17), channel_id=1, source_target_pairs={{0,1},{1,0},{2,3},{3,2},{4,5},{5,4},{6,7},{7,6},{8,9},{9,8},{10,11... | collective-permute-start | bytes 196616 | tf_op jit(solution)/shard_map/ppermute | solution.py:427

commit v5 on v4

--- a/solution.py
+++ b/solution.py
@@ -135,17 +135,24 @@
         out_ref[lax.rem(x - d + 4, 4)] = ref[...]
 
 
-def ctx_kv_body(mine_ref, theirs_ref, mod_ref, gain_hbm, wk_ref, wv_ref, out_ref, xn_ref, gain_ref, sem):
+def ctx_pre_body(mine_ref, gain_hbm, gain_ref, square_ref, sem):
     copy = pltpu.make_async_copy(gain_hbm, gain_ref, sem)
     copy.start()
+    square = jnp.zeros((128, 256), F32)
+    for j in range(4):
+        x = mine_ref[j, 0:128].astype(F32)
+        square = square + x * x
+    square_ref[...] = square
+    copy.wait()
+
+
+def ctx_kv_body(mine_ref, theirs_ref, square_ref, mod_ref, gain_ref, wk_ref, wv_ref, out_ref, xn_ref):
     core = lax.axis_index("c")
-    square = jnp.zeros((128, 256), F32)
-    for ref in (mine_ref, theirs_ref):
-        for j in range(4):
-            x = ref[j, 0:128].astype(F32)
-            square = square + x * x
+    square = square_ref[...]
+    for j in range(4):
+        x = theirs_ref[j, 0:128].astype(F32)
+        square = square + x * x
     inv = lax.rsqrt(jnp.sum(square, axis=-1, keepdims=True) * (1.0 / D) + NORM_EPS)
-    copy.wait()
     for ref, c in ((mine_ref, core), (theirs_ref, 1 - core)):
         for j in range(4):
             cols = column_block(j, c)
@@ -169,7 +176,7 @@
 
 def kv_body(
     mine_hbm, theirs_hbm, mod_ref, gain_hbm, wk_ref, wv_ref,
-    head_ref, tail_ref, gate_ref, xn_ref, lat_ref, gain_ref, sems,
+    head_ref, tail_ref, start_ref, gate_ref, xn_ref, lat_ref, gain_ref, sems,
 ):
     copies = [
         pltpu.make_async_copy(src, lat_ref.at[i], sems.at[i])
@@ -194,6 +201,7 @@
         res = jnp.dot(xn, w_ref[...], preferred_element_type=F32).astype(BF)
         head_ref[i] = res[:128]
         tail_ref[i] = res[128:]
+        start_ref[i] = res[:96]
 
 
 def query_body(xn_ref, wq_ref, q_ref):
@@ -235,7 +243,7 @@
 
 
 def attend_body(
-    q_hbm, prev_ref, head_hbm, tail_hbm, next_ref, bias_hbm, ctx_ref, w_hbm, wp_hbm,
+    q_hbm, prev_ref, head_hbm, tail_hbm, next_ref, bias_hbm, ctx_ref, w_hbm,
     mine_ref, other_ref, w_ref, q_ref, kv_ref, bias_ref, sems,
 ):
     copies = [
@@ -246,39 +254,52 @@
                 (head_hbm, kv_ref.at[0]),
                 (tail_hbm, kv_ref.at[1]),
                 (bias_hbm, bias_ref),
-                (w_hbm, w_ref.at[0]),
-                (wp_hbm, w_ref.at[1]),
+                (w_hbm, w_ref),
             )
         )
     ]
     for copy in copies:
         copy.start()
-    segs = (prev_ref, kv_ref.at[0], kv_ref.at[1], next_ref)
+
+    def seg(index, kind, hc):
+        if index == 3:
+            return jnp.concatenate([next_ref[kind, :, hc], jnp.zeros((32, 128), BF)], axis=0)
+        return (prev_ref, kv_ref.at[0], kv_ref.at[1])[index][kind, :, hc]
+
     core = lax.axis_index("c")
     nt = (((1,), (1,)), ((), ()))
     copies[0].wait()
-    for h in range(2):
-        hc = slice(h * 128, (h + 1) * 128)
-        kc = ctx_ref[:, 0, :, hc].reshape(1024, 128)
-        vc = ctx_ref[:, 1, :, hc].reshape(1024, 128)
-        s_ctx = lax.dot_general(q_ref[:, hc], kc, nt, preferred_element_type=F32)
-        if h == 0:
-            for copy in copies[1:4]:
-                copy.wait()
-        s_win = [
-            [
-                lax.dot_general(
-                    q_ref[half * 128 : (half + 1) * 128, hc],
-                    segs[half + s][0, :, hc],
-                    nt,
-                    preferred_element_type=F32,
-                )
-                + bias_ref[h, half, s]
-                for half in range(2)
-            ]
+    heads = [slice(h * 128, (h + 1) * 128) for h in range(2)]
+    scores_ctx = [
+        lax.dot_general(
+            q_ref[:, hc], ctx_ref[:, 0, :, hc].reshape(1024, 128), nt, preferred_element_type=F32
+        )
+        for hc in heads
+    ]
+    for copy in copies[1:4]:
+        copy.wait()
+    scores_win = [
+        [
+            jnp.concatenate(
+                [
+                    lax.dot_general(
+                        q_ref[half * 128 : (half + 1) * 128, hc],
+                        seg(half + s, 0, hc),
+                        nt,
+                        preferred_element_type=F32,
+                    )
+                    + bias_ref[h, half, s]
+                    for half in range(2)
+                ],
+                axis=0,
+            )
             for s in range(3)
         ]
-        s_win = [jnp.concatenate(pair, axis=0) for pair in s_win]
+        for h, hc in enumerate(heads)
+    ]
+    for h, hc in enumerate(heads):
+        vc = ctx_ref[:, 1, :, hc].reshape(1024, 128)
+        s_ctx, s_win = scores_ctx[h], scores_win[h]
         peak = jnp.maximum(jnp.maximum(s_win[0], s_win[1]), s_win[2])
         for i in range(8):
             peak = jnp.maximum(peak, s_ctx[:, i * 128 : (i + 1) * 128])
@@ -296,7 +317,7 @@
             for s in range(3):
                 acc_half = acc_half + jnp.dot(
                     e_win[s][rows].astype(BF),
-                    segs[half + s][1, :, hc],
+                    seg(half + s, 1, hc),
                     preferred_element_type=F32,
                 )
             out = (acc_half / total[rows]).astype(BF)
@@ -311,11 +332,11 @@
 
 
 def out_own_body(mine_ref, w_ref, out_ref):
-    out_ref[...] = jnp.dot(mine_ref[...], w_ref[0], preferred_element_type=F32)
+    out_ref[...] = jnp.dot(mine_ref[...], w_ref[...], preferred_element_type=F32)
 
 
 def out_proj_body(own_ref, got_ref, w_ref, out_ref):
-    res = own_ref[...] + jnp.dot(got_ref[...], w_ref[1], preferred_element_type=F32)
+    res = own_ref[...] + jnp.dot(got_ref[...], w_ref[...], preferred_element_type=F32)
     out_ref[...] = res.astype(BF).reshape(4, 32, D)
 
 
@@ -376,35 +397,39 @@
     lat_mine = call(gather_x_body, shape((4, 32, D), BF), flops=10**8)(*lat_parts)
     lat_theirs = lax.ppermute(lat_mine, "c", SWAP)
     ctx_theirs = lax.ppermute(ctx_mine, "c", SWAP)
+    gain_near, square = call(
+        ctx_pre_body,
+        (shape((1, D), F32), shape((128, 256), F32)),
+        [pltpu.SemaphoreType.DMA],
+        flops=10**8,
+        in_specs=[VMEM_SPEC, HBM_SPEC],
+        out_specs=[VMEM_SPEC] * 2,
+    )(ctx_mine, gain)
     mod_own = call(relay_mod_body, shape((4, 8, D), BF), flops=10**7)(ctx_mine, ctx_theirs)
     mod = exchange(mod_own, "y")
     ctx_kv = call(
-        ctx_kv_body,
-        shape((8, 2, 128, 256), BF),
-        [pltpu.VMEM((128, D), BF), pltpu.VMEM((1, D), F32), pltpu.SemaphoreType.DMA],
-        flops=10**9,
-        in_specs=[VMEM_SPEC] * 3 + [HBM_SPEC] + [VMEM_SPEC] * 2,
-        out_specs=VMEM_SPEC,
-    )(ctx_mine, ctx_theirs, mod, gain, w_key, w_value)
+        ctx_kv_body, shape((8, 2, 128, 256), BF), [pltpu.VMEM((128, D), BF)], flops=10**9
+    )(ctx_mine, ctx_theirs, square, mod, gain_near, w_key, w_value)
     ctx_all = exchange(ctx_kv, ("zl", "y"))
 
-    head, tail, gate, xn = call(
+    head, tail, start, gate, xn = call(
         kv_body,
         (
             shape((2, 128, 256), BF),
             shape((2, 128, 256), BF),
+            shape((2, 96, 256), BF),
             shape((1, D), F32),
             shape((256, D), BF),
         ),
         [pltpu.VMEM((2, 4, 32, D), BF), pltpu.VMEM((1, D), F32), pltpu.SemaphoreType.DMA((3,))],
         flops=2 * 10**9,
         in_specs=[HBM_SPEC] * 2 + [VMEM_SPEC, HBM_SPEC] + [VMEM_SPEC] * 2,
-        out_specs=[VMEM_SPEC] * 4,
+        out_specs=[VMEM_SPEC] * 5,
         vmem=16 << 20,
     )(in_hbm(lat_mine), in_hbm(lat_theirs), mod, gain, w_key, w_value)
     q = call(query_body, shape((256, 256), BF), flops=10**9)(xn, w_query)
     prev = lax.ppermute(tail, SP, [(i, i + 1) for i in range(63)])
-    nxt = lax.ppermute(head, SP, [(i + 1, i) for i in range(63)])
+    nxt = lax.ppermute(start, SP, [(i + 1, i) for i in range(63)])
     bias = call(
         functools.partial(bias_body, 512),
         shape((2, 2, 3, 128, 128), F32),
@@ -413,20 +438,20 @@
     )(table)
     att, away, w_near = call(
         attend_body,
-        (shape((128, 256), BF), shape((128, 256), BF), shape((2, 256, D), BF)),
+        (shape((128, 256), BF), shape((128, 256), BF), shape((256, D), BF)),
         [
             pltpu.VMEM((256, 256), BF),
             pltpu.VMEM((2, 2, 128, 256), BF),
             pltpu.VMEM((2, 2, 3, 128, 128), F32),
-            pltpu.SemaphoreType.DMA((6,)),
+            pltpu.SemaphoreType.DMA((5,)),
         ],
         flops=10**9,
-        in_specs=[HBM_SPEC, VMEM_SPEC, HBM_SPEC, HBM_SPEC, VMEM_SPEC, HBM_SPEC, VMEM_SPEC, HBM_SPEC, HBM_SPEC],
+        in_specs=[HBM_SPEC, VMEM_SPEC, HBM_SPEC, HBM_SPEC, VMEM_SPEC, HBM_SPEC, VMEM_SPEC, HBM_SPEC],
         out_specs=[VMEM_SPEC] * 3,
-    )(in_hbm(q), prev, in_hbm(head), in_hbm(tail), nxt, in_hbm(bias), ctx_all, in_hbm(w_out), in_hbm(w_pair))
+    )(in_hbm(q), prev, in_hbm(head), in_hbm(tail), nxt, in_hbm(bias), ctx_all, in_hbm(w_out))
     other = lax.ppermute(away, "c", SWAP)
     own = call(out_own_body, shape((128, D), F32), flops=10**9)(att, w_near)
-    parts = call(out_proj_body, shape((4, 32, D), BF), flops=10**9)(own, other, w_near)
+    parts = call(out_proj_body, shape((4, 32, D), BF), flops=10**9)(own, other, w_pair)
     arrived = exchange(parts, "x")
     return call(final_body, shape((32, D), BF))(arrived, latent, gate)
 

time: 119 us -> 117 us (0.983)
  the two profiles are of different devices: /device:TPU:1 before, /device:TPU:24 now
where the time goes in v5:
time: 117 us; the launch traced here: 116 us
  blocking collectives  54 us (46%)
  starting transfers between devices  33.6 us (29%)
  waiting for transfers between devices  12.9 us (11%)
  Pallas kernels  12.5 us (11%)
  local copies, waits for them, and re-layouts  2.41 us (2%)
    all_to_all x3, blocking collectives, exchange(): return lax.all_to_all(blocks, axes, 0, 0, tiled=True)  54 us
    all_to_all x2, starting transfers between devices, exchange(): return lax.all_to_all(blocks, axes, 0, 0, tiled=True)  10.4 us
    ppermute x3, starting transfers between devices, along_x(): parts.append(lax.ppermute(own, 'x', [(i, (i + d) % 4) for i in range(4)]))  9.47 us
    ppermute x1, waiting for transfers between devices, on_device(): nxt = lax.ppermute(start, SP, [(i + 1, i) for i in range(63)])  3.53 us
    ppermute x1, starting transfers between devices, on_device(): prev = lax.ppermute(tail, SP, [(i, i + 1) for i in range(63)])  3.51 us
    all_to_all x2, waiting for transfers between devices, exchange(): return lax.all_to_all(blocks, axes, 0, 0, tiled=True)  3.2 us
    pallas_call x1, Pallas kernels, on_device(): call(attend_body, (shape((128, 256), BF), shape((128, 256), BF), shape((2...  2.54 us
    ppermute x1, starting transfers between devices, on_device(): nxt = lax.ppermute(start, SP, [(i + 1, i) for i in range(63)])  2.46 us
  transfers between devices with their start and end apart: 11, of which 6 were waited for; matrix products, arithmetic and copies ran while one was open for 0% of the time, Pallas kernels for 6%

profile of v5, /device:TPU:24, one launch (start us, length us, event | category | flops | bytes accessed | tf_op | source)
XLA Modules:
  0.0 115.8 jit_solution(4878799958992435748)
XLA Ops:
  0.0 1.0 shard_map.128
  1.0 29.8 %all_to_all.25.in_ref = bf16[16,16,256]{2,1,0:T(8,128)(2,1)S(1)} all-to-all(bf16[16,16,256]{2,1,0:T(8,128)(2,1)S(1)} %shard_map.128), channel_id=1, replica_groups=mesh['zh'=8,'zl'=2,'y'=4,'x'=4,'c'=2] {'zh','zl'}, dimensions={0} | all-to-all | bytes 262144 | tf_op jit(solution)/shard_map/all_to_all | solution.py:349
  30.8 11.0 %all_to_all.26.mine_ref = bf16[4,136,256]{2,1,0:T(8,128)(2,1)S(1)} all-to-all(bf16[4,136,256]{2,1,0:T(8,128)(2,1)S(1)} %shard_map.129), channel_id=1, replica_groups=mesh['zh'=8,'zl'=2,'y'=4,'x'=4,'c'=2] {'x'}, dimensions={0} | all-to-all | bytes 557056 | tf_op jit(solution)/shard_map/all_to_all | solution.py:349
  41.8 1.9 %collective-permute-start.4 = (bf16[4,136,256]{2,1,0:T(8,128)(2,1)S(1)}, bf16[4,136,256]{2,1,0:T(8,128)(2,1)S(1)}, u32[]{:S(2)}, u32[]{:S(2)}) collective-permute-start(bf16[4,136,256]{2,1,0:T(8,128)(2,1)S(1)} %all_to_all.26.mine_ref), channel_id=1, source_target_pairs={{0,1},{1,0},{2,3},{3,2},{4,5},{5,4},{6,7},{7,6},{8,9},{9,8},{10,11... | collective-permute-start | bytes 835592 | tf_op jit(solution)/shard_map/ppermute | solution.py:399
  43.7 1.5 %collective-permute-done.4.theirs_ref = bf16[4,136,256]{2,1,0:T(8,128)(2,1)S(1)} collective-permute-done((bf16[4,136,256]{2,1,0:T(8,128)(2,1)S(1)}, bf16[4,136,256]{2,1,0:T(8,128)(2,1)S(1)}, u32[]{:S(2)}, u32[]{:S(2)}) %collective-permute-start.4) | collective-permute-done | bytes 278560 | tf_op jit(solution)/shard_map/ppermute | solution.py:399
  45.9 4.7 %all-to-all-start.2 = ((bf16[4,8,2048]{2,1,0:T(8,128)(2,1)}), bf16[4,8,2048]{2,1,0:T(8,128)(2,1)S(1)}, u32[]{:S(2)}, u32[]{:S(2)}) async-start(bf16[4,8,2048]{2,1,0:T(8,128)(2,1)} %shard_map.130), calls=%async_computation.2 | async-start | bytes 262144 | tf_op jit(solution)/shard_map/all_to_all | solution.py:349
  51.3 3.2 %all-to-all-done.2.mod_ref = bf16[4,8,2048]{2,1,0:T(8,128)(2,1)S(1)} async-done(((bf16[4,8,2048]{2,1,0:T(8,128)(2,1)}), bf16[4,8,2048]{2,1,0:T(8,128)(2,1)S(1)}, u32[]{:S(2)}, u32[]{:S(2)}) %all-to-all-start.2) | async-done | bytes 131104 | tf_op jit(solution)/shard_map/all_to_all | solution.py:349
  54.5 1.7 %shard_map.136 = bf16[8,2,128,256]{3,2,1,0:T(8,128)(2,1)} custom-call(bf16[4,136,256]{2,1,0:T(8,128)(2,1)S(1)} %all_to_all.26.mine_ref, bf16[4,136,256]{2,1,0:T(8,128)(2,1)S(1)} %collective-permute-done.4.theirs_ref, f32[128,256]{1,0:T(8,128)S(1)} %get-tuple-element.19.square_ref, bf16[4,8,2048]{2,1,0:T(8,128)(2,1)S(1)} %all-to-all-done.2.mod_ref, ...), custom_call_target="tpu_custom_call" | custom-call | flops 1000000000 | tf_op jit(solution)/shard_map/pallas_call | solution.py:410
  56.2 5.7 %all-to-all-start.3 = ((bf16[8,2,128,256]{3,2,1,0:T(8,128)(2,1)}), bf16[8,2,128,256]{3,2,1,0:T(8,128)(2,1)S(1)}, u32[]{:S(2)}, u32[]{:S(2)}) async-start(bf16[8,2,128,256]{3,2,1,0:T(8,128)(2,1)} %shard_map.136), calls=%async_computation.3 | async-start | bytes 2097152 | tf_op jit(solution)/shard_map/all_to_all | solution.py:349
  61.9 2.5 %collective-permute-start = (bf16[32,2048]{1,0:T(8,128)(2,1)S(1)}, bf16[32,2048]{1,0:T(8,128)(2,1)S(1)}, u32[]{:S(2)}, u32[]{:S(2)}) collective-permute-start(bf16[32,2048]{1,0:T(8,128)(2,1)S(1)} %copy-done.4), channel_id=1, source_target_pairs={{0,2},{2,4},{4,6},{6,0},{1,3},{3,5},{5,7},{7,1},{8,10},{10,12},{12... | collective-permute-start | bytes 393224 | tf_op jit(solution)/shard_map/ppermute | solution.py:358
  64.4 4.0 %collective-permute-start.1 = (bf16[32,2048]{1,0:T(8,128)(2,1)S(1)}, bf16[32,2048]{1,0:T(8,128)(2,1)S(1)}, u32[]{:S(2)}, u32[]{:S(2)}) collective-permute-start(bf16[32,2048]{1,0:T(8,128)(2,1)S(1)} %copy-done.4), channel_id=1, source_target_pairs={{0,4},{2,6},{4,0},{6,2},{1,5},{3,7},{5,1},{7,3},{8,12},{10,14},{12... | collective-permute-start | bytes 393224 | tf_op jit(solution)/shard_map/ppermute | solution.py:358
  68.4 3.0 %collective-permute-start.2 = (bf16[32,2048]{1,0:T(8,128)(2,1)S(1)}, bf16[32,2048]{1,0:T(8,128)(2,1)S(1)}, u32[]{:S(2)}, u32[]{:S(2)}) collective-permute-start(bf16[32,2048]{1,0:T(8,128)(2,1)S(1)} %copy-done.4), channel_id=1, source_target_pairs={{0,6},{2,0},{4,2},{6,4},{1,7},{3,1},{5,3},{7,5},{8,14},{10,8},{12,... | collective-permute-start | bytes 393224 | tf_op jit(solution)/shard_map/ppermute | solution.py:358
  71.4 1.9 %collective-permute-start.8 = (bf16[256,2048]{1,0:T(8,128)(2,1)}, bf16[256,2048]{1,0:T(8,128)(2,1)}, u32[]{:S(2)}, u32[]{:S(2)}) collective-permute-start(bf16[256,2048]{1,0:T(8,128)(2,1)} %w_hbm.1), channel_id=1, source_target_pairs={{0,1},{1,0},{2,3},{3,2},{4,5},{5,4},{6,7},{7,6},{8,9},{9,8},{10,11... | collective-permute-start | bytes 3145736 | tf_op jit(solution)/shard_map/ppermute | solution.py:394
  73.3 1.9 %collective-permute-done.2.p3_ref = bf16[32,2048]{1,0:T(8,128)(2,1)S(1)} collective-permute-done((bf16[32,2048]{1,0:T(8,128)(2,1)S(1)}, bf16[32,2048]{1,0:T(8,128)(2,1)S(1)}, u32[]{:S(2)}, u32[]{:S(2)}) %collective-permute-start.2) | collective-permute-done | bytes 131104 | tf_op jit(solution)/shard_map/ppermute | solution.py:358
  75.3 2.1 %collective-permute-start.3 = (bf16[4,32,2048]{2,1,0:T(8,128)(2,1)S(1)}, bf16[4,32,2048]{2,1,0:T(8,128)(2,1)S(1)}, u32[]{:S(2)}, u32[]{:S(2)}) collective-permute-start(bf16[4,32,2048]{2,1,0:T(8,128)(2,1)S(1)} %shard_map.127.mine_hbm), channel_id=1, source_target_pairs={{0,1},{1,0},{2,3},{3,2},{4,5},{5,4},{6,7},{7,6},{8,9},{9,8},{10,11... | collective-permute-start | bytes 1572872 | tf_op jit(solution)/shard_map/ppermute | solution.py:398
  77.3 1.9 %collective-permute-done.3.theirs_hbm = bf16[4,32,2048]{2,1,0:T(8,128)(2,1)S(1)} collective-permute-done((bf16[4,32,2048]{2,1,0:T(8,128)(2,1)S(1)}, bf16[4,32,2048]{2,1,0:T(8,128)(2,1)S(1)}, u32[]{:S(2)}, u32[]{:S(2)}) %collective-permute-start.3) | collective-permute-done | bytes 524320 | tf_op jit(solution)/shard_map/ppermute | solution.py:398
  80.0 2.2 %shard_map.131 = (bf16[2,128,256]{2,1,0:T(8,128)(2,1)S(1)}, bf16[2,128,256]{2,1,0:T(8,128)(2,1)S(1)}, bf16[2,96,256]{2,1,0:T(8,128)(2,1)S(1)}, f32[1,2048]{1,0:T(1,128)S(1)}, bf16[256,2048]{1,0:T(8,128)(2,1)S(1)}) custom-call(bf16[4,32,2048]{2,1,0:T(8,128)(2,1)} %copy-done.3, bf16[4,32,2048]{2,1,0:T(8,128)(2,1)} %copy-done.10, ...), custom_call_target="tpu_custom_call" | custom-call | flops 2000000000 | tf_op jit(solution)/shard_map/pallas_call | solution.py:415
  82.3 3.5 %collective-permute-start.5 = (bf16[2,128,256]{2,1,0:T(8,128)(2,1)S(1)}, bf16[2,128,256]{2,1,0:T(8,128)(2,1)S(1)}, u32[]{:S(2)}, u32[]{:S(2)}) collective-permute-start(bf16[2,128,256]{2,1,0:T(8,128)(2,1)S(1)} %get-tuple-element.16.tail_hbm), channel_id=1, source_target_pairs={{0,8},{8,16},{16,24},{24,32},{32,40},{40,48},{48,56},{56,64},{64,7... | collective-permute-start | bytes 393224 | tf_op jit(solution)/shard_map/ppermute | solution.py:431
  85.9 2.5 %collective-permute-start.6 = (bf16[2,96,256]{2,1,0:T(8,128)(2,1)S(1)}, bf16[2,96,256]{2,1,0:T(8,128)(2,1)S(1)}, u32[]{:S(2)}, u32[]{:S(2)}) collective-permute-start(bf16[2,96,256]{2,1,0:T(8,128)(2,1)S(1)} %get-tuple-element.18), channel_id=1, source_target_pairs={{8,0},{16,8},{24,16},{32,24},{40,32},{48,40},{56,48},{64,56},{72,6... | collective-permute-start | bytes 294920 | tf_op jit(solution)/shard_map/ppermute | solution.py:432
  91.0 3.5 %collective-permute-done.6.next_ref = bf16[2,96,256]{2,1,0:T(8,128)(2,1)S(1)} collective-permute-done((bf16[2,96,256]{2,1,0:T(8,128)(2,1)S(1)}, bf16[2,96,256]{2,1,0:T(8,128)(2,1)S(1)}, u32[]{:S(2)}, u32[]{:S(2)}) %collective-permute-start.6) | collective-permute-done | bytes 98336 | tf_op jit(solution)/shard_map/ppermute | solution.py:432
  94.5 2.5 %shard_map.137 = (bf16[128,256]{1,0:T(8,128)(2,1)S(1)}, bf16[128,256]{1,0:T(8,128)(2,1)S(1)}, bf16[256,2048]{1,0:T(8,128)(2,1)S(1)}) custom-call(bf16[256,256]{1,0:T(8,128)(2,1)} %copy-done.8, bf16[2,128,256]{2,1,0:T(8,128)(2,1)S(1)} %collective-permute-done.5.prev_ref, bf16[2,128,256]{2,1,0:T(8,128)(2,1)} %copy-done.7, bf16[2,128,256]{2,1,0:T(8,128)(2,1)} %copy-done.6, ...), custom_call_target="tpu_custom_call" | custom-call | flops 1000000000 | tf_op jit(solution)/shard_map/pallas_call | solution.py:439
  97.1 1.9 %collective-permute-start.7 = (bf16[128,256]{1,0:T(8,128)(2,1)S(1)}, bf16[128,256]{1,0:T(8,128)(2,1)S(1)}, u32[]{:S(2)}, u32[]{:S(2)}) collective-permute-start(bf16[128,256]{1,0:T(8,128)(2,1)S(1)} %get-tuple-element.23), channel_id=1, source_target_pairs={{0,1},{1,0},{2,3},{3,2},{4,5},{5,4},{6,7},{7,6},{8,9},{9,8},{10,11... | collective-permute-start | bytes 196616 | tf_op jit(solution)/shard_map/ppermute | solution.py:452
  100.2 1.5 %shard_map.139 = bf16[4,32,2048]{2,1,0:T(8,128)(2,1)S(1)} custom-call(f32[128,2048]{1,0:T(8,128)S(1)} %shard_map.138.own_ref, bf16[128,256]{1,0:T(8,128)(2,1)S(1)} %collective-permute-done.7.got_ref, bf16[256,2048]{1,0:T(8,128)(2,1)} %collective-permute-done.8.w_ref), custom_call_target="tpu_custom_call" | custom-call | flops 1000000000 | tf_op jit(solution)/shard_map/pallas_call | solution.py:454
  101.8 13.3 %all_to_all.27.parts_ref = bf16[4,32,2048]{2,1,0:T(8,128)(2,1)S(1)} all-to-all(bf16[4,32,2048]{2,1,0:T(8,128)(2,1)S(1)} %shard_map.139), channel_id=1, replica_groups=mesh['zh'=8,'zl'=2,'y'=4,'x'=4,'c'=2] {'x'}, dimensions={0} | all-to-all | bytes 1048576 | tf_op jit(solution)/shard_map/all_to_all | solution.py:349
  (38 shorter events, 6.9 us)
Async XLA Ops:
  30.8 23.7 %copy-start = (bf16[2048,256]{1,0:T(8,128)(2,1)S(1)}, bf16[2048,256]{1,0:T(8,128)(2,1)}, u32[]{:S(2)}) copy-start(bf16[2048,256]{1,0:T(8,128)(2,1)} %wk_ref.3) | copy-start | bytes 3145732
  30.8 23.7 %copy-start.1 = (bf16[2048,256]{1,0:T(8,128)(2,1)S(1)}, bf16[2048,256]{1,0:T(8,128)(2,1)}, u32[]{:S(2)}) copy-start(bf16[2048,256]{1,0:T(8,128)(2,1)} %wv_ref.3) | copy-start | bytes 3145732
  41.8 3.4 %collective-permute-start.4 = (bf16[4,136,256]{2,1,0:T(8,128)(2,1)S(1)}, bf16[4,136,256]{2,1,0:T(8,128)(2,1)S(1)}, u32[]{:S(2)}, u32[]{:S(2)}) collective-permute-start(bf16[4,136,256]{2,1,0:T(8,128)(2,1)S(1)} %all_to_all.26.mine_ref), channel_id=1, source_target_pairs={{0,1},{1,0},{2,3},{3,2},{4,5},{5,4},{6,7},{7,6},{8,9},{9,8},{10,11... | collective-permute-start | bytes 835592 | tf_op jit(solution)/shard_map/ppermute | solution.py:399
  45.9 8.6 %all-to-all-start.2 = ((bf16[4,8,2048]{2,1,0:T(8,128)(2,1)}), bf16[4,8,2048]{2,1,0:T(8,128)(2,1)S(1)}, u32[]{:S(2)}, u32[]{:S(2)}) async-start(bf16[4,8,2048]{2,1,0:T(8,128)(2,1)} %shard_map.130), calls=%async_computation.2 | async-start | bytes 262144 | tf_op jit(solution)/shard_map/all_to_all | solution.py:349
  56.2 5.7 %copy-start.4 = (bf16[32,2048]{1,0:T(8,128)(2,1)S(1)}, bf16[32,2048]{1,0:T(8,128)(2,1)}, u32[]{:S(2)}) copy-start(bf16[32,2048]{1,0:T(8,128)(2,1)} %lat_ref.1) | copy-start | bytes 393220
  56.2 38.3 %all-to-all-start.3 = ((bf16[8,2,128,256]{3,2,1,0:T(8,128)(2,1)}), bf16[8,2,128,256]{3,2,1,0:T(8,128)(2,1)S(1)}, u32[]{:S(2)}, u32[]{:S(2)}) async-start(bf16[8,2,128,256]{3,2,1,0:T(8,128)(2,1)} %shard_map.136), calls=%async_computation.3 | async-start | bytes 2097152 | tf_op jit(solution)/shard_map/all_to_all | solution.py:349
  61.9 11.4 %collective-permute-start = (bf16[32,2048]{1,0:T(8,128)(2,1)S(1)}, bf16[32,2048]{1,0:T(8,128)(2,1)S(1)}, u32[]{:S(2)}, u32[]{:S(2)}) collective-permute-start(bf16[32,2048]{1,0:T(8,128)(2,1)S(1)} %copy-done.4), channel_id=1, source_target_pairs={{0,2},{2,4},{4,6},{6,0},{1,3},{3,5},{5,7},{7,1},{8,10},{10,12},{12... | collective-permute-start | bytes 393224 | tf_op jit(solution)/shard_map/ppermute | solution.py:358
  64.4 9.0 %collective-permute-start.1 = (bf16[32,2048]{1,0:T(8,128)(2,1)S(1)}, bf16[32,2048]{1,0:T(8,128)(2,1)S(1)}, u32[]{:S(2)}, u32[]{:S(2)}) collective-permute-start(bf16[32,2048]{1,0:T(8,128)(2,1)S(1)} %copy-done.4), channel_id=1, source_target_pairs={{0,4},{2,6},{4,0},{6,2},{1,5},{3,7},{5,1},{7,3},{8,12},{10,14},{12... | collective-permute-start | bytes 393224 | tf_op jit(solution)/shard_map/ppermute | solution.py:358
  68.4 6.9 %collective-permute-start.2 = (bf16[32,2048]{1,0:T(8,128)(2,1)S(1)}, bf16[32,2048]{1,0:T(8,128)(2,1)S(1)}, u32[]{:S(2)}, u32[]{:S(2)}) collective-permute-start(bf16[32,2048]{1,0:T(8,128)(2,1)S(1)} %copy-done.4), channel_id=1, source_target_pairs={{0,6},{2,0},{4,2},{6,4},{1,7},{3,1},{5,3},{7,5},{8,14},{10,8},{12,... | collective-permute-start | bytes 393224 | tf_op jit(solution)/shard_map/ppermute | solution.py:358
  71.4 27.9 %collective-permute-start.8 = (bf16[256,2048]{1,0:T(8,128)(2,1)}, bf16[256,2048]{1,0:T(8,128)(2,1)}, u32[]{:S(2)}, u32[]{:S(2)}) collective-permute-start(bf16[256,2048]{1,0:T(8,128)(2,1)} %w_hbm.1), channel_id=1, source_target_pairs={{0,1},{1,0},{2,3},{3,2},{4,5},{5,4},{6,7},{7,6},{8,9},{9,8},{10,11... | collective-permute-start | bytes 3145736 | tf_op jit(solution)/shard_map/ppermute | solution.py:394
  75.3 4.0 %copy-start.3 = (bf16[4,32,2048]{2,1,0:T(8,128)(2,1)}, bf16[4,32,2048]{2,1,0:T(8,128)(2,1)S(1)}, u32[]{:S(2)}) copy-start(bf16[4,32,2048]{2,1,0:T(8,128)(2,1)S(1)} %shard_map.127.mine_hbm) | copy-start | bytes 1572868
  75.3 10.5 %copy-start.9 = (f32[16,15,31]{2,0,1:T(8,128)S(1)}, f32[16,15,31]{2,0,1:T(8,128)}, u32[]{:S(2)}) copy-start(f32[16,15,31]{2,0,1:T(8,128)} %param.25) | copy-start | bytes 89284
  75.3 3.9 %collective-permute-start.3 = (bf16[4,32,2048]{2,1,0:T(8,128)(2,1)S(1)}, bf16[4,32,2048]{2,1,0:T(8,128)(2,1)S(1)}, u32[]{:S(2)}, u32[]{:S(2)}) collective-permute-start(bf16[4,32,2048]{2,1,0:T(8,128)(2,1)S(1)} %shard_map.127.mine_hbm), channel_id=1, source_target_pairs={{0,1},{1,0},{2,3},{3,2},{4,5},{5,4},{6,7},{7,6},{8,9},{9,8},{10,11... | collective-permute-start | bytes 1572872 | tf_op jit(solution)/shard_map/ppermute | solution.py:398
  79.2 0.8 copy-start.10
  82.2 3.6 %copy-start.6 = (bf16[2,128,256]{2,1,0:T(8,128)(2,1)}, bf16[2,128,256]{2,1,0:T(8,128)(2,1)S(1)}, u32[]{:S(2)}) copy-start(bf16[2,128,256]{2,1,0:T(8,128)(2,1)S(1)} %get-tuple-element.16.tail_hbm) | copy-start | bytes 393220
  82.2 3.6 %copy-start.7 = (bf16[2,128,256]{2,1,0:T(8,128)(2,1)}, bf16[2,128,256]{2,1,0:T(8,128)(2,1)S(1)}, u32[]{:S(2)}) copy-start(bf16[2,128,256]{2,1,0:T(8,128)(2,1)S(1)} %get-tuple-element.17.head_hbm) | copy-start | bytes 393220
  82.3 7.6 %copy-start.5 = (bf16[2048,256]{1,0:T(8,128)(2,1)S(1)}, bf16[2048,256]{1,0:T(8,128)(2,1)}, u32[]{:S(2)}) copy-start(bf16[2048,256]{1,0:T(8,128)(2,1)} %wq_ref.1) | copy-start | bytes 3145732
  82.3 12.3 %collective-permute-start.5 = (bf16[2,128,256]{2,1,0:T(8,128)(2,1)S(1)}, bf16[2,128,256]{2,1,0:T(8,128)(2,1)S(1)}, u32[]{:S(2)}, u32[]{:S(2)}) collective-permute-start(bf16[2,128,256]{2,1,0:T(8,128)(2,1)S(1)} %get-tuple-element.16.tail_hbm), channel_id=1, source_target_pairs={{0,8},{8,16},{16,24},{24,32},{32,40},{40,48},{48,56},{56,64},{64,7... | collective-permute-start | bytes 393224 | tf_op jit(solution)/shard_map/ppermute | solution.py:431
  85.9 8.6 %collective-permute-start.6 = (bf16[2,96,256]{2,1,0:T(8,128)(2,1)S(1)}, bf16[2,96,256]{2,1,0:T(8,128)(2,1)S(1)}, u32[]{:S(2)}, u32[]{:S(2)}) collective-permute-start(bf16[2,96,256]{2,1,0:T(8,128)(2,1)S(1)} %get-tuple-element.18), channel_id=1, source_target_pairs={{8,0},{16,8},{24,16},{32,24},{40,32},{48,40},{56,48},{64,56},{72,6... | collective-permute-start | bytes 294920 | tf_op jit(solution)/shard_map/ppermute | solution.py:432
  89.0 0.9 copy-start.2
  90.3 0.7 copy-start.8
  97.1 3.1 %collective-permute-start.7 = (bf16[128,256]{1,0:T(8,128)(2,1)S(1)}, bf16[128,256]{1,0:T(8,128)(2,1)S(1)}, u32[]{:S(2)}, u32[]{:S(2)}) collective-permute-start(bf16[128,256]{1,0:T(8,128)(2,1)S(1)} %get-tuple-element.23), channel_id=1, source_target_pairs={{0,1},{1,0},{2,3},{3,2},{4,5},{5,4},{6,7},{7,6},{8,9},{9,8},{10,11... | collective-permute-start | bytes 196616 | tf_op jit(solution)/shard_map/ppermute | solution.py:452
